TPU v7x, 256 devices: a whole 4x4x8 slice. The times are simulated.
256 devices in a mesh: sp: 16 (over y, x), tp: 16 (over z, core).
Axes of the slice: x: 4, y: 4, z: 8, core: 2. Of those that a mesh axis runs over, the one named last changes fastest.
Arguments:
- residual: bfloat16 [16384, 2048], P(('sp', 'tp')), may hold values from -6 to 6
- wide_query: bfloat16 [16384, 1024], P('sp', 'tp'), may hold values from -8 to 8
- narrow_query: bfloat16 [16384, 1024], P('sp', 'tp'), may hold values from -8 to 8
- wide_keys: bfloat16 [16384, 256], P('sp'), may hold values from -6 to 6
- narrow_keys: bfloat16 [16384, 256], P('sp'), may hold values from -6 to 6
- wide_values: bfloat16 [16384, 256], P('sp'), may hold values from -6 to 6
- narrow_values: bfloat16 [16384, 256], P('sp'), may hold values from -6 to 6
- wide_query_gain: float32 [64], replicated, may hold values from 1.2 to 10
- wide_key_gain: float32 [64], replicated, may hold values from 1.2 to 10
- narrow_query_gain: float32 [32], replicated, may hold values from 1.2 to 10
- narrow_key_gain: float32 [32], replicated, may hold values from 1.2 to 10
- wide_out: bfloat16 [1024, 2048], P('tp'), may hold values from -0.25 to 0.25
- narrow_out: bfloat16 [1024, 2048], P('tp'), may hold values from -0.25 to 0.25
- first_gain: float32 [2048], replicated, may hold values from 0.1 to 1.9
- first_bias: float32 [2048], replicated, may hold values from -1.8 to 1.8
- route_ids: int32 [16384, 2], P(('sp', 'tp')), may hold values from 0 to 31, all different within a row; in each aligned block of 64 rows (0 to 63, 64 to 127, ...) at most 5 rows name the same one
- route_weights: float32 [16384, 2], P(('sp', 'tp')), may hold values from 0.25 to 2.5
- expert_gate: bfloat16 [32, 2048, 3072], P('sp', None, 'tp'), may hold values from -0.125 to 0.125
- expert_up: bfloat16 [32, 2048, 3072], P('sp', None, 'tp'), may hold values from -0.125 to 0.125
- expert_down: bfloat16 [32, 3072, 2048], P('sp', 'tp'), may hold values from -0.109375 to 0.109375
- shared_gate: bfloat16 [2048, 256], replicated, may hold values from -0.125 to 0.125
- shared_up: bfloat16 [2048, 256], replicated, may hold values from -0.125 to 0.125
- shared_down: bfloat16 [256, 2048], replicated, may hold values from -0.375 to 0.375
- second_gain: float32 [2048], replicated, may hold values from 0.1 to 1.9
- second_bias: float32 [2048], replicated, may hold values from -1.8 to 1.8
Outputs:
- layer_output: bfloat16 [16384, 2048], P(('sp', 'tp'))
Inputs may be any that keep to these rules, and one draw needn't show every extreme that they name: `route_ids`: each row names 2 different experts. The rows of one device (aligned blocks of 64 rows) name each expert at most 5 times, and in every draw some expert is named exactly 5 times in the rows of some device.
All inputs are finite; a program needn't handle non-finite values.
Results may differ from a plain program's by a relative error of at most 0.02.
The roundings to bfloat16 on the way count: a program that leaves them out, or rounds other values in their place, can miss the bound.
Values may be sent and summed in bfloat16 or wider, within the bound.
No kernel may reach another device: no remote copies, remote signals or barrier semaphores. Data moves between devices by JAX's collectives and lax.ppermute only.
A program may use at most 128 MiB of HBM per device.

v0:
```python
import jax
import jax.numpy as jnp
from jax import lax
from jax.sharding import PartitionSpec as P

WIDE_HEADS = 16
WIDE_GROUPS = 4
NARROW_HEADS = 32
NARROW_GROUPS = 8
GRID_WIDTH = 64
SEQ_SHARDS = 4
LOCAL_EXPERTS = 2


EPS_HEAD = 1e-06
EPS_LAYER = 1e-05
ALPHA = 2.0**0.25
THETA = 10000.0


def swapped(x, axis, apart):
    return lax.ppermute(x, axis, [(i, i ^ 1 << apart) for i in range(lax.axis_size(axis))])


def head_norm(values, gain_vec):
    mean_square = jnp.mean(values * values, axis=-1, keepdims=True)
    return values * lax.rsqrt(mean_square + EPS_HEAD) * gain_vec


def rotate(values, position):
    half_size = values.shape[-1] // 2
    frequency = THETA ** (-jnp.arange(half_size, dtype=jnp.float32) / half_size)
    angles = position.astype(jnp.float32)[:, None] * frequency
    cosine = jnp.cos(angles)[:, None, :]
    sine_part = jnp.sin(angles)[:, None, :]
    leading = values[..., :half_size]
    trailing = values[..., half_size:]
    return jnp.concatenate(
        [leading * cosine - trailing * sine_part, trailing * cosine + leading * sine_part], axis=-1
    )


def grid_rotate(values, position):
    half_size = values.shape[-1] // 2
    grid_row = position // GRID_WIDTH
    grid_col = position % GRID_WIDTH
    return jnp.concatenate(
        [rotate(values[..., :half_size], grid_row), rotate(values[..., half_size:], grid_col)],
        axis=-1,
    )


def layer_norm(values, gain_vec, bias_vec):
    center = jnp.mean(values, axis=-1, keepdims=True)
    shifted = values - center
    variance = jnp.mean(shifted * shifted, axis=-1, keepdims=True)
    return (shifted * lax.rsqrt(variance + EPS_LAYER) * gain_vec + bias_vec).astype(jnp.bfloat16)


def prepare(queries, key_block, value_block, query_gain, key_gain, heads_total, groups, position):
    head_size = query_gain.shape[0]
    local_heads = queries.shape[1] // head_size
    group_index = lax.axis_index("tp") * local_heads // (heads_total // groups)
    query_rows = queries.reshape(queries.shape[0], local_heads, head_size).astype(jnp.float32)
    rotated_queries = grid_rotate(head_norm(query_rows, query_gain), position).astype(jnp.bfloat16)
    column_start = group_index * head_size
    key_rows = lax.dynamic_slice_in_dim(key_block, column_start, head_size, 1).astype(jnp.float32)[
        :, None, :
    ]
    rotated_keys = grid_rotate(head_norm(key_rows, key_gain), position)[:, 0, :].astype(
        jnp.bfloat16
    )
    value_rows = lax.dynamic_slice_in_dim(value_block, column_start, head_size, 1)
    return (rotated_queries, jnp.concatenate([rotated_keys, value_rows], axis=1))


def attend_local(rotated_queries, key_block, value_block):
    seg_rows, local_heads, head_size = rotated_queries.shape
    block_rows = min(512, seg_rows)
    score_scale = head_size ** (-0.5)
    blocks = rotated_queries.reshape(seg_rows // block_rows, block_rows, local_heads, head_size)

    def one_block(query_block):
        scores = (
            jnp.einsum("qhd,kd->hqk", query_block, key_block, preferred_element_type=jnp.float32)
            * score_scale
        )
        largest = jnp.max(scores, axis=-1, keepdims=True)
        weights = jnp.exp(scores - largest)
        weights = (weights / jnp.sum(weights, axis=-1, keepdims=True)).astype(jnp.bfloat16)
        return jnp.einsum(
            "hqk,kd->qhd", weights, value_block, preferred_element_type=jnp.float32
        ).astype(jnp.bfloat16)

    mixed_rows = lax.map(one_block, blocks)
    return mixed_rows.reshape(seg_rows, local_heads * head_size)


def local(
    residual,
    wide_query,
    narrow_query,
    wide_keys,
    narrow_keys,
    wide_values,
    narrow_values,
    wide_query_gain,
    wide_key_gain,
    narrow_query_gain,
    narrow_key_gain,
    wide_out,
    narrow_out,
    first_gain,
    first_bias,
    route_ids,
    route_weights,
    expert_gate,
    expert_up,
    expert_down,
    shared_gate,
    shared_up,
    shared_down,
    second_gain,
    second_bias,
):
    seg_rows = wide_query.shape[0]
    position = lax.axis_index("sp") % SEQ_SHARDS * seg_rows + jnp.arange(seg_rows, dtype=jnp.int32)
    wide_rotated, wide_pack = prepare(
        wide_query,
        wide_keys,
        wide_values,
        wide_query_gain,
        wide_key_gain,
        WIDE_HEADS,
        WIDE_GROUPS,
        position,
    )
    narrow_rotated, narrow_pack = prepare(
        narrow_query,
        narrow_keys,
        narrow_values,
        narrow_query_gain,
        narrow_key_gain,
        NARROW_HEADS,
        NARROW_GROUPS,
        position,
    )
    gathered = jnp.concatenate([wide_pack, narrow_pack], axis=1)
    for level in range(SEQ_SHARDS.bit_length() - 1):
        partner = swapped(gathered, "sp", level)
        is_upper = lax.axis_index("sp") // 2**level % 2 == 1
        gathered = jnp.where(
            is_upper,
            jnp.concatenate([partner, gathered], axis=0),
            jnp.concatenate([gathered, partner], axis=0),
        )
    wide_size = wide_query_gain.shape[0]
    narrow_size = narrow_query_gain.shape[0]
    narrow_start = 2 * wide_size
    wide_mixed = attend_local(
        wide_rotated, gathered[:, :wide_size], gathered[:, wide_size:narrow_start]
    )
    narrow_mixed = attend_local(
        narrow_rotated,
        gathered[:, narrow_start : narrow_start + narrow_size],
        gathered[:, narrow_start + narrow_size :],
    )
    wide_tokens, narrow_tokens = (
        lax.all_to_all(wide_mixed, "tp", split_axis=0, concat_axis=1, tiled=True),
        lax.all_to_all(narrow_mixed, "tp", split_axis=0, concat_axis=1, tiled=True),
    )
    running = jnp.dot(
        wide_tokens,
        lax.all_gather(wide_out, "tp", axis=0, tiled=True),
        preferred_element_type=jnp.float32,
    )
    projected = running + jnp.dot(
        narrow_tokens,
        lax.all_gather(narrow_out, "tp", axis=0, tiled=True),
        preferred_element_type=jnp.float32,
    )
    hidden = layer_norm(ALPHA * residual.astype(jnp.float32) + projected, first_gain, first_bias)
    device_rows = hidden.shape[0]
    model_width = hidden.shape[1]
    sp_size = lax.axis_size("sp")
    top_count = route_ids.shape[1]
    experts = LOCAL_EXPERTS * sp_size
    capacity = max(2, (5 * device_rows * top_count + 4 * experts - 1) // (4 * experts))
    flat_ids = route_ids.reshape(-1)
    expert_hits = (flat_ids[:, None] == jnp.arange(experts, dtype=jnp.int32)[None, :]).astype(
        jnp.int32
    )
    earlier = jnp.sum((jnp.cumsum(expert_hits, axis=0) - expert_hits) * expert_hits, axis=1)
    slot_index = flat_ids * capacity + earlier
    chosen = (
        slot_index[:, None] == jnp.arange(experts * capacity, dtype=jnp.int32)[None, :]
    ).astype(jnp.float32)
    chosen = chosen.reshape(device_rows, top_count, experts * capacity)
    placing = jnp.sum(chosen, axis=1).astype(jnp.bfloat16)
    mixing = jnp.sum(chosen * route_weights[:, :, None], axis=1)
    outgoing = jnp.einsum("rs,rd->sd", placing, hidden, preferred_element_type=jnp.float32).astype(
        jnp.bfloat16
    )
    outgoing = outgoing.reshape(sp_size, LOCAL_EXPERTS, capacity, model_width)
    piece_rows = lax.all_gather(
        lax.all_to_all(outgoing, "sp", split_axis=0, concat_axis=0, tiled=True),
        "tp",
        axis=0,
        tiled=True,
    )
    gate_values = jnp.einsum(
        "secd,edf->secf", piece_rows, expert_gate, preferred_element_type=jnp.float32
    )
    up_values = jnp.einsum(
        "secd,edf->secf", piece_rows, expert_up, preferred_element_type=jnp.float32
    )
    active = (jax.nn.silu(gate_values) * up_values).astype(jnp.bfloat16)
    partial_value = jnp.einsum(
        "secf,efd->secd", active, expert_down, preferred_element_type=jnp.float32
    )
    rounded = lax.optimization_barrier(partial_value.astype(jnp.bfloat16))
    partials = rounded.astype(jnp.float32)
    summed = lax.psum_scatter(partials.astype(jnp.bfloat16), "tp", scatter_dimension=0, tiled=True)
    returned = lax.all_to_all(summed, "sp", split_axis=0, concat_axis=0, tiled=True)
    routed = jnp.dot(mixing, returned.reshape(-1, model_width).astype(jnp.float32))
    shared_gate_values = jnp.dot(hidden, shared_gate, preferred_element_type=jnp.float32)
    shared_up_values = jnp.dot(hidden, shared_up, preferred_element_type=jnp.float32)
    shared_active = (jax.nn.silu(shared_gate_values) * shared_up_values).astype(jnp.bfloat16)
    shared_output = jnp.dot(shared_active, shared_down, preferred_element_type=jnp.float32)
    return layer_norm(
        ALPHA * hidden.astype(jnp.float32) + routed + shared_output, second_gain, second_bias
    )


def solution(mesh):
    in_specs = (
        P(("sp", "tp"), None),
        P("sp", "tp"),
        P("sp", "tp"),
        P("sp", None),
        P("sp", None),
        P("sp", None),
        P("sp", None),
        P(),
        P(),
        P(),
        P(),
        P("tp", None),
        P("tp", None),
        P(),
        P(),
        P(("sp", "tp"), None),
        P(("sp", "tp"), None),
        P("sp", None, "tp"),
        P("sp", None, "tp"),
        P("sp", "tp", None),
        P(),
        P(),
        P(),
        P(),
        P(),
    )
    out_specs = P(("sp", "tp"), None)
    return jax.shard_map(local, mesh=mesh, in_specs=in_specs, out_specs=out_specs, check_vma=False)
```

profile of v0, /device:TPU:1, one launch (start us, length us, event | category | flops | bytes accessed | tf_op | source)
XLA Modules:
  0.0 330.2 jit_solution(2909898347180493930)
XLA Ops:
  12.6 2.1 collective-permute-start
  15.7 6.6 %collective-permute-done = bf16[1024,192]{0,1:T(8,128)(2,1)} collective-permute-done((bf16[1024,192]{0,1:T(8,128)(2,1)S(1)}, bf16[1024,192]{0,1:T(8,128)(2,1)}, u32[]{:S(2)}, u32[]{:S(2)}) %collective-permute-start) | collective-permute-done | bytes 393248 | tf_op jit(solution)/shard_map/ppermute | solution.py:22
  22.3 1.4 maximum_select_fusion.1
  23.6 4.2 %collective-permute-start.1 = (bf16[2048,192]{0,1:T(8,128)(2,1)S(1)}, bf16[2048,192]{0,1:T(8,128)(2,1)S(1)}, u32[]{:S(2)}, u32[]{:S(2)}) collective-permute-start(bf16[2048,192]{0,1:T(8,128)(2,1)S(1)} %maximum_select_fusion.1), channel_id=1, source_target_pairs={{0,32},{16,48},{32,0},{48,16},{64,96},{80,112},{96,64},{112,80},{1... | collective-permute-start | bytes 2359304 | tf_op jit(solution)/shard_map/ppermute | solution.py:22
  33.4 10.5 %collective-permute-done.1 = bf16[2048,192]{0,1:T(8,128)(2,1)S(1)} collective-permute-done((bf16[2048,192]{0,1:T(8,128)(2,1)S(1)}, bf16[2048,192]{0,1:T(8,128)(2,1)S(1)}, u32[]{:S(2)}, u32[]{:S(2)}) %collective-permute-start.1) | collective-permute-done | bytes 786464 | tf_op jit(solution)/shard_map/ppermute | solution.py:22
  45.9 1.5 copy.143
  48.7 10.7 %while.20 = (s32[]{:T(128)}, bf16[2,512,1,64]{1,3,2,0:T(8,128)(2,1)S(1)}, bf16[2,512,1,64]{1,3,2,0:T(8,128)(2,1)S(1)}, bf16[4096,64]{1,0:T(8,128)(2,1)S(1)}, bf16[4096,64]{1,0:T(8,128)(2,1)}, /*index=5*/s32[]{:T(128)}) while((s32[]{:T(128)}, bf16[2,512,1,64]{1,3,2,0:T(8,128)(2,1)S(1)}, bf16[2,512,1,64]{1,3,2,0:T(8,128)(2,1)S(1)}, ...), condition=%wide.region_6.7_spmd, body=%wide.region_3.6_spmd.sunk | while | flops 555777024 | bytes 29501552 | solution.py:95
  48.7 1.4 multiply_reduce_fusion.4
  50.1 1.5 fusion.220
  51.6 2.4 fusion.221
  54.1 1.4 multiply_reduce_fusion.4
  55.5 1.5 fusion.220
  57.0 2.4 fusion.221
  60.8 11.1 %all-to-all-start = ((bf16[16,2,2048]{2,1,0:T(2,128)(2,1)}), bf16[16,2,2048]{2,1,0:T(2,128)(2,1)S(1)}, u32[]{:S(2)}, u32[]{:S(2)}) async-start(bf16[16,2,2048]{2,1,0:T(2,128)(2,1)} %reshape.649), calls=%async_computation | async-start | bytes 262144 | tf_op jit(solution)/shard_map/all_to_all | solution.py:169
  73.0 23.8 %while.21 = (s32[]{:T(128)}, bf16[2,512,2,32]{1,3,2,0:T(8,128)(2,1)S(1)}, bf16[2,512,2,32]{1,3,2,0:T(8,128)(2,1)S(1)}, bf16[4096,32]{0,1:T(8,128)(2,1)S(1)}, bf16[4096,32]{0,1:T(8,128)(2,1)S(1)}, /*index=5*/s32[]{:T(128)}) while((s32[]{:T(128)}, bf16[2,512,2,32]{1,3,2,0:T(8,128)(2,1)S(1)}, bf16[2,512,2,32]{1,3,2,0:T(8,128)(2,1)S(1)}, ...), condition=%wide.region_11.12_spmd, body=%wide.region_8.11_spmd.sunk | while | flops 834708480 | bytes 992337 | solution.py:95
  73.0 5.9 %fusion.228 = f32[2,512]{1,0:T(2,128)S(1)} fusion(bf16[4096,32]{0,1:T(8,128)(2,1)S(1)} %get-tuple-element.287, bf16[2,512,2,32]{1,3,2,0:T(8,128)(2,1)S(1)} %get-tuple-element.286, s32[]{:T(128)S(6)} %copy.193), kind=kOutput, calls=%fused_computation.205.clone.1 | convolution fusion | flops 281022464 | bytes 331780 | tf_op jit(solution)/shard_map/while/body/eval_jaxpr/sub | solution.py:89
  78.9 6.0 %fusion.229 = bf16[2,512,2,32]{1,3,2,0:T(8,128)(2,1)S(1)} fusion(bf16[2,512,2,32]{1,3,2,0:T(8,128)(2,1)S(1)} %get-tuple-element.279, s32[]{:T(128)S(6)} %copy.193, f32[2,512]{1,0:T(2,128)S(1)} %fusion.228, bf16[4096,32]{0,1:T(8,128)(2,1)S(1)} %get-tuple-element.288, bf16[4096,32]{0,1:T(8,128)(2,1)S(1)} %get-tuple-element.287, ...), kind=kOutput, calls=%fused_computation.28.clone.1 | convolution fusion | flops 553686016 | bytes 660480 | tf_op jit(solution)/shard_map/while/body/eval_jaxpr/hqk,kd->qhd/dot_general | solution.py:91
  84.9 5.9 %fusion.228 = f32[2,512]{1,0:T(2,128)S(1)} fusion(bf16[4096,32]{0,1:T(8,128)(2,1)S(1)} %get-tuple-element.287, bf16[2,512,2,32]{1,3,2,0:T(8,128)(2,1)S(1)} %get-tuple-element.286, s32[]{:T(128)S(6)} %copy.193), kind=kOutput, calls=%fused_computation.205.clone.1 | convolution fusion | flops 281022464 | bytes 331780 | tf_op jit(solution)/shard_map/while/body/eval_jaxpr/sub | solution.py:89
  90.8 6.0 %fusion.229 = bf16[2,512,2,32]{1,3,2,0:T(8,128)(2,1)S(1)} fusion(bf16[2,512,2,32]{1,3,2,0:T(8,128)(2,1)S(1)} %get-tuple-element.279, s32[]{:T(128)S(6)} %copy.193, f32[2,512]{1,0:T(2,128)S(1)} %fusion.228, bf16[4096,32]{0,1:T(8,128)(2,1)S(1)} %get-tuple-element.288, bf16[4096,32]{0,1:T(8,128)(2,1)S(1)} %get-tuple-element.287, ...), kind=kOutput, calls=%fused_computation.28.clone.1 | convolution fusion | flops 553686016 | bytes 660480 | tf_op jit(solution)/shard_map/while/body/eval_jaxpr/hqk,kd->qhd/dot_general | solution.py:91
  98.1 7.4 %all-to-all-start.1 = ((bf16[16,2,2048]{2,1,0:T(2,128)(2,1)}), bf16[16,2,2048]{2,1,0:T(2,128)(2,1)S(1)}, u32[]{:S(2)}, u32[]{:S(2)}) async-start(bf16[16,2,2048]{2,1,0:T(2,128)(2,1)} %reshape.651), calls=%async_computation.1 | async-start | bytes 262144 | tf_op jit(solution)/shard_map/all_to_all | solution.py:170
  106.7 7.7 %all-to-all-done.1 = bf16[16,2,2048]{2,1,0:T(2,128)(2,1)S(1)} async-done(((bf16[16,2,2048]{2,1,0:T(2,128)(2,1)}), bf16[16,2,2048]{2,1,0:T(2,128)(2,1)S(1)}, u32[]{:S(2)}, u32[]{:S(2)}) %all-to-all-start.1) | async-done | bytes 131104 | tf_op jit(solution)/shard_map/all_to_all | solution.py:170
  114.6 3.1 fusion.185
  117.8 3.2 fusion.183
  122.8 19.6 %all_to_all.48 = bf16[16,2,5,2048]{3,1,2,0:T(2,128)(2,1)S(1)} all-to-all(bf16[16,2,5,2048]{3,1,2,0:T(2,128)(2,1)S(1)} %copy.154), channel_id=1, replica_groups=mesh['sp'=16,'tp'=16] {'sp'}, dimensions={0} | all-to-all | bytes 1310720 | tf_op jit(solution)/shard_map/all_to_all | solution.py:206
  143.5 59.8 %all-gather.8.cloned.1.call-done = bf16[256,2,5,2048]{3,0,2,1:T(8,128)(2,1)} async-done(((bf16[16,2,5,2048]{3,0,2,1:T(8,128)(2,1)}), bf16[256,2,5,2048]{3,0,2,1:T(8,128)(2,1)}) %all-gather.8.cloned.1.call-update) | async-done | bytes 10485776 | tf_op jit(solution)/shard_map/all_gather | solution.py:205
  203.2 8.9 %fusion.90 = f32[2,256,5,192]{1,3,2,0:T(8,128)} fusion(bf16[256,2,5,2048]{3,0,2,1:T(8,128)(2,1)} %all-gather.8.cloned.1.call-done, bf16[2,2048,192]{1,2,0:T(8,128)(2,1)S(1)} %copy-done.2), kind=kOutput, calls=%fused_computation.58 | convolution fusion | flops 2013265920 | bytes 14024704 | tf_op jit(solution)/shard_map/secd,edf->secf/dot_general | solution.py:214
  212.1 17.2 %convert_bitcast_fusion = bf16[256,2,5,2048]{3,0,2,1:T(8,128)(2,1)} fusion(f32[2,256,5,192]{1,3,2,0:T(8,128)} %fusion.90, bf16[256,2,5,2048]{3,0,2,1:T(8,128)(2,1)} %all-gather.8.cloned.1.call-done, bf16[2,192,2048]{2,1,0:T(8,128)(2,1)S(1)} %copy-done, bf16[2,2048,192]{1,2,0:T(8,128)(2,1)} %param.46), kind=kOutput, calls=%fused_computation.43 | convolution fusion | flops 4034723840 | bytes 26083328 | tf_op jit(solution)/shard_map/secf,efd->secd/dot_general | solution.py:218
  229.4 70.3 %reduce-scatter.2.cloned.1.call-done = bf16[16,2,5,2048]{3,0,2,1:T(8,128)(2,1)} async-done(((bf16[256,2,5,2048]{3,0,2,1:T(8,128)(2,1)}), bf16[16,2,5,2048]{3,0,2,1:T(8,128)(2,1)}) %reduce-scatter.2.cloned.1.call-update) | async-done | bytes 655376 | tf_op jit(solution)/shard_map/reduce_scatter | solution.py:223
  299.6 2.6 copy.156
  302.2 6.5 %all-to-all-start.3 = ((bf16[16,2,5,2048]{3,1,2,0:T(2,128)(2,1)}), bf16[16,2,5,2048]{3,1,2,0:T(2,128)(2,1)S(1)}, u32[]{:S(2)}, u32[]{:S(2)}) async-start(bf16[16,2,5,2048]{3,1,2,0:T(2,128)(2,1)} %copy.156), calls=%async_computation.4 | async-start | bytes 1310720 | tf_op jit(solution)/shard_map/all_to_all | solution.py:224
  309.7 8.8 %all-to-all-done.3 = bf16[16,2,5,2048]{3,1,2,0:T(2,128)(2,1)S(1)} async-done(((bf16[16,2,5,2048]{3,1,2,0:T(2,128)(2,1)}), bf16[16,2,5,2048]{3,1,2,0:T(2,128)(2,1)S(1)}, u32[]{:S(2)}, u32[]{:S(2)}) %all-to-all-start.3) | async-done | bytes 655392 | tf_op jit(solution)/shard_map/all_to_all | solution.py:224
  320.1 2.5 fusion.184
  (137 shorter events, 27.2 us)
Async XLA Ops:
  6.5 205.6 %copy-start = (bf16[2,192,2048]{2,1,0:T(8,128)(2,1)S(1)}, bf16[2,192,2048]{2,1,0:T(8,128)(2,1)}, u32[]{:S(2)}) copy-start(bf16[2,192,2048]{2,1,0:T(8,128)(2,1)} %param.48) | copy-start | bytes 4718596
  6.5 4.0 %copy-start.19 = (f32[32]{0:T(128)S(1)}, f32[32]{0:T(128)}, u32[]{:S(2)}) copy-start(f32[32]{0:T(128)} %param.39) | copy-start | bytes 388
  6.5 4.4 %copy-start.5 = (bf16[1024,64]{0,1:T(8,128)(2,1)S(1)}, bf16[1024,64]{0,1:T(8,128)(2,1)}, u32[]{:S(2)}) copy-start(bf16[1024,64]{0,1:T(8,128)(2,1)} %param.30) | copy-start | bytes 393220
  6.5 4.6 %copy-start.20 = (f32[64]{0:T(128)S(1)}, f32[64]{0:T(128)}, u32[]{:S(2)}) copy-start(f32[64]{0:T(128)} %param.36) | copy-start | bytes 772
  6.5 4.7 %copy-start.21 = (f32[64]{0:T(128)S(1)}, f32[64]{0:T(128)}, u32[]{:S(2)}) copy-start(f32[64]{0:T(128)} %param.37) | copy-start | bytes 772
  6.5 108.1 %all-gather.4.cloned.1.call-start = ((), (), s32[]{:S(2)}) async-start(), calls=%async_computation.5 | async-start | bytes 4456448 | tf_op jit(solution)/shard_map/all_gather | solution.py:174
  7.3 110.4 %all-gather.6.cloned.1.call-start = ((), (), s32[]{:S(2)}) async-start(), calls=%async_computation.6 | async-start | bytes 4456448 | tf_op jit(solution)/shard_map/all_gather | solution.py:179
  8.6 6.1 %copy-start.15 = (s32[64,2]{0,1:T(2,128)S(1)}, s32[64,2]{0,1:T(2,128)}, u32[]{:S(2)}) copy-start(s32[64,2]{0,1:T(2,128)} %param.44) | copy-start | bytes 1540
  8.8 6.5 %copy-start.6 = (bf16[1024,64]{0,1:T(8,128)(2,1)S(1)}, bf16[1024,64]{0,1:T(8,128)(2,1)}, u32[]{:S(2)}) copy-start(bf16[1024,64]{0,1:T(8,128)(2,1)} %param.31) | copy-start | bytes 393220
  12.6 9.7 %collective-permute-start = (bf16[1024,192]{0,1:T(8,128)(2,1)S(1)}, bf16[1024,192]{0,1:T(8,128)(2,1)}, u32[]{:S(2)}, u32[]{:S(2)}) collective-permute-start(bf16[1024,192]{0,1:T(8,128)(2,1)S(1)} %pad_maximum_fusion), channel_id=1, source_target_pairs={{0,16},{16,0},{32,48},{48,32},{64,80},{80,64},{96,112},{112,96},{1... | collective-permute-start | bytes 1179656 | tf_op jit(solution)/shard_map/ppermute | solution.py:22
  23.6 20.3 %collective-permute-start.1 = (bf16[2048,192]{0,1:T(8,128)(2,1)S(1)}, bf16[2048,192]{0,1:T(8,128)(2,1)S(1)}, u32[]{:S(2)}, u32[]{:S(2)}) collective-permute-start(bf16[2048,192]{0,1:T(8,128)(2,1)S(1)} %maximum_select_fusion.1), channel_id=1, source_target_pairs={{0,32},{16,48},{32,0},{48,16},{64,96},{80,112},{96,64},{112,80},{1... | collective-permute-start | bytes 2359304 | tf_op jit(solution)/shard_map/ppermute | solution.py:22
  44.5 1.4 copy-start.1
  44.5 4.3 %copy-start.9 = (bf16[2,512,1,64]{1,3,2,0:T(8,128)(2,1)S(1)}, bf16[2,512,1,64]{1,3,2,0:T(8,128)(2,1)}, u32[]{:S(2)}) copy-start(bf16[2,512,1,64]{1,3,2,0:T(8,128)(2,1)} %custom-call) | copy-start | bytes 393220
  48.7 24.2 %copy-start.8 = (bf16[2,512,2,32]{1,3,2,0:T(8,128)(2,1)S(1)}, bf16[2,512,2,32]{1,3,2,0:T(8,128)(2,1)}, u32[]{:S(2)}) copy-start(bf16[2,512,2,32]{1,3,2,0:T(8,128)(2,1)} %custom-call.1) | copy-start | bytes 393220
  50.1 1.5 copy-start.3
  55.5 1.5 copy-start.3
  60.8 37.3 %all-to-all-start = ((bf16[16,2,2048]{2,1,0:T(2,128)(2,1)}), bf16[16,2,2048]{2,1,0:T(2,128)(2,1)S(1)}, u32[]{:S(2)}, u32[]{:S(2)}) async-start(bf16[16,2,2048]{2,1,0:T(2,128)(2,1)} %reshape.649), calls=%async_computation | async-start | bytes 262144 | tf_op jit(solution)/shard_map/all_to_all | solution.py:169
  73.0 32.8 %copy-start.16 = (s32[64,2]{0,1:T(2,128)S(1)}, s32[64,2]{0,1:T(2,128)}, u32[]{:S(2)}) copy-start(s32[64,2]{0,1:T(2,128)} %param.44) | copy-start | bytes 1540
  73.0 32.8 %copy-start.17 = (s32[64,2]{0,1:T(2,128)S(1)}, s32[64,2]{0,1:T(2,128)}, u32[]{:S(2)}) copy-start(s32[64,2]{0,1:T(2,128)} %copy.153) | copy-start | bytes 1540
  73.0 32.8 %copy-start.18 = (f32[64,2]{0,1:T(2,128)S(1)}, f32[64,2]{0,1:T(2,128)}, u32[]{:S(2)}) copy-start(f32[64,2]{0,1:T(2,128)} %param.45) | copy-start | bytes 1540
  98.1 19.6 %copy-start.7 = (bf16[64,2048]{1,0:T(8,128)(2,1)S(1)}, bf16[64,2048]{1,0:T(8,128)(2,1)}, u32[]{:S(2)}) copy-start(bf16[64,2048]{1,0:T(8,128)(2,1)} %param.29) | copy-start | bytes 786436
  98.1 16.2 %all-to-all-start.1 = ((bf16[16,2,2048]{2,1,0:T(2,128)(2,1)}), bf16[16,2,2048]{2,1,0:T(2,128)(2,1)S(1)}, u32[]{:S(2)}, u32[]{:S(2)}) async-start(bf16[16,2,2048]{2,1,0:T(2,128)(2,1)} %reshape.651), calls=%async_computation.1 | async-start | bytes 262144 | tf_op jit(solution)/shard_map/all_to_all | solution.py:170
  105.5 97.8 %all-gather.8.cloned.1.call-start = ((), (), s32[]{:S(2)}) async-start(), calls=%async_computation.7 | async-start | bytes 11141120 | tf_op jit(solution)/shard_map/all_gather | solution.py:205
  117.7 3.5 %copy-start.11 = (f32[2048]{0:T(1024)S(1)}, f32[2048]{0:T(1024)}, u32[]{:S(2)}) copy-start(f32[2048]{0:T(1024)} %param.43) | copy-start | bytes 24580
  117.7 3.5 %copy-start.12 = (f32[2048]{0:T(1024)S(1)}, f32[2048]{0:T(1024)}, u32[]{:S(2)}) copy-start(f32[2048]{0:T(1024)} %param.42) | copy-start | bytes 24580
  117.7 3.6 %copy-start.10 = (bf16[64,160]{1,0:T(8,128)(2,1)S(1)}, bf16[64,160]{1,0:T(8,128)(2,1)}, u32[]{:S(2)}) copy-start(bf16[64,160]{1,0:T(8,128)(2,1)} %get-tuple-element.116) | copy-start | bytes 61444
  122.7 80.5 %copy-start.2 = (bf16[2,2048,192]{1,2,0:T(8,128)(2,1)S(1)}, bf16[2,2048,192]{1,2,0:T(8,128)(2,1)}, u32[]{:S(2)}) copy-start(bf16[2,2048,192]{1,2,0:T(8,128)(2,1)} %param.47) | copy-start | bytes 4718596
  143.4 156.2 %reduce-scatter.2.cloned.1.call-start = ((), (), s32[]{:S(2)}) async-start(), calls=%async_computation.8 | async-start | bytes 11141120 | tf_op jit(solution)/shard_map/reduce_scatter | solution.py:223
  229.3 79.4 %copy-start.4 = (bf16[2048,256]{1,0:T(8,128)(2,1)S(1)}, bf16[2048,256]{1,0:T(8,128)(2,1)}, u32[]{:S(2)}) copy-start(bf16[2048,256]{1,0:T(8,128)(2,1)} %param.49) | copy-start | bytes 3145732
  302.2 16.2 %all-to-all-start.3 = ((bf16[16,2,5,2048]{3,1,2,0:T(2,128)(2,1)}), bf16[16,2,5,2048]{3,1,2,0:T(2,128)(2,1)S(1)}, u32[]{:S(2)}, u32[]{:S(2)}) async-start(bf16[16,2,5,2048]{3,1,2,0:T(2,128)(2,1)} %copy.156), calls=%async_computation.4 | async-start | bytes 1310720 | tf_op jit(solution)/shard_map/all_to_all | solution.py:224
  319.0 3.8 %copy-start.13 = (f32[2048]{0:T(1024)S(1)}, f32[2048]{0:T(1024)}, u32[]{:S(2)}) copy-start(f32[2048]{0:T(1024)} %param.53) | copy-start | bytes 24580
  319.0 3.8 %copy-start.14 = (f32[2048]{0:T(1024)S(1)}, f32[2048]{0:T(1024)}, u32[]{:S(2)}) copy-start(f32[2048]{0:T(1024)} %param.52) | copy-start | bytes 24580
Sparse Core Ops, SparseCore 0:
  9.2 46.0 all-gather.3
  57.1 42.5 all-gather.5
  143.5 59.6 all-gather.7
  229.5 70.0 reduce-scatter.1
where the time goes:
time: 333 us; the launch traced here: 330 us
  waiting for transfers between devices  164 us (49%)
  matrix products  68.5 us (21%)
  starting transfers between devices  31.6 us (9%)
  local copies, waits for them, and re-layouts  20.5 us (6%)
  blocking collectives  19.6 us (6%)
  between operations  13.9 us (4%)
  other arithmetic  11.7 us (4%)
    reduce_scatter x1, waiting for transfers between devices, local(): lax.psum_scatter(partials.astype(jnp.bfloat16), 'tp', scatter_dimension=0...  70.3 us
    all_gather x1, waiting for transfers between devices, local(): lax.all_gather(lax.all_to_all(outgoing, 'sp', split_axis=0, concat_axis=0...  59.8 us
    all_to_all x1, blocking collectives, local(): lax.all_to_all(outgoing, 'sp', split_axis=0, concat_axis=0, tiled=True)  19.6 us
    dot_general x1, matrix products, local(): jnp.einsum('secf,efd->secd', active, expert_down, preferred_element_type=...  17.2 us
    ppermute x2, waiting for transfers between devices, swapped(): lax.ppermute(x, axis, [(i, i ^ 1 << apart) for i in range(lax.axis_size(a...  17.1 us
    dot_general x4, matrix products, one_block(): jnp.einsum('hqk,kd->qhd', weights, value_block, preferred_element_type=jn...  16.9 us
    sub x2, matrix products, one_block(): weights = jnp.exp(scores - largest)  11.7 us
    all_to_all x1, starting transfers between devices, local(): lax.all_to_all(wide_mixed, 'tp', split_axis=0, concat_axis=1, tiled=True)  11.1 us
  transfers between devices with their start and end apart: 9, of which 6 were waited for; matrix products, arithmetic and copies ran while one was open for 18% of the time, Pallas kernels for 0%

commit v1 on v0

v1 whole, which is shorter than its diff:
```python
import jax
import jax.numpy as jnp
from jax import lax
from jax.experimental import pallas as pl
from jax.experimental.pallas import tpu as pltpu
from jax.sharding import PartitionSpec as P

LOCAL_EXPERTS = 2
EPS_LAYER = 1e-05
ALPHA = 2.0**0.25
EPS_HEAD = 1e-06
THETA = 10000.0
GRID_WIDTH = 64
SEQ_SHARDS = 4
LOG2E = 1.4426950408889634
WIDE_SIZE = 64
NARROW_SIZE = 32
KEY_ROWS = WIDE_SIZE + NARROW_SIZE
ONES_ROWS = 16
BLOCK_Q = 256
CHUNK = 512


def column(ref):
    size = ref.shape[1]
    spread = jnp.broadcast_to(ref[...], (size, size))
    diagonal = lax.broadcasted_iota(jnp.int32, (size, size), 0) == lax.broadcasted_iota(
        jnp.int32, (size, size), 1
    )
    return jnp.sum(jnp.where(diagonal, spread, 0.0), axis=1, keepdims=True)


def normed(heads, gain):
    mean_square = jnp.mean(heads * heads, axis=0, keepdims=True)
    return heads * lax.rsqrt(mean_square + EPS_HEAD) * gain


def turned(heads, tables):
    n = heads.shape[0] // 4
    parts = []
    for half, (cosine, sine) in enumerate(tables):
        a = heads[2 * half * n : (2 * half + 1) * n]
        b = heads[(2 * half + 1) * n : (2 * half + 2) * n]
        parts += [a * cosine - b * sine, b * cosine + a * sine]
    return jnp.concatenate(parts, axis=0)


def angle_tables(quarter, first_row, tokens):
    frequency = jnp.exp(
        lax.broadcasted_iota(jnp.int32, (quarter, tokens), 0).astype(jnp.float32)
        * (-jnp.log(jnp.float32(THETA)) / quarter)
    )
    token = lax.broadcasted_iota(jnp.int32, (quarter, tokens), 1)
    row_angle = (token // GRID_WIDTH + first_row).astype(jnp.float32) * frequency
    col_angle = (token % GRID_WIDTH).astype(jnp.float32) * frequency
    return ((jnp.cos(row_angle), jnp.sin(row_angle)), (jnp.cos(col_angle), jnp.sin(col_angle)))


def prepare_kernel(place, wqt, nqt, wk, nk, wv, nv, wqg, wkg, nqg, nkg, q_out, kv_out, turn):
    tokens = wqt.shape[1]
    tp = place[0]
    first_row = place[1]
    wide_tables = angle_tables(WIDE_SIZE // 4, first_row, tokens)
    narrow_tables = angle_tables(NARROW_SIZE // 4, first_row, tokens)

    def picked(ref, start, size):
        block = start // 128
        columns = ref[:, pl.ds(pl.multiple_of(block * 128, 128), 128)]
        turn[...] = columns.astype(jnp.float32).T
        return turn[pl.ds(pl.multiple_of(start % 128, size), size), :]

    wide_start = tp // 4 * WIDE_SIZE
    narrow_start = tp // 2 * NARROW_SIZE
    keys = turned(normed(picked(wk, wide_start, WIDE_SIZE), column(wkg)), wide_tables)
    kv_out[0:64, :] = keys.astype(jnp.bfloat16)
    keys = turned(normed(picked(nk, narrow_start, NARROW_SIZE), column(nkg)), narrow_tables)
    kv_out[64:96, :] = keys.astype(jnp.bfloat16)
    kv_out[96:160, :] = picked(wv, wide_start, WIDE_SIZE).astype(jnp.bfloat16)
    kv_out[160:192, :] = picked(nv, narrow_start, NARROW_SIZE).astype(jnp.bfloat16)
    wide = turned(normed(wqt[...].astype(jnp.float32), column(wqg)), wide_tables)
    q_out[0:64, 0:tokens] = wide.astype(jnp.bfloat16)
    q_out[64:128, 0:tokens] = jnp.zeros((64, tokens), jnp.bfloat16)
    q_out[0:64, tokens:] = jnp.zeros((64, 2 * tokens), jnp.bfloat16)
    q_out[96:128, tokens:] = jnp.zeros((32, 2 * tokens), jnp.bfloat16)
    for head in range(2):
        rows = nqt[NARROW_SIZE * head : NARROW_SIZE * (head + 1), :].astype(jnp.float32)
        narrow = turned(normed(rows, column(nqg)), narrow_tables)
        q_out[64:96, tokens * (head + 1) : tokens * (head + 2)] = narrow.astype(jnp.bfloat16)


def prepare(place, wqt, nqt, wk, nk, wv, nv, wqg, wkg, nqg, nkg):
    tokens = wqt.shape[1]
    vmem = pl.BlockSpec(memory_space=pltpu.VMEM)
    return pl.pallas_call(
        prepare_kernel,
        out_shape=(
            jax.ShapeDtypeStruct((128, 3 * tokens), jnp.bfloat16),
            jax.ShapeDtypeStruct((192, tokens), jnp.bfloat16),
        ),
        in_specs=[pl.BlockSpec(memory_space=pltpu.SMEM)] + [vmem] * 10,
        out_specs=(vmem, vmem),
        scratch_shapes=[pltpu.VMEM((128, tokens), jnp.float32)],
        name="prepare_heads",
    )(
        place, wqt, nqt, wk, nk, wv, nv,
        wqg.reshape(1, -1), wkg.reshape(1, -1), nqg.reshape(1, -1), nkg.reshape(1, -1),
    )


def attend_kernel(q, kv0, kv1, kv2, kv3, out, keys, values, scores0, scores1, mixed):
    tokens = kv0.shape[1]
    total = 4 * tokens
    blocks = q.shape[1] // BLOCK_Q
    wide_blocks = tokens // BLOCK_Q
    values[KEY_ROWS:, :] = jnp.ones((ONES_ROWS, total), jnp.bfloat16)
    for n, kv in enumerate((kv0, kv1, kv2, kv3)):
        piece = kv[0:KEY_ROWS, :].astype(jnp.float32)
        padded = jnp.concatenate([piece, jnp.zeros((128 - KEY_ROWS, tokens), jnp.float32)], axis=0)
        keys[n * tokens : (n + 1) * tokens, :] = padded.T.astype(jnp.bfloat16)
        values[0:KEY_ROWS, n * tokens : (n + 1) * tokens] = kv[KEY_ROWS:, :]

    def scored(c, query, into, largest):
        part = jnp.dot(
            keys[c * CHUNK : (c + 1) * CHUNK, :], query, preferred_element_type=jnp.float32
        )
        into[c * CHUNK : (c + 1) * CHUNK, :] = part
        return jnp.maximum(largest, jnp.max(part.reshape(CHUNK // 8, 8, BLOCK_Q), axis=0))

    lowest = jnp.full((8, BLOCK_Q), -jnp.inf, jnp.float32)
    query_at = lambda b: q[:, pl.ds(pl.multiple_of(b * BLOCK_Q, BLOCK_Q), BLOCK_Q)]

    def step(b, current, following, largest):
        query = query_at(jnp.minimum(b + 1, blocks - 1))
        peak = jnp.max(largest, axis=0, keepdims=True)
        factor = jnp.where(
            b < wide_blocks,
            jnp.float32(WIDE_SIZE**-0.5 * LOG2E),
            jnp.float32(NARROW_SIZE**-0.5 * LOG2E),
        )
        next_largest = lowest
        total_mixed = jnp.zeros((KEY_ROWS + ONES_ROWS, BLOCK_Q), jnp.float32)
        for c in range(total // CHUNK):
            next_largest = scored(c, query, following, next_largest)
            raw = current[c * CHUNK : (c + 1) * CHUNK, :]
            weights = jnp.exp2((raw - peak) * factor).astype(jnp.bfloat16)
            total_mixed = total_mixed + jnp.dot(
                values[:, c * CHUNK : (c + 1) * CHUNK], weights, preferred_element_type=jnp.float32
            )
        mixed[b] = total_mixed[:KEY_ROWS] / total_mixed[KEY_ROWS : KEY_ROWS + 1]
        return next_largest

    largest = lowest
    first = query_at(0)
    for c in range(total // CHUNK):
        largest = scored(c, first, scores0, largest)

    def pair(i, largest):
        largest = step(2 * i, scores0, scores1, largest)
        return step(2 * i + 1, scores1, scores0, largest)

    lax.fori_loop(0, blocks // 2, pair, largest)
    for b in range(wide_blocks):
        rows = jnp.concatenate(
            [
                mixed[b, 0:WIDE_SIZE],
                mixed[wide_blocks + b, WIDE_SIZE:KEY_ROWS],
                mixed[2 * wide_blocks + b, WIDE_SIZE:KEY_ROWS],
            ],
            axis=0,
        )
        out[b * BLOCK_Q : (b + 1) * BLOCK_Q, :] = rows.T.astype(jnp.bfloat16)


def attend(q, pieces):
    tokens = pieces[0].shape[1]
    vmem = pl.BlockSpec(memory_space=pltpu.VMEM)
    return pl.pallas_call(
        attend_kernel,
        out_shape=jax.ShapeDtypeStruct((tokens, 128), jnp.bfloat16),
        in_specs=[vmem] * 5,
        out_specs=vmem,
        scratch_shapes=[
            pltpu.VMEM((4 * tokens, 128), jnp.bfloat16),
            pltpu.VMEM((KEY_ROWS + ONES_ROWS, 4 * tokens), jnp.bfloat16),
            pltpu.VMEM((4 * tokens, BLOCK_Q), jnp.float32),
            pltpu.VMEM((4 * tokens, BLOCK_Q), jnp.float32),
            pltpu.VMEM((q.shape[1] // BLOCK_Q, KEY_ROWS, BLOCK_Q), jnp.float32),
        ],
        name="attend_blocks",
    )(q, *pieces)


def turned_ring(x, away):
    size = lax.axis_size("sp")
    return lax.ppermute(
        x,
        "sp",
        [(i, i // SEQ_SHARDS * SEQ_SHARDS + (i + away) % SEQ_SHARDS) for i in range(size)],
    )


def layer_norm(values, gain_vec, bias_vec):
    center = jnp.mean(values, axis=-1, keepdims=True)
    shifted = values - center
    variance = jnp.mean(shifted * shifted, axis=-1, keepdims=True)
    return (shifted * lax.rsqrt(variance + EPS_LAYER) * gain_vec + bias_vec).astype(jnp.bfloat16)


def local(
    residual,
    wide_query,
    narrow_query,
    wide_keys,
    narrow_keys,
    wide_values,
    narrow_values,
    wide_query_gain,
    wide_key_gain,
    narrow_query_gain,
    narrow_key_gain,
    wide_out,
    narrow_out,
    first_gain,
    first_bias,
    route_ids,
    route_weights,
    expert_gate,
    expert_up,
    expert_down,
    shared_gate,
    shared_up,
    shared_down,
    second_gain,
    second_bias,
):
    tp_size = lax.axis_size("tp")
    place = jnp.stack(
        [
            lax.axis_index("tp"),
            lax.axis_index("sp") % SEQ_SHARDS * (wide_query.shape[0] // GRID_WIDTH),
        ]
    )
    out_weights = lax.all_gather(
        jnp.concatenate([wide_out, narrow_out], axis=0), "tp", axis=0, tiled=True
    )
    rotated_queries, own_pack = prepare(
        place,
        wide_query.T,
        narrow_query.T,
        wide_keys,
        narrow_keys,
        wide_values,
        narrow_values,
        wide_query_gain,
        wide_key_gain,
        narrow_query_gain,
        narrow_key_gain,
    )
    packs = [own_pack] + [turned_ring(own_pack, away) for away in range(1, SEQ_SHARDS)]
    mixed = attend(rotated_queries, packs)
    tokens = lax.all_to_all(mixed, "tp", split_axis=0, concat_axis=1, tiled=True)
    projected = jnp.dot(tokens, out_weights, preferred_element_type=jnp.float32)
    hidden = layer_norm(ALPHA * residual.astype(jnp.float32) + projected, first_gain, first_bias)
    device_rows = hidden.shape[0]
    model_width = hidden.shape[1]
    sp_size = lax.axis_size("sp")
    top_count = route_ids.shape[1]
    experts = LOCAL_EXPERTS * sp_size
    capacity = max(2, (5 * device_rows * top_count + 4 * experts - 1) // (4 * experts))
    flat_ids = route_ids.reshape(-1)
    expert_hits = (flat_ids[:, None] == jnp.arange(experts, dtype=jnp.int32)[None, :]).astype(
        jnp.int32
    )
    earlier = jnp.sum((jnp.cumsum(expert_hits, axis=0) - expert_hits) * expert_hits, axis=1)
    slot_index = flat_ids * capacity + earlier
    chosen = (
        slot_index[:, None] == jnp.arange(experts * capacity, dtype=jnp.int32)[None, :]
    ).astype(jnp.float32)
    chosen = chosen.reshape(device_rows, top_count, experts * capacity)
    placing = jnp.sum(chosen, axis=1).astype(jnp.bfloat16)
    mixing = jnp.sum(chosen * route_weights[:, :, None], axis=1)
    outgoing = jnp.einsum("rs,rd->sd", placing, hidden, preferred_element_type=jnp.float32).astype(
        jnp.bfloat16
    )
    outgoing = outgoing.reshape(sp_size, LOCAL_EXPERTS, capacity, model_width)
    piece_rows = lax.all_gather(
        lax.all_to_all(outgoing, "sp", split_axis=0, concat_axis=0, tiled=True),
        "tp",
        axis=0,
        tiled=True,
    )
    gate_values = jnp.einsum(
        "secd,edf->secf", piece_rows, expert_gate, preferred_element_type=jnp.float32
    )
    up_values = jnp.einsum(
        "secd,edf->secf", piece_rows, expert_up, preferred_element_type=jnp.float32
    )
    active = (jax.nn.silu(gate_values) * up_values).astype(jnp.bfloat16)
    partial_value = jnp.einsum(
        "secf,efd->secd", active, expert_down, preferred_element_type=jnp.float32
    )
    rounded = lax.optimization_barrier(partial_value.astype(jnp.bfloat16))
    partials = rounded.astype(jnp.float32)
    summed = lax.psum_scatter(partials.astype(jnp.bfloat16), "tp", scatter_dimension=0, tiled=True)
    returned = lax.all_to_all(summed, "sp", split_axis=0, concat_axis=0, tiled=True)
    routed = jnp.dot(mixing, returned.reshape(-1, model_width).astype(jnp.float32))
    shared_gate_values = jnp.dot(hidden, shared_gate, preferred_element_type=jnp.float32)
    shared_up_values = jnp.dot(hidden, shared_up, preferred_element_type=jnp.float32)
    shared_active = (jax.nn.silu(shared_gate_values) * shared_up_values).astype(jnp.bfloat16)
    shared_output = jnp.dot(shared_active, shared_down, preferred_element_type=jnp.float32)
    return layer_norm(
        ALPHA * hidden.astype(jnp.float32) + routed + shared_output, second_gain, second_bias
    )


def solution(mesh):
    in_specs = (
        P(("sp", "tp"), None),
        P("sp", "tp"),
        P("sp", "tp"),
        P("sp", None),
        P("sp", None),
        P("sp", None),
        P("sp", None),
        P(),
        P(),
        P(),
        P(),
        P("tp", None),
        P("tp", None),
        P(),
        P(),
        P(("sp", "tp"), None),
        P(("sp", "tp"), None),
        P("sp", None, "tp"),
        P("sp", None, "tp"),
        P("sp", "tp", None),
        P(),
        P(),
        P(),
        P(),
        P(),
    )
    out_specs = P(("sp", "tp"), None)
    return jax.shard_map(local, mesh=mesh, in_specs=in_specs, out_specs=out_specs, check_vma=False)
```

time: 333 us -> 292 us (0.88)
  matrix products: 68.5 us -> 36 us
  Pallas kernels: 0 us -> 21.9 us
  local copies, waits for them, and re-layouts: 20.5 us -> 6.6 us
  starting transfers between devices: 31.6 us -> 22.5 us
  other arithmetic: 11.7 us -> 5.32 us
    pallas_call x0 -> x2, Pallas kernels: none -> 21.9 us  [the longest x1 17.8 us: attend(): pl.pallas_call(attend_kernel, out_shape=jax.ShapeDtypeStruct((tokens, 128...]
    dot_general x8 -> x1, matrix products: 25.9 us -> 5.06 us  [local(): projected = jnp.dot(tokens, out_weights, preferred_element_type=jnp.float32)]
    sub x2 -> x0, matrix products: 11.7 us -> none  [one_block(): weights = jnp.exp(scores - largest)]
    all_to_all x2 -> x1, starting transfers between devices: 18.5 us -> 10 us  [local(): lax.all_to_all(mixed, 'tp', split_axis=0, concat_axis=1, tiled=True)]
    all_to_all x2 -> x1, waiting for transfers between devices: 7.66 us -> 10.1 us  [local(): lax.all_to_all(mixed, 'tp', split_axis=0, concat_axis=1, tiled=True)]
    ppermute x2 -> x3, waiting for transfers between devices: 17.1 us -> 15.8 us  [turned_ring(): lax.ppermute(x, 'sp', [(i, i // SEQ_SHARDS * SEQ_SHARDS + (i + away) % SE...]
  transfers between devices with their start and end apart: 9 -> 8, of which waited for: 6 -> 6; matrix products, arithmetic and copies ran while one was open for 18% -> 1% of each run, Pallas kernels for 0% -> 8%
where the time goes in v1:
time: 292 us; the launch traced here: 289 us
  waiting for transfers between devices  165 us (57%)
  matrix products  36 us (12%)
  starting transfers between devices  22.5 us (8%)
  Pallas kernels  21.9 us (8%)
  blocking collectives  19.1 us (7%)
  between operations  13.3 us (5%)
  local copies, waits for them, and re-layouts  6.6 us (2%)
  other arithmetic  5.32 us (2%)
    reduce_scatter x1, waiting for transfers between devices, local(): lax.psum_scatter(partials.astype(jnp.bfloat16), 'tp', scatter_dimension=0...  70.2 us
    all_gather x1, waiting for transfers between devices, local(): lax.all_gather(lax.all_to_all(outgoing, 'sp', split_axis=0, concat_axis=0...  59.6 us
    all_to_all x1, blocking collectives, local(): lax.all_to_all(outgoing, 'sp', split_axis=0, concat_axis=0, tiled=True)  19.1 us
    pallas_call x1, Pallas kernels, attend(): pl.pallas_call(attend_kernel, out_shape=jax.ShapeDtypeStruct((tokens, 128...  17.8 us
    dot_general x1, matrix products, local(): jnp.einsum('secf,efd->secd', active, expert_down, preferred_element_type=...  17.3 us
    ppermute x3, waiting for transfers between devices, turned_ring(): lax.ppermute(x, 'sp', [(i, i // SEQ_SHARDS * SEQ_SHARDS + (i + away) % SE...  15.8 us
    all_to_all x1, waiting for transfers between devices, local(): lax.all_to_all(mixed, 'tp', split_axis=0, concat_axis=1, tiled=True)  10.1 us
    all_to_all x1, starting transfers between devices, local(): lax.all_to_all(mixed, 'tp', split_axis=0, concat_axis=1, tiled=True)  10 us
  transfers between devices with their start and end apart: 8, of which 6 were waited for; matrix products, arithmetic and copies ran while one was open for 1% of the time, Pallas kernels for 8%

profile of v1, /device:TPU:1, one launch (start us, length us, event | category | flops | bytes accessed | tf_op | source)
XLA Modules:
  0.0 289.4 jit_solution(9860191080937837239)
XLA Ops:
  6.5 2.0 pad_maximum_fusion
  8.6 0.7 pad_add_fusion.place
  9.3 4.1 %prepare_heads.1 = (bf16[128,3072]{1,0:T(8,128)(2,1)}, bf16[192,1024]{1,0:T(8,128)(2,1)}) custom-call(s32[2]{0:T(128)} %pad_add_fusion.place, bf16[64,1024]{1,0:T(8,128)(2,1)} %bitcast.71, bf16[64,1024]{1,0:T(8,128)(2,1)} %bitcast.72, bf16[1024,256]{1,0:T(8,128)(2,1)} %wk.1, bf16[1024,256]{1,0:T(8,128)(2,1)} %nk.1, bf16[1024,256]{1,0:T(8,128)(2,1)} %wv.1, ...), custom_call_target="tpu_custom_call" | custom-call | tf_op jit(solution)/shard_map/prepare_heads/pallas_call | solution.py:94
  13.4 2.1 collective-permute-start
  15.5 2.5 collective-permute-start.1
  17.9 1.2 collective-permute-start.2
  19.3 4.3 %collective-permute-done.kv1 = bf16[192,1024]{1,0:T(8,128)(2,1)S(1)} collective-permute-done((bf16[192,1024]{1,0:T(8,128)(2,1)}, bf16[192,1024]{1,0:T(8,128)(2,1)S(1)}, u32[]{:S(2)}, u32[]{:S(2)}) %collective-permute-start) | collective-permute-done | bytes 393248 | tf_op jit(solution)/shard_map/ppermute | solution.py:195
  23.6 11.5 %collective-permute-done.1.kv2 = bf16[192,1024]{1,0:T(8,128)(2,1)S(1)} collective-permute-done((bf16[192,1024]{1,0:T(8,128)(2,1)}, bf16[192,1024]{1,0:T(8,128)(2,1)S(1)}, u32[]{:S(2)}, u32[]{:S(2)}) %collective-permute-start.1) | collective-permute-done | bytes 393248 | tf_op jit(solution)/shard_map/ppermute | solution.py:195
  35.1 0.8 copy-done.4
  36.0 17.8 %attend_blocks.1 = bf16[1024,128]{1,0:T(8,128)(2,1)} custom-call(bf16[128,3072]{1,0:T(8,128)(2,1)} %get-tuple-element.7.q, bf16[192,1024]{1,0:T(8,128)(2,1)} %get-tuple-element.8.kv0, bf16[192,1024]{1,0:T(8,128)(2,1)} %copy-done.3, bf16[192,1024]{1,0:T(8,128)(2,1)} %copy-done.4, bf16[192,1024]{1,0:T(8,128)(2,1)} %copy-done.5), custom_call_target="tpu_custom_call" | custom-call | tf_op jit(solution)/shard_map/attend_blocks/pallas_call | solution.py:177
  53.8 10.0 %all-to-all-start = ((bf16[16,64,128]{2,1,0:T(8,128)(2,1)}), bf16[16,64,128]{2,1,0:T(8,128)(2,1)S(1)}, u32[]{:S(2)}, u32[]{:S(2)}) async-start(bf16[16,64,128]{2,1,0:T(8,128)(2,1)} %bitcast.70), calls=%async_computation | async-start | bytes 524288 | tf_op jit(solution)/shard_map/all_to_all | solution.py:261
  64.5 0.7 convert_reduce_fusion
  65.3 10.1 %all-to-all-done = bf16[16,64,128]{2,1,0:T(8,128)(2,1)S(1)} async-done(((bf16[16,64,128]{2,1,0:T(8,128)(2,1)}), bf16[16,64,128]{2,1,0:T(8,128)(2,1)S(1)}, u32[]{:S(2)}, u32[]{:S(2)}) %all-to-all-start) | async-done | bytes 262176 | tf_op jit(solution)/shard_map/all_to_all | solution.py:261
  75.4 5.1 %fusion.23 = (f32[64]{0:T(128)S(1)}, f32[64,2048]{1,0:T(8,128)S(1)}) fusion(bf16[2048,2048]{1,0:T(8,128)(2,1)} %all-gather.3.cloned.1.call-done, bf16[64,2048]{1,0:T(8,128)(2,1)S(1)} %copy-done.6, bf16[16,64,128]{2,1,0:T(8,128)(2,1)S(1)} %all-to-all-done), kind=kOutput, calls=%fused_computation.47 | convolution fusion | flops 537395136 | bytes 9437440 | tf_op jit(solution)/shard_map/dot_general | solution.py:262
  80.9 0.3 convolution_convert_fusion
  81.3 0.3 reshape.73
  81.5 0.7 copy.66
  82.3 19.1 %all_to_all.29 = bf16[16,2,5,2048]{3,1,2,0:T(2,128)(2,1)S(1)} all-to-all(bf16[16,2,5,2048]{3,1,2,0:T(2,128)(2,1)S(1)} %copy.66), channel_id=1, replica_groups=mesh['sp'=16,'tp'=16] {'sp'}, dimensions={0} | all-to-all | bytes 1310720 | tf_op jit(solution)/shard_map/all_to_all | solution.py:287
  101.4 1.1 copy.67
  102.7 59.6 %all-gather.5.cloned.1.call-done = bf16[256,2,5,2048]{3,0,2,1:T(8,128)(2,1)} async-done(((bf16[16,2,5,2048]{3,0,2,1:T(8,128)(2,1)}), bf16[256,2,5,2048]{3,0,2,1:T(8,128)(2,1)}) %all-gather.5.cloned.1.call-update) | async-done | bytes 10485776 | tf_op jit(solution)/shard_map/all_gather | solution.py:286
  162.4 8.9 %fusion.5 = f32[2,256,5,192]{1,3,2,0:T(8,128)} fusion(bf16[256,2,5,2048]{3,0,2,1:T(8,128)(2,1)} %all-gather.5.cloned.1.call-done, bf16[2,2048,192]{1,2,0:T(8,128)(2,1)S(1)} %copy-done.1), kind=kOutput, calls=%fused_computation.13 | convolution fusion | flops 2013265920 | bytes 14024704 | tf_op jit(solution)/shard_map/secd,edf->secf/dot_general | solution.py:295
  171.2 17.3 %convert_bitcast_fusion = bf16[256,2,5,2048]{3,0,2,1:T(8,128)(2,1)} fusion(f32[2,256,5,192]{1,3,2,0:T(8,128)} %fusion.5, bf16[256,2,5,2048]{3,0,2,1:T(8,128)(2,1)} %all-gather.5.cloned.1.call-done, bf16[2,192,2048]{2,1,0:T(8,128)(2,1)S(1)} %copy-done, bf16[2,2048,192]{1,2,0:T(8,128)(2,1)} %param.42), kind=kOutput, calls=%fused_computation | convolution fusion | flops 4034723840 | bytes 26083328 | tf_op jit(solution)/shard_map/secf,efd->secd/dot_general | solution.py:299
  188.6 70.2 %reduce-scatter.2.cloned.1.call-done = bf16[16,2,5,2048]{3,0,2,1:T(8,128)(2,1)} async-done(((bf16[256,2,5,2048]{3,0,2,1:T(8,128)(2,1)}), bf16[16,2,5,2048]{3,0,2,1:T(8,128)(2,1)}) %reduce-scatter.2.cloned.1.call-update) | async-done | bytes 655376 | tf_op jit(solution)/shard_map/reduce_scatter | solution.py:304
  258.8 2.6 copy.68
  261.4 6.5 %all-to-all-start.2 = ((bf16[16,2,5,2048]{3,1,2,0:T(2,128)(2,1)}), bf16[16,2,5,2048]{3,1,2,0:T(2,128)(2,1)S(1)}, u32[]{:S(2)}, u32[]{:S(2)}) async-start(bf16[16,2,5,2048]{3,1,2,0:T(2,128)(2,1)} %copy.68), calls=%async_computation.3 | async-start | bytes 1310720 | tf_op jit(solution)/shard_map/all_to_all | solution.py:305
  268.0 0.9 fusion.25
  268.9 8.8 %all-to-all-done.2 = bf16[16,2,5,2048]{3,1,2,0:T(2,128)(2,1)S(1)} async-done(((bf16[16,2,5,2048]{3,1,2,0:T(2,128)(2,1)}), bf16[16,2,5,2048]{3,1,2,0:T(2,128)(2,1)S(1)}, u32[]{:S(2)}, u32[]{:S(2)}) %all-to-all-start.2) | async-done | bytes 655392 | tf_op jit(solution)/shard_map/all_to_all | solution.py:305
  277.7 0.3 copy.69
  278.0 0.3 reshape.74
  278.2 1.0 convolution_add_fusion.2
  279.3 2.5 fusion.24
  282.0 0.9 add_convert_fusion
  (48 shorter events, 2.0 us)
Async XLA Ops:
  6.5 164.7 %copy-start = (bf16[2,192,2048]{2,1,0:T(8,128)(2,1)S(1)}, bf16[2,192,2048]{2,1,0:T(8,128)(2,1)}, u32[]{:S(2)}) copy-start(bf16[2,192,2048]{2,1,0:T(8,128)(2,1)} %param.44) | copy-start | bytes 4718596
  6.5 12.5 %copy-start.11 = (s32[64,2]{0,1:T(2,128)S(1)}, s32[64,2]{0,1:T(2,128)}, u32[]{:S(2)}) copy-start(s32[64,2]{0,1:T(2,128)} %param.40) | copy-start | bytes 1540
  6.5 68.9 %all-gather.3.cloned.1.call-start = ((), (), s32[]{:S(2)}) async-start(), calls=%async_computation.4 | async-start | bytes 8912896 | tf_op jit(solution)/shard_map/all_gather | solution.py:243
  13.4 51.2 %copy-start.12 = (f32[64,2]{0,1:T(2,128)S(1)}, f32[64,2]{0,1:T(2,128)}, u32[]{:S(2)}) copy-start(f32[64,2]{0,1:T(2,128)} %param.41) | copy-start | bytes 1540
  13.4 62.1 %copy-start.6 = (bf16[64,2048]{1,0:T(8,128)(2,1)S(1)}, bf16[64,2048]{1,0:T(8,128)(2,1)}, u32[]{:S(2)}) copy-start(bf16[64,2048]{1,0:T(8,128)(2,1)} %param.25) | copy-start | bytes 786436
  13.4 10.2 %collective-permute-start = (bf16[192,1024]{1,0:T(8,128)(2,1)}, bf16[192,1024]{1,0:T(8,128)(2,1)S(1)}, u32[]{:S(2)}, u32[]{:S(2)}) collective-permute-start(bf16[192,1024]{1,0:T(8,128)(2,1)} %get-tuple-element.8.kv0), channel_id=1, source_target_pairs={{0,16},{16,32},{32,48},{48,0},{64,80},{80,96},{96,112},{112,64},{1... | collective-permute-start | bytes 1179656 | tf_op jit(solution)/shard_map/ppermute | solution.py:195
  15.5 19.6 %collective-permute-start.1 = (bf16[192,1024]{1,0:T(8,128)(2,1)}, bf16[192,1024]{1,0:T(8,128)(2,1)S(1)}, u32[]{:S(2)}, u32[]{:S(2)}) collective-permute-start(bf16[192,1024]{1,0:T(8,128)(2,1)} %get-tuple-element.8.kv0), channel_id=1, source_target_pairs={{0,32},{16,48},{32,0},{48,16},{64,96},{80,112},{96,64},{112,80},{1... | collective-permute-start | bytes 1179656 | tf_op jit(solution)/shard_map/ppermute | solution.py:195
  17.9 17.2 %collective-permute-start.2 = (bf16[192,1024]{1,0:T(8,128)(2,1)}, bf16[192,1024]{1,0:T(8,128)(2,1)S(1)}, u32[]{:S(2)}, u32[]{:S(2)}) collective-permute-start(bf16[192,1024]{1,0:T(8,128)(2,1)} %get-tuple-element.8.kv0), channel_id=1, source_target_pairs={{0,48},{16,0},{32,16},{48,32},{64,112},{80,64},{96,80},{112,96},{1... | collective-permute-start | bytes 1179656 | tf_op jit(solution)/shard_map/ppermute | solution.py:195
  23.6 11.5 %copy-start.3 = (bf16[192,1024]{1,0:T(8,128)(2,1)}, bf16[192,1024]{1,0:T(8,128)(2,1)S(1)}, u32[]{:S(2)}) copy-start(bf16[192,1024]{1,0:T(8,128)(2,1)S(1)} %collective-permute-done.kv1) | copy-start | bytes 1179652
  35.1 0.8 copy-start.4
  35.1 0.9 copy-start.5
  53.8 21.6 %all-to-all-start = ((bf16[16,64,128]{2,1,0:T(8,128)(2,1)}), bf16[16,64,128]{2,1,0:T(8,128)(2,1)S(1)}, u32[]{:S(2)}, u32[]{:S(2)}) async-start(bf16[16,64,128]{2,1,0:T(8,128)(2,1)} %bitcast.70), calls=%async_computation | async-start | bytes 524288 | tf_op jit(solution)/shard_map/all_to_all | solution.py:261
  63.8 98.5 %all-gather.5.cloned.1.call-start = ((), (), s32[]{:S(2)}) async-start(), calls=%async_computation.5 | async-start | bytes 11141120 | tf_op jit(solution)/shard_map/all_gather | solution.py:286
  65.3 15.5 %copy-start.7 = (f32[2048]{0:T(1024)S(1)}, f32[2048]{0:T(1024)}, u32[]{:S(2)}) copy-start(f32[2048]{0:T(1024)} %param.39) | copy-start | bytes 24580
  65.3 15.5 %copy-start.8 = (f32[2048]{0:T(1024)S(1)}, f32[2048]{0:T(1024)}, u32[]{:S(2)}) copy-start(f32[2048]{0:T(1024)} %param.38) | copy-start | bytes 24580
  82.3 80.1 %copy-start.1 = (bf16[2,2048,192]{1,2,0:T(8,128)(2,1)S(1)}, bf16[2,2048,192]{1,2,0:T(8,128)(2,1)}, u32[]{:S(2)}) copy-start(bf16[2,2048,192]{1,2,0:T(8,128)(2,1)} %param.43) | copy-start | bytes 4718596
  102.5 156.3 %reduce-scatter.2.cloned.1.call-start = ((), (), s32[]{:S(2)}) async-start(), calls=%async_computation.6 | async-start | bytes 11141120 | tf_op jit(solution)/shard_map/reduce_scatter | solution.py:304
  188.6 79.4 %copy-start.2 = (bf16[2048,256]{1,0:T(8,128)(2,1)S(1)}, bf16[2048,256]{1,0:T(8,128)(2,1)}, u32[]{:S(2)}) copy-start(bf16[2048,256]{1,0:T(8,128)(2,1)} %param.45) | copy-start | bytes 3145732
  261.4 16.2 %all-to-all-start.2 = ((bf16[16,2,5,2048]{3,1,2,0:T(2,128)(2,1)}), bf16[16,2,5,2048]{3,1,2,0:T(2,128)(2,1)S(1)}, u32[]{:S(2)}, u32[]{:S(2)}) async-start(bf16[16,2,5,2048]{3,1,2,0:T(2,128)(2,1)} %copy.68), calls=%async_computation.3 | async-start | bytes 1310720 | tf_op jit(solution)/shard_map/all_to_all | solution.py:305
  279.3 2.8 copy-start.9
  279.3 2.8 copy-start.10
Sparse Core Ops, SparseCore 0:
  9.2 60.0 all-gather.2
  102.6 59.7 all-gather.4
  188.7 70.0 reduce-scatter.1

commit v2 on v1

--- a/solution.py
+++ b/solution.py
@@ -188,6 +188,34 @@
         ],
         name="attend_blocks",
     )(q, *pieces)
+
+
+def expert_kernel(rows, gate, up, down, out):
+    e = pl.program_id(0)
+    sources, _, slots, width = rows.shape
+    x = rows[...].reshape(sources * slots, width)
+    along = (((1,), (1,)), ((), ()))
+    gate_values = lax.dot_general(x, gate[e], along, preferred_element_type=jnp.float32)
+    up_values = lax.dot_general(x, up[e], along, preferred_element_type=jnp.float32)
+    active = gate_values / (1.0 + jnp.exp(-gate_values)) * up_values
+    partial_value = jnp.dot(
+        active.astype(jnp.bfloat16), down[e], preferred_element_type=jnp.float32
+    )
+    out[...] = partial_value.astype(jnp.bfloat16).reshape(rows.shape)
+
+
+def run_experts(rows, gate, up, down):
+    sources, experts, slots, width = rows.shape
+    block = pl.BlockSpec((sources // 4, 1, slots, width), lambda e, r: (r, e, 0, 0))
+    whole = pl.BlockSpec(memory_space=pltpu.VMEM)
+    return pl.pallas_call(
+        expert_kernel,
+        grid=(experts, 4),
+        out_shape=jax.ShapeDtypeStruct(rows.shape, jnp.bfloat16),
+        in_specs=[block, whole, whole, whole],
+        out_specs=block,
+        name="run_experts",
+    )(rows, gate, up, down)
 
 
 def turned_ring(x, away):
@@ -283,26 +311,22 @@
         jnp.bfloat16
     )
     outgoing = outgoing.reshape(sp_size, LOCAL_EXPERTS, capacity, model_width)
-    piece_rows = lax.all_gather(
-        lax.all_to_all(outgoing, "sp", split_axis=0, concat_axis=0, tiled=True),
-        "tp",
-        axis=0,
-        tiled=True,
-    )
-    gate_values = jnp.einsum(
-        "secd,edf->secf", piece_rows, expert_gate, preferred_element_type=jnp.float32
-    )
-    up_values = jnp.einsum(
-        "secd,edf->secf", piece_rows, expert_up, preferred_element_type=jnp.float32
-    )
-    active = (jax.nn.silu(gate_values) * up_values).astype(jnp.bfloat16)
-    partial_value = jnp.einsum(
-        "secf,efd->secd", active, expert_down, preferred_element_type=jnp.float32
-    )
-    rounded = lax.optimization_barrier(partial_value.astype(jnp.bfloat16))
-    partials = rounded.astype(jnp.float32)
-    summed = lax.psum_scatter(partials.astype(jnp.bfloat16), "tp", scatter_dimension=0, tiled=True)
-    returned = lax.all_to_all(summed, "sp", split_axis=0, concat_axis=0, tiled=True)
+    arrived = lax.all_to_all(outgoing, "sp", split_axis=0, concat_axis=0, tiled=True)
+    slab = jnp.transpose(arrived, (1, 2, 0, 3)).reshape(
+        LOCAL_EXPERTS, capacity * sp_size, model_width
+    )
+    piece_rows = lax.all_gather(slab, "tp", axis=0, tiled=False)
+    partial_value = run_experts(
+        piece_rows,
+        jnp.transpose(expert_gate, (0, 2, 1)),
+        jnp.transpose(expert_up, (0, 2, 1)),
+        expert_down,
+    )
+    summed = lax.psum_scatter(partial_value, "tp", scatter_dimension=0, tiled=False)
+    summed = summed.reshape(LOCAL_EXPERTS, capacity, sp_size, model_width)
+    returned = lax.all_to_all(
+        jnp.transpose(summed, (2, 0, 1, 3)), "sp", split_axis=0, concat_axis=0, tiled=True
+    )
     routed = jnp.dot(mixing, returned.reshape(-1, model_width).astype(jnp.float32))
     shared_gate_values = jnp.dot(hidden, shared_gate, preferred_element_type=jnp.float32)
     shared_up_values = jnp.dot(hidden, shared_up, preferred_element_type=jnp.float32)

time: 292 us -> 281 us (0.962)
  matrix products: 36 us -> 8.07 us
  Pallas kernels: 21.9 us -> 37.9 us
    dot_general x2 -> x0, matrix products: 26.2 us -> none  [the longest x1 17.3 us: local(): jnp.einsum('secf,efd->secd', active, expert_down, preferred_element_type=...]
    pallas_call x0 -> x1, Pallas kernels: none -> 16 us  [run_experts(): pl.pallas_call(expert_kernel, grid=(experts, 4), out_shape=jax.ShapeDtype...]
where the time goes in v2:
time: 281 us; the launch traced here: 278 us
  waiting for transfers between devices  164 us (58%)
  Pallas kernels  37.9 us (13%)
  starting transfers between devices  22.3 us (8%)
  blocking collectives  18.6 us (7%)
  between operations  13.3 us (5%)
  matrix products  8.07 us (3%)
  local copies, waits for them, and re-layouts  7.26 us (3%)
  other arithmetic  5.98 us (2%)
    reduce_scatter x1, waiting for transfers between devices, local(): lax.psum_scatter(partial_value, 'tp', scatter_dimension=0, tiled=False)  70.4 us
    all_gather x1, waiting for transfers between devices, local(): piece_rows = lax.all_gather(slab, 'tp', axis=0, tiled=False)  60 us
    all_to_all x1, blocking collectives, local(): lax.all_to_all(outgoing, 'sp', split_axis=0, concat_axis=0, tiled=True)  18.6 us
    pallas_call x1, Pallas kernels, attend(): pl.pallas_call(attend_kernel, out_shape=jax.ShapeDtypeStruct((tokens, 128...  17.8 us
    pallas_call x1, Pallas kernels, run_experts(): pl.pallas_call(expert_kernel, grid=(experts, 4), out_shape=jax.ShapeDtype...  16 us
    ppermute x3, waiting for transfers between devices, turned_ring(): lax.ppermute(x, 'sp', [(i, i // SEQ_SHARDS * SEQ_SHARDS + (i + away) % SE...  15.1 us
    all_to_all x1, starting transfers between devices, local(): lax.all_to_all(mixed, 'tp', split_axis=0, concat_axis=1, tiled=True)  10.1 us
    all_to_all x1, waiting for transfers between devices, local(): lax.all_to_all(jnp.transpose(summed, (2, 0, 1, 3)), 'sp', split_axis=0, c...  9.38 us
  transfers between devices with their start and end apart: 8, of which 6 were waited for; matrix products, arithmetic and copies ran while one was open for 1% of the time, Pallas kernels for 8%

profile of v2, /device:TPU:1, one launch (start us, length us, event | category | flops | bytes accessed | tf_op | source)
XLA Modules:
  0.0 277.8 jit_solution(12585631901022175348)
XLA Ops:
  6.5 2.0 pad_maximum_fusion
  8.5 0.6 pad_add_fusion.place
  9.2 4.1 %prepare_heads.1 = (bf16[128,3072]{1,0:T(8,128)(2,1)}, bf16[192,1024]{1,0:T(8,128)(2,1)}) custom-call(s32[2]{0:T(128)} %pad_add_fusion.place, bf16[64,1024]{1,0:T(8,128)(2,1)} %bitcast.43, bf16[64,1024]{1,0:T(8,128)(2,1)} %bitcast.44, bf16[1024,256]{1,0:T(8,128)(2,1)} %wk.1, bf16[1024,256]{1,0:T(8,128)(2,1)} %nk.1, bf16[1024,256]{1,0:T(8,128)(2,1)} %wv.1, ...), custom_call_target="tpu_custom_call" | custom-call | tf_op jit(solution)/shard_map/prepare_heads/pallas_call | solution.py:94
  13.3 2.0 collective-permute-start
  15.3 2.5 collective-permute-start.1
  17.8 1.2 collective-permute-start.2
  18.9 0.8 copy.65
  19.8 3.6 %collective-permute-done.kv1 = bf16[192,1024]{1,0:T(8,128)(2,1)S(1)} collective-permute-done((bf16[192,1024]{1,0:T(8,128)(2,1)}, bf16[192,1024]{1,0:T(8,128)(2,1)S(1)}, u32[]{:S(2)}, u32[]{:S(2)}) %collective-permute-start) | collective-permute-done | bytes 393248 | tf_op jit(solution)/shard_map/ppermute | solution.py:223
  23.4 11.5 %collective-permute-done.1.kv2 = bf16[192,1024]{1,0:T(8,128)(2,1)S(1)} collective-permute-done((bf16[192,1024]{1,0:T(8,128)(2,1)}, bf16[192,1024]{1,0:T(8,128)(2,1)S(1)}, u32[]{:S(2)}, u32[]{:S(2)}) %collective-permute-start.1) | collective-permute-done | bytes 393248 | tf_op jit(solution)/shard_map/ppermute | solution.py:223
  34.9 0.8 copy-done.3
  35.8 17.8 %attend_blocks.1 = bf16[1024,128]{1,0:T(8,128)(2,1)} custom-call(bf16[128,3072]{1,0:T(8,128)(2,1)} %get-tuple-element.7.q, bf16[192,1024]{1,0:T(8,128)(2,1)} %get-tuple-element.8.kv0, bf16[192,1024]{1,0:T(8,128)(2,1)} %copy-done.2, bf16[192,1024]{1,0:T(8,128)(2,1)} %copy-done.3, bf16[192,1024]{1,0:T(8,128)(2,1)} %copy-done.4), custom_call_target="tpu_custom_call" | custom-call | tf_op jit(solution)/shard_map/attend_blocks/pallas_call | solution.py:177
  53.6 10.1 %all-to-all-start = ((bf16[16,64,128]{2,1,0:T(8,128)(2,1)}), bf16[16,64,128]{2,1,0:T(8,128)(2,1)S(1)}, u32[]{:S(2)}, u32[]{:S(2)}) async-start(bf16[16,64,128]{2,1,0:T(8,128)(2,1)} %bitcast.41), calls=%async_computation | async-start | bytes 524288 | tf_op jit(solution)/shard_map/all_to_all | solution.py:289
  64.4 0.7 multiply_add_fusion
  65.1 0.8 convert_reduce_fusion
  65.9 9.4 %all-to-all-done = bf16[16,64,128]{2,1,0:T(8,128)(2,1)S(1)} async-done(((bf16[16,64,128]{2,1,0:T(8,128)(2,1)}), bf16[16,64,128]{2,1,0:T(8,128)(2,1)S(1)}, u32[]{:S(2)}, u32[]{:S(2)}) %all-to-all-start) | async-done | bytes 262176 | tf_op jit(solution)/shard_map/all_to_all | solution.py:289
  75.2 5.1 %fusion.12 = (f32[64]{0:T(128)S(1)}, f32[64,2048]{1,0:T(8,128)S(1)}) fusion(bf16[2048,2048]{1,0:T(8,128)(2,1)} %all-gather.3.cloned.1.call-done, bf16[64,2048]{1,0:T(8,128)(2,1)} %param.25, bf16[16,64,128]{2,1,0:T(8,128)(2,1)S(1)} %all-to-all-done), kind=kOutput, calls=%fused_computation.34 | convolution fusion | flops 537395136 | bytes 9437440 | tf_op jit(solution)/shard_map/dot_general | solution.py:290
  80.7 0.3 convolution_convert_fusion
  81.1 0.3 reshape.73
  81.4 0.7 copy.67
  82.1 18.6 %all_to_all.29 = bf16[16,2,5,2048]{3,1,2,0:T(2,128)(2,1)S(1)} all-to-all(bf16[16,2,5,2048]{3,1,2,0:T(2,128)(2,1)S(1)} %copy.67), channel_id=1, replica_groups=mesh['sp'=16,'tp'=16] {'sp'}, dimensions={0} | all-to-all | bytes 1310720 | tf_op jit(solution)/shard_map/all_to_all | solution.py:314
  100.7 1.1 copy.68
  102.0 60.0 %all-gather.5.cloned.1.call-done.rows = bf16[16,2,80,2048]{3,2,1,0:T(8,128)(2,1)} async-done(((bf16[1,2,80,2048]{3,2,1,0:T(8,128)(2,1)}), bf16[16,2,80,2048]{3,2,1,0:T(8,128)(2,1)}) %all-gather.5.cloned.1.call-update) | async-done | bytes 10485776 | tf_op jit(solution)/shard_map/all_gather | solution.py:318
  162.0 16.0 %run_experts.1 = bf16[16,2,80,2048]{3,2,1,0:T(8,128)(2,1)} custom-call(bf16[16,2,80,2048]{3,2,1,0:T(8,128)(2,1)} %all-gather.5.cloned.1.call-done.rows, bf16[2,192,2048]{2,1,0:T(8,128)(2,1)} %bitcast.39, bf16[2,192,2048]{2,1,0:T(8,128)(2,1)} %bitcast.40, bf16[2,192,2048]{2,1,0:T(8,128)(2,1)} %down.1), custom_call_target="tpu_custom_call" | custom-call | tf_op jit(solution)/shard_map/run_experts/pallas_call | solution.py:211
  178.1 70.4 %reduce-scatter.2.cloned.1.call-done = bf16[1,2,80,2048]{3,2,1,0:T(8,128)(2,1)} async-done(((bf16[16,2,80,2048]{3,2,1,0:T(8,128)(2,1)}), bf16[1,2,80,2048]{3,2,1,0:T(8,128)(2,1)}) %reduce-scatter.2.cloned.1.call-update) | async-done | bytes 655376 | tf_op jit(solution)/shard_map/reduce_scatter | solution.py:325
  248.5 2.6 copy.79
  251.1 6.4 %all-to-all-start.2 = ((bf16[16,2,5,2048]{3,1,2,0:T(2,128)(2,1)}), bf16[16,2,5,2048]{3,1,2,0:T(2,128)(2,1)S(1)}, u32[]{:S(2)}, u32[]{:S(2)}) async-start(bf16[16,2,5,2048]{3,1,2,0:T(2,128)(2,1)} %bitcast.37), calls=%async_computation.3 | async-start | bytes 1310720 | tf_op jit(solution)/shard_map/all_to_all | solution.py:327
  257.5 0.3 fusion.14
  257.8 9.4 %all-to-all-done.2 = bf16[16,2,5,2048]{3,1,2,0:T(2,128)(2,1)S(1)} async-done(((bf16[16,2,5,2048]{3,1,2,0:T(2,128)(2,1)}), bf16[16,2,5,2048]{3,1,2,0:T(2,128)(2,1)S(1)}, u32[]{:S(2)}, u32[]{:S(2)}) %all-to-all-start.2) | async-done | bytes 655392 | tf_op jit(solution)/shard_map/all_to_all | solution.py:327
  267.1 0.3 copy.70
  267.4 0.3 reshape.74
  268.0 2.1 fusion.13
  270.4 0.9 add_convert_fusion
  (39 shorter events, 2.1 us)
Async XLA Ops:
  6.5 261.4 %copy-start = (bf16[256,2048]{1,0:T(8,128)(2,1)S(1)}, bf16[256,2048]{1,0:T(8,128)(2,1)}, u32[]{:S(2)}) copy-start(bf16[256,2048]{1,0:T(8,128)(2,1)} %param.47) | copy-start | bytes 3145732
  6.5 68.7 %all-gather.3.cloned.1.call-start = ((), (), s32[]{:S(2)}) async-start(), calls=%async_computation.4 | async-start | bytes 8912896 | tf_op jit(solution)/shard_map/all_gather | solution.py:271
  13.3 10.1 %collective-permute-start = (bf16[192,1024]{1,0:T(8,128)(2,1)}, bf16[192,1024]{1,0:T(8,128)(2,1)S(1)}, u32[]{:S(2)}, u32[]{:S(2)}) collective-permute-start(bf16[192,1024]{1,0:T(8,128)(2,1)} %get-tuple-element.8.kv0), channel_id=1, source_target_pairs={{0,16},{16,32},{32,48},{48,0},{64,80},{80,96},{96,112},{112,64},{1... | collective-permute-start | bytes 1179656 | tf_op jit(solution)/shard_map/ppermute | solution.py:223
  15.3 19.6 %collective-permute-start.1 = (bf16[192,1024]{1,0:T(8,128)(2,1)}, bf16[192,1024]{1,0:T(8,128)(2,1)S(1)}, u32[]{:S(2)}, u32[]{:S(2)}) collective-permute-start(bf16[192,1024]{1,0:T(8,128)(2,1)} %get-tuple-element.8.kv0), channel_id=1, source_target_pairs={{0,32},{16,48},{32,0},{48,16},{64,96},{80,112},{96,64},{112,80},{1... | collective-permute-start | bytes 1179656 | tf_op jit(solution)/shard_map/ppermute | solution.py:223
  17.8 17.2 %collective-permute-start.2 = (bf16[192,1024]{1,0:T(8,128)(2,1)}, bf16[192,1024]{1,0:T(8,128)(2,1)S(1)}, u32[]{:S(2)}, u32[]{:S(2)}) collective-permute-start(bf16[192,1024]{1,0:T(8,128)(2,1)} %get-tuple-element.8.kv0), channel_id=1, source_target_pairs={{0,48},{16,0},{32,16},{48,32},{64,112},{80,64},{96,80},{112,96},{1... | collective-permute-start | bytes 1179656 | tf_op jit(solution)/shard_map/ppermute | solution.py:223
  23.4 11.5 %copy-start.2 = (bf16[192,1024]{1,0:T(8,128)(2,1)}, bf16[192,1024]{1,0:T(8,128)(2,1)S(1)}, u32[]{:S(2)}) copy-start(bf16[192,1024]{1,0:T(8,128)(2,1)S(1)} %collective-permute-done.kv1) | copy-start | bytes 1179652
  34.9 0.8 copy-start.3
  34.9 0.9 copy-start.4
  53.6 21.7 %all-to-all-start = ((bf16[16,64,128]{2,1,0:T(8,128)(2,1)}), bf16[16,64,128]{2,1,0:T(8,128)(2,1)S(1)}, u32[]{:S(2)}, u32[]{:S(2)}) async-start(bf16[16,64,128]{2,1,0:T(8,128)(2,1)} %bitcast.41), calls=%async_computation | async-start | bytes 524288 | tf_op jit(solution)/shard_map/all_to_all | solution.py:289
  63.6 98.4 %all-gather.5.cloned.1.call-start = ((), (), s32[]{:S(2)}) async-start(), calls=%async_computation.5 | async-start | bytes 11141120 | tf_op jit(solution)/shard_map/all_gather | solution.py:318
  63.8 16.8 %copy-start.5 = (f32[2048]{0:T(1024)S(1)}, f32[2048]{0:T(1024)}, u32[]{:S(2)}) copy-start(f32[2048]{0:T(1024)} %param.39) | copy-start | bytes 24580
  63.8 16.8 %copy-start.6 = (f32[2048]{0:T(1024)S(1)}, f32[2048]{0:T(1024)}, u32[]{:S(2)}) copy-start(f32[2048]{0:T(1024)} %param.38) | copy-start | bytes 24580
  101.8 146.7 %reduce-scatter.2.cloned.1.call-start = ((), (), s32[]{:S(2)}) async-start(), calls=%async_computation.6 | async-start | bytes 11141120 | tf_op jit(solution)/shard_map/reduce_scatter | solution.py:325
  178.0 79.4 %copy-start.1 = (bf16[2048,256]{1,0:T(8,128)(2,1)S(1)}, bf16[2048,256]{1,0:T(8,128)(2,1)}, u32[]{:S(2)}) copy-start(bf16[2048,256]{1,0:T(8,128)(2,1)} %param.45) | copy-start | bytes 3145732
  178.1 92.3 %copy-start.7 = (f32[2048]{0:T(1024)S(1)}, f32[2048]{0:T(1024)}, u32[]{:S(2)}) copy-start(f32[2048]{0:T(1024)} %param.49) | copy-start | bytes 24580
  178.1 92.3 %copy-start.8 = (f32[2048]{0:T(1024)S(1)}, f32[2048]{0:T(1024)}, u32[]{:S(2)}) copy-start(f32[2048]{0:T(1024)} %param.48) | copy-start | bytes 24580
  251.1 16.1 %all-to-all-start.2 = ((bf16[16,2,5,2048]{3,1,2,0:T(2,128)(2,1)}), bf16[16,2,5,2048]{3,1,2,0:T(2,128)(2,1)S(1)}, u32[]{:S(2)}, u32[]{:S(2)}) async-start(bf16[16,2,5,2048]{3,1,2,0:T(2,128)(2,1)} %bitcast.37), calls=%async_computation.3 | async-start | bytes 1310720 | tf_op jit(solution)/shard_map/all_to_all | solution.py:327
Sparse Core Ops, SparseCore 0:
  9.2 60.0 all-gather.2
  101.9 60.1 all-gather.4
  178.2 70.2 reduce-scatter.1

commit v3 on v2

--- a/solution.py
+++ b/solution.py
@@ -1,3 +1,5 @@
+import functools
+
 import jax
 import jax.numpy as jnp
 from jax import lax
@@ -56,10 +58,10 @@
     return ((jnp.cos(row_angle), jnp.sin(row_angle)), (jnp.cos(col_angle), jnp.sin(col_angle)))
 
 
-def prepare_kernel(place, wqt, nqt, wk, nk, wv, nv, wqg, wkg, nqg, nkg, q_out, kv_out, turn):
+def prepare_kernel(wqt, nqt, wk, nk, wv, nv, wqg, wkg, nqg, nkg, q_out, kv_out, turn):
     tokens = wqt.shape[1]
-    tp = place[0]
-    first_row = place[1]
+    tp = lax.axis_index("tp")
+    first_row = lax.axis_index("sp") % SEQ_SHARDS * (tokens // GRID_WIDTH)
     wide_tables = angle_tables(WIDE_SIZE // 4, first_row, tokens)
     narrow_tables = angle_tables(NARROW_SIZE // 4, first_row, tokens)
 
@@ -88,7 +90,7 @@
         q_out[64:96, tokens * (head + 1) : tokens * (head + 2)] = narrow.astype(jnp.bfloat16)
 
 
-def prepare(place, wqt, nqt, wk, nk, wv, nv, wqg, wkg, nqg, nkg):
+def prepare(wqt, nqt, wk, nk, wv, nv, wqg, wkg, nqg, nkg):
     tokens = wqt.shape[1]
     vmem = pl.BlockSpec(memory_space=pltpu.VMEM)
     return pl.pallas_call(
@@ -97,23 +99,30 @@
             jax.ShapeDtypeStruct((128, 3 * tokens), jnp.bfloat16),
             jax.ShapeDtypeStruct((192, tokens), jnp.bfloat16),
         ),
-        in_specs=[pl.BlockSpec(memory_space=pltpu.SMEM)] + [vmem] * 10,
+        in_specs=[vmem] * 10,
         out_specs=(vmem, vmem),
         scratch_shapes=[pltpu.VMEM((128, tokens), jnp.float32)],
         name="prepare_heads",
     )(
-        place, wqt, nqt, wk, nk, wv, nv,
+        wqt, nqt, wk, nk, wv, nv,
         wqg.reshape(1, -1), wkg.reshape(1, -1), nqg.reshape(1, -1), nkg.reshape(1, -1),
     )
 
 
-def attend_kernel(q, kv0, kv1, kv2, kv3, out, keys, values, scores0, scores1, mixed):
-    tokens = kv0.shape[1]
-    total = 4 * tokens
+def attend_kernel(*refs, pieces, resumed):
+    q = refs[0]
+    packs = refs[1 : 1 + pieces]
+    refs = refs[1 + pieces :]
+    if resumed:
+        before, peak_before, out, keys, values, scores0, scores1, mixed = refs
+    else:
+        sums, peaks, keys, values, scores0, scores1 = refs
+    tokens = packs[0].shape[1]
+    total = pieces * tokens
     blocks = q.shape[1] // BLOCK_Q
     wide_blocks = tokens // BLOCK_Q
     values[KEY_ROWS:, :] = jnp.ones((ONES_ROWS, total), jnp.bfloat16)
-    for n, kv in enumerate((kv0, kv1, kv2, kv3)):
+    for n, kv in enumerate(packs):
         piece = kv[0:KEY_ROWS, :].astype(jnp.float32)
         padded = jnp.concatenate([piece, jnp.zeros((128 - KEY_ROWS, tokens), jnp.float32)], axis=0)
         keys[n * tokens : (n + 1) * tokens, :] = padded.T.astype(jnp.bfloat16)
@@ -137,8 +146,13 @@
             jnp.float32(WIDE_SIZE**-0.5 * LOG2E),
             jnp.float32(NARROW_SIZE**-0.5 * LOG2E),
         )
+        if resumed:
+            earlier = peak_before[b][0:1]
+            peak = jnp.maximum(peak, earlier)
+            total_mixed = before[b] * jnp.exp2((earlier - peak) * factor)
+        else:
+            total_mixed = jnp.zeros((KEY_ROWS + ONES_ROWS, BLOCK_Q), jnp.float32)
         next_largest = lowest
-        total_mixed = jnp.zeros((KEY_ROWS + ONES_ROWS, BLOCK_Q), jnp.float32)
         for c in range(total // CHUNK):
             next_largest = scored(c, query, following, next_largest)
             raw = current[c * CHUNK : (c + 1) * CHUNK, :]
@@ -146,7 +160,11 @@
             total_mixed = total_mixed + jnp.dot(
                 values[:, c * CHUNK : (c + 1) * CHUNK], weights, preferred_element_type=jnp.float32
             )
-        mixed[b] = total_mixed[:KEY_ROWS] / total_mixed[KEY_ROWS : KEY_ROWS + 1]
+        if resumed:
+            mixed[b] = total_mixed[:KEY_ROWS] / total_mixed[KEY_ROWS : KEY_ROWS + 1]
+        else:
+            sums[b] = total_mixed
+            peaks[b] = jnp.broadcast_to(peak, (8, BLOCK_Q))
         return next_largest
 
     largest = lowest
@@ -159,6 +177,8 @@
         return step(2 * i + 1, scores1, scores0, largest)
 
     lax.fori_loop(0, blocks // 2, pair, largest)
+    if not resumed:
+        return
     for b in range(wide_blocks):
         rows = jnp.concatenate(
             [
@@ -171,51 +191,78 @@
         out[b * BLOCK_Q : (b + 1) * BLOCK_Q, :] = rows.T.astype(jnp.bfloat16)
 
 
-def attend(q, pieces):
-    tokens = pieces[0].shape[1]
+def attend(q, packs, earlier=()):
+    tokens = packs[0].shape[1]
+    total = len(packs) * tokens
+    blocks = q.shape[1] // BLOCK_Q
+    sums = jax.ShapeDtypeStruct((blocks, KEY_ROWS + ONES_ROWS, BLOCK_Q), jnp.float32)
+    peaks = jax.ShapeDtypeStruct((blocks, 8, BLOCK_Q), jnp.float32)
+    vmem = pl.BlockSpec(memory_space=pltpu.VMEM)
+    scratch = [
+        pltpu.VMEM((total, 128), jnp.bfloat16),
+        pltpu.VMEM((KEY_ROWS + ONES_ROWS, total), jnp.bfloat16),
+        pltpu.VMEM((total, BLOCK_Q), jnp.float32),
+        pltpu.VMEM((total, BLOCK_Q), jnp.float32),
+    ]
+    if earlier:
+        scratch.append(pltpu.VMEM((blocks, KEY_ROWS, BLOCK_Q), jnp.float32))
+    return pl.pallas_call(
+        functools.partial(attend_kernel, pieces=len(packs), resumed=bool(earlier)),
+        out_shape=jax.ShapeDtypeStruct((tokens, 128), jnp.bfloat16) if earlier else (sums, peaks),
+        in_specs=[vmem] * (1 + len(packs) + len(earlier)),
+        out_specs=vmem if earlier else (vmem, vmem),
+        scratch_shapes=scratch,
+        name="attend_rest" if earlier else "attend_first",
+    )(q, *packs, *earlier)
+
+
+def stack_kernel(first, second, out):
+    out[: first.shape[0]] = first[...]
+    out[first.shape[0] :] = second[...]
+
+
+def stacked(first, second):
     vmem = pl.BlockSpec(memory_space=pltpu.VMEM)
     return pl.pallas_call(
-        attend_kernel,
-        out_shape=jax.ShapeDtypeStruct((tokens, 128), jnp.bfloat16),
-        in_specs=[vmem] * 5,
+        stack_kernel,
+        out_shape=jax.ShapeDtypeStruct((2 * first.shape[0], first.shape[1]), first.dtype),
+        in_specs=[vmem, vmem],
         out_specs=vmem,
-        scratch_shapes=[
-            pltpu.VMEM((4 * tokens, 128), jnp.bfloat16),
-            pltpu.VMEM((KEY_ROWS + ONES_ROWS, 4 * tokens), jnp.bfloat16),
-            pltpu.VMEM((4 * tokens, BLOCK_Q), jnp.float32),
-            pltpu.VMEM((4 * tokens, BLOCK_Q), jnp.float32),
-            pltpu.VMEM((q.shape[1] // BLOCK_Q, KEY_ROWS, BLOCK_Q), jnp.float32),
-        ],
-        name="attend_blocks",
-    )(q, *pieces)
-
-
-def expert_kernel(rows, gate, up, down, out):
-    e = pl.program_id(0)
+        name="stack_rows",
+    )(first, second)
+
+
+def expert_kernel(rows, gate, gate_far, up, up_far, down, down_far, out):
     sources, _, slots, width = rows.shape
     x = rows[...].reshape(sources * slots, width)
     along = (((1,), (1,)), ((), ()))
-    gate_values = lax.dot_general(x, gate[e], along, preferred_element_type=jnp.float32)
-    up_values = lax.dot_general(x, up[e], along, preferred_element_type=jnp.float32)
-    active = gate_values / (1.0 + jnp.exp(-gate_values)) * up_values
-    partial_value = jnp.dot(
-        active.astype(jnp.bfloat16), down[e], preferred_element_type=jnp.float32
-    )
+    partial_value = jnp.zeros(x.shape, jnp.float32)
+    for g, u, d in ((gate, up, down), (gate_far, up_far, down_far)):
+        gate_values = lax.dot_general(x, g[0], along, preferred_element_type=jnp.float32)
+        up_values = lax.dot_general(x, u[0], along, preferred_element_type=jnp.float32)
+        active = gate_values / (1.0 + jnp.exp(-gate_values)) * up_values
+        partial_value = partial_value + jnp.dot(
+            active.astype(jnp.bfloat16), d[0], preferred_element_type=jnp.float32
+        )
     out[...] = partial_value.astype(jnp.bfloat16).reshape(rows.shape)
 
 
-def run_experts(rows, gate, up, down):
+def run_experts(rows, *weights):
     sources, experts, slots, width = rows.shape
-    block = pl.BlockSpec((sources // 4, 1, slots, width), lambda e, r: (r, e, 0, 0))
-    whole = pl.BlockSpec(memory_space=pltpu.VMEM)
+    block = pl.BlockSpec((sources // 2, 1, slots, width), lambda e, r: (r, e, 0, 0))
+    weight = pl.BlockSpec((1, *weights[0].shape[1:]), lambda e, r: (e, 0, 0))
     return pl.pallas_call(
         expert_kernel,
-        grid=(experts, 4),
+        grid=(experts, 2),
         out_shape=jax.ShapeDtypeStruct(rows.shape, jnp.bfloat16),
-        in_specs=[block, whole, whole, whole],
+        in_specs=[block] + [weight] * len(weights),
         out_specs=block,
         name="run_experts",
-    )(rows, gate, up, down)
+    )(rows, *weights)
+
+
+def other_core(x):
+    return lax.ppermute(x, "tp", [(i, i ^ 1) for i in range(lax.axis_size("tp"))])
 
 
 def turned_ring(x, away):
@@ -262,17 +309,10 @@
     second_bias,
 ):
     tp_size = lax.axis_size("tp")
-    place = jnp.stack(
-        [
-            lax.axis_index("tp"),
-            lax.axis_index("sp") % SEQ_SHARDS * (wide_query.shape[0] // GRID_WIDTH),
-        ]
-    )
     out_weights = lax.all_gather(
-        jnp.concatenate([wide_out, narrow_out], axis=0), "tp", axis=0, tiled=True
+        stacked(wide_out, narrow_out), "tp", axis=0, tiled=True
     )
     rotated_queries, own_pack = prepare(
-        place,
         wide_query.T,
         narrow_query.T,
         wide_keys,
@@ -285,7 +325,8 @@
         narrow_key_gain,
     )
     packs = [own_pack] + [turned_ring(own_pack, away) for away in range(1, SEQ_SHARDS)]
-    mixed = attend(rotated_queries, packs)
+    earlier = attend(rotated_queries, packs[:2])
+    mixed = attend(rotated_queries, packs[2:], earlier)
     tokens = lax.all_to_all(mixed, "tp", split_axis=0, concat_axis=1, tiled=True)
     projected = jnp.dot(tokens, out_weights, preferred_element_type=jnp.float32)
     hidden = layer_norm(ALPHA * residual.astype(jnp.float32) + projected, first_gain, first_bias)
@@ -315,14 +356,22 @@
     slab = jnp.transpose(arrived, (1, 2, 0, 3)).reshape(
         LOCAL_EXPERTS, capacity * sp_size, model_width
     )
-    piece_rows = lax.all_gather(slab, "tp", axis=0, tiled=False)
+    core_lines = [list(range(core, tp_size, 2)) for core in range(2)]
+    piece_rows = lax.all_gather(slab, "tp", axis=0, tiled=False, axis_index_groups=core_lines)
+    gate_rows = jnp.transpose(expert_gate, (0, 2, 1))
+    up_rows = jnp.transpose(expert_up, (0, 2, 1))
     partial_value = run_experts(
         piece_rows,
-        jnp.transpose(expert_gate, (0, 2, 1)),
-        jnp.transpose(expert_up, (0, 2, 1)),
+        gate_rows,
+        other_core(gate_rows),
+        up_rows,
+        other_core(up_rows),
         expert_down,
-    )
-    summed = lax.psum_scatter(partial_value, "tp", scatter_dimension=0, tiled=False)
+        other_core(expert_down),
+    )
+    summed = lax.psum_scatter(
+        partial_value, "tp", scatter_dimension=0, tiled=False, axis_index_groups=core_lines
+    )
     summed = summed.reshape(LOCAL_EXPERTS, capacity, sp_size, model_width)
     returned = lax.all_to_all(
         jnp.transpose(summed, (2, 0, 1, 3)), "sp", split_axis=0, concat_axis=0, tiled=True

time: 281 us -> 273 us (0.972)
  waiting for transfers between devices: 164 us -> 149 us
  Pallas kernels: 37.9 us -> 42.8 us
  starting transfers between devices: 22.3 us -> 26.4 us
  other arithmetic: 5.98 us -> 2.65 us
    ppermute x3, waiting for transfers between devices: 15.1 us -> 4.27 us  [turned_ring(): lax.ppermute(x, 'sp', [(i, i // SEQ_SHARDS * SEQ_SHARDS + (i + away) % SE...]
    all_gather x2, waiting for transfers between devices: 60 us -> 52 us  [the longest x1 51.2 us: local(): lax.all_gather(slab, 'tp', axis=0, tiled=False, axis_index_groups=core_li...]
    reduce_scatter x1, waiting for transfers between devices: 70.4 us -> 64.1 us  [local(): lax.psum_scatter(partial_value, 'tp', scatter_dimension=0, tiled=False, a...]
    pallas_call x2 -> x4, Pallas kernels: 33.8 us -> 38.8 us  [the longest x2 22.9 us: attend(): pl.pallas_call(functools.partial(attend_kernel, pieces=len(packs), resume...]
    ppermute x0 -> x3, waiting for transfers between devices: none -> 4.76 us  [other_core(): lax.ppermute(x, 'tp', [(i, i ^ 1) for i in range(lax.axis_size('tp'))])]
    all_to_all x1, waiting for transfers between devices: 9.37 us -> 13.1 us  [local(): lax.all_to_all(mixed, 'tp', split_axis=0, concat_axis=1, tiled=True)]
  transfers between devices with their start and end apart: 8 -> 11, of which waited for: 6 -> 9; matrix products, arithmetic and copies ran while one was open for 1% -> 1% of each run, Pallas kernels for 8% -> 10%
where the time goes in v3:
time: 273 us; the launch traced here: 272 us
  waiting for transfers between devices  149 us (55%)
  Pallas kernels  42.8 us (16%)
  starting transfers between devices  26.4 us (10%)
  blocking collectives  19 us (7%)
  between operations  13.3 us (5%)
  local copies, waits for them, and re-layouts  9.86 us (4%)
  matrix products  9.2 us (3%)
    reduce_scatter x1, waiting for transfers between devices, local(): lax.psum_scatter(partial_value, 'tp', scatter_dimension=0, tiled=False, a...  64.1 us
    all_gather x1, waiting for transfers between devices, local(): lax.all_gather(slab, 'tp', axis=0, tiled=False, axis_index_groups=core_li...  51.2 us
    pallas_call x2, Pallas kernels, attend(): pl.pallas_call(functools.partial(attend_kernel, pieces=len(packs), resume...  22.9 us
    all_to_all x1, blocking collectives, local(): lax.all_to_all(outgoing, 'sp', split_axis=0, concat_axis=0, tiled=True)  19 us
    pallas_call x1, Pallas kernels, run_experts(): pl.pallas_call(expert_kernel, grid=(experts, 2), out_shape=jax.ShapeDtype...  13.9 us
    all_to_all x1, waiting for transfers between devices, local(): lax.all_to_all(mixed, 'tp', split_axis=0, concat_axis=1, tiled=True)  13.1 us
    all_to_all x1, starting transfers between devices, local(): lax.all_to_all(mixed, 'tp', split_axis=0, concat_axis=1, tiled=True)  12 us
    all_to_all x1, waiting for transfers between devices, local(): lax.all_to_all(jnp.transpose(summed, (2, 0, 1, 3)), 'sp', split_axis=0, c...  10.8 us
  transfers between devices with their start and end apart: 11, of which 9 were waited for; matrix products, arithmetic and copies ran while one was open for 1% of the time, Pallas kernels for 10%

profile of v3, /device:TPU:1, one launch (start us, length us, event | category | flops | bytes accessed | tf_op | source)
XLA Modules:
  0.0 272.3 jit_solution(13199492410373477270)
XLA Ops:
  6.5 2.0 stack_rows.1
  8.5 4.0 %prepare_heads.1 = (bf16[128,3072]{1,0:T(8,128)(2,1)}, bf16[192,1024]{1,0:T(8,128)(2,1)}) custom-call(bf16[64,1024]{1,0:T(8,128)(2,1)} %bitcast.43, bf16[64,1024]{1,0:T(8,128)(2,1)} %bitcast.44, bf16[1024,256]{1,0:T(8,128)(2,1)} %wk.1, bf16[1024,256]{1,0:T(8,128)(2,1)} %nk.1, bf16[1024,256]{1,0:T(8,128)(2,1)} %wv.1, bf16[1024,256]{1,0:T(8,128)(2,1)} %nv.1, ...), custom_call_target="tpu_custom_call" | custom-call | tf_op jit(solution)/shard_map/prepare_heads/pallas_call | solution.py:96
  12.6 2.0 collective-permute-start.2
  14.6 2.5 collective-permute-start
  17.0 1.2 collective-permute-start.1
  18.4 4.3 %collective-permute-done.2.refs_2_ = bf16[192,1024]{1,0:T(8,128)(2,1)S(1)} collective-permute-done((bf16[192,1024]{1,0:T(8,128)(2,1)}, bf16[192,1024]{1,0:T(8,128)(2,1)S(1)}, u32[]{:S(2)}, u32[]{:S(2)}) %collective-permute-start.2) | collective-permute-done | bytes 393248 | tf_op jit(solution)/shard_map/ppermute | solution.py:270
  22.7 0.7 copy-done.8
  23.4 11.2 %attend_first.1 = (f32[12,112,256]{2,1,0:T(8,128)}, f32[12,8,256]{2,1,0:T(8,128)}) custom-call(bf16[128,3072]{1,0:T(8,128)(2,1)} %get-tuple-element.9.refs_0_, bf16[192,1024]{1,0:T(8,128)(2,1)} %get-tuple-element.10.refs_1_, bf16[192,1024]{1,0:T(8,128)(2,1)} %copy-done.8), custom_call_target="tpu_custom_call" | custom-call | tf_op jit(solution)/shard_map/attend_first/pallas_call | solution.py:209
  35.5 11.7 %attend_rest.1 = bf16[1024,128]{1,0:T(8,128)(2,1)} custom-call(bf16[128,3072]{1,0:T(8,128)(2,1)} %get-tuple-element.9.refs_0_, bf16[192,1024]{1,0:T(8,128)(2,1)} %copy-done.6, bf16[192,1024]{1,0:T(8,128)(2,1)} %copy-done.7, f32[12,112,256]{2,1,0:T(8,128)} %get-tuple-element.11.refs_3_, f32[12,8,256]{2,1,0:T(8,128)} %get-tuple-element.12.refs_4_), custom_call_target="tpu_custom_call" | custom-call | tf_op jit(solution)/shard_map/attend_rest/pallas_call | solution.py:209
  47.2 12.0 %all-to-all-start = ((bf16[16,64,128]{2,1,0:T(8,128)(2,1)}), bf16[16,64,128]{2,1,0:T(8,128)(2,1)S(1)}, u32[]{:S(2)}, u32[]{:S(2)}) async-start(bf16[16,64,128]{2,1,0:T(8,128)(2,1)} %bitcast.41), calls=%async_computation | async-start | bytes 524288 | tf_op jit(solution)/shard_map/all_to_all | solution.py:330
  60.6 13.1 %all-to-all-done = bf16[16,64,128]{2,1,0:T(8,128)(2,1)S(1)} async-done(((bf16[16,64,128]{2,1,0:T(8,128)(2,1)}), bf16[16,64,128]{2,1,0:T(8,128)(2,1)S(1)}, u32[]{:S(2)}, u32[]{:S(2)}) %all-to-all-start) | async-done | bytes 262176 | tf_op jit(solution)/shard_map/all_to_all | solution.py:330
  73.8 0.8 all-gather.3.cloned.1.call-done
  74.6 5.1 %fusion.12 = (f32[64]{0:T(128)S(1)}, f32[64,2048]{1,0:T(8,128)S(1)}) fusion(bf16[2048,2048]{1,0:T(8,128)(2,1)} %all-gather.3.cloned.1.call-done, bf16[64,2048]{1,0:T(8,128)(2,1)S(1)} %copy-done.9, bf16[16,64,128]{2,1,0:T(8,128)(2,1)S(1)} %all-to-all-done), kind=kOutput, calls=%fused_computation.32 | convolution fusion | flops 537395136 | bytes 9437440 | tf_op jit(solution)/shard_map/dot_general | solution.py:331
  80.7 0.7 copy.67
  81.5 19.0 %all_to_all.29 = bf16[16,2,5,2048]{3,1,2,0:T(2,128)(2,1)S(1)} all-to-all(bf16[16,2,5,2048]{3,1,2,0:T(2,128)(2,1)S(1)} %copy.67), channel_id=1, replica_groups=mesh['sp'=16,'tp'=16] {'sp'}, dimensions={0} | all-to-all | bytes 1310720 | tf_op jit(solution)/shard_map/all_to_all | solution.py:355
  100.5 1.1 copy.68
  101.6 1.6 collective-permute-start.3
  103.8 2.5 collective-permute-done.3.gate_far
  106.3 1.2 copy-done.2
  107.4 1.1 collective-permute-done.4.up_far
  108.5 1.2 copy-done.3
  109.8 1.1 collective-permute-done.5.down_far
  110.9 51.2 %all-gather.5.cloned.1.call-done.rows = bf16[8,2,80,2048]{3,2,1,0:T(8,128)(2,1)} async-done(((bf16[1,2,80,2048]{3,2,1,0:T(8,128)(2,1)}), bf16[8,2,80,2048]{3,2,1,0:T(8,128)(2,1)}) %all-gather.5.cloned.1.call-update) | async-done | bytes 5242896 | tf_op jit(solution)/shard_map/all_gather | solution.py:360
  162.1 13.9 %run_experts.1 = bf16[8,2,80,2048]{3,2,1,0:T(8,128)(2,1)} custom-call(bf16[8,2,80,2048]{3,2,1,0:T(8,128)(2,1)} %all-gather.5.cloned.1.call-done.rows, bf16[2,192,2048]{2,1,0:T(8,128)(2,1)} %bitcast.37, bf16[2,192,2048]{2,1,0:T(8,128)(2,1)} %copy-done.2, bf16[2,192,2048]{2,1,0:T(8,128)(2,1)} %bitcast.40, bf16[2,192,2048]{2,1,0:T(8,128)(2,1)} %copy-done.3, ...), custom_call_target="tpu_custom_call" | custom-call | tf_op jit(solution)/shard_map/run_experts/pallas_call | solution.py:254
  176.1 64.1 %reduce-scatter.2.cloned.1.call-done = bf16[1,2,80,2048]{3,2,1,0:T(8,128)(2,1)} async-done(((bf16[8,2,80,2048]{3,2,1,0:T(8,128)(2,1)}), bf16[1,2,80,2048]{3,2,1,0:T(8,128)(2,1)}) %reduce-scatter.2.cloned.1.call-update) | async-done | bytes 655376 | tf_op jit(solution)/shard_map/reduce_scatter | solution.py:372
  240.2 2.6 copy.79
  242.8 6.5 %all-to-all-start.2 = ((bf16[16,2,5,2048]{3,1,2,0:T(2,128)(2,1)}), bf16[16,2,5,2048]{3,1,2,0:T(2,128)(2,1)S(1)}, u32[]{:S(2)}, u32[]{:S(2)}) async-start(bf16[16,2,5,2048]{3,1,2,0:T(2,128)(2,1)} %bitcast.35), calls=%async_computation.3 | async-start | bytes 1310720 | tf_op jit(solution)/shard_map/all_to_all | solution.py:376
  249.3 0.9 fusion.14
  250.3 10.8 %all-to-all-done.2 = bf16[16,2,5,2048]{3,1,2,0:T(2,128)(2,1)S(1)} async-done(((bf16[16,2,5,2048]{3,1,2,0:T(2,128)(2,1)}), bf16[16,2,5,2048]{3,1,2,0:T(2,128)(2,1)S(1)}, u32[]{:S(2)}, u32[]{:S(2)}) %all-to-all-start.2) | async-done | bytes 655392 | tf_op jit(solution)/shard_map/all_to_all | solution.py:376
  261.7 1.1 convolution_add_fusion.2
  262.9 1.8 fusion.13
  265.0 0.9 add_convert_fusion
  (59 shorter events, 5.1 us)
Async XLA Ops:
  6.5 256.2 %copy-start = (bf16[256,2048]{1,0:T(8,128)(2,1)S(1)}, bf16[256,2048]{1,0:T(8,128)(2,1)}, u32[]{:S(2)}) copy-start(bf16[256,2048]{1,0:T(8,128)(2,1)} %param.47) | copy-start | bytes 3145732
  6.5 68.1 %all-gather.3.cloned.1.call-start = ((), (), s32[]{:S(2)}) async-start(), calls=%async_computation.4 | async-start | bytes 8912896 | tf_op jit(solution)/shard_map/all_gather | solution.py:312
  8.5 9.7 %copy-start.14 = (s32[64,2]{0,1:T(2,128)S(1)}, s32[64,2]{0,1:T(2,128)}, u32[]{:S(2)}) copy-start(s32[64,2]{0,1:T(2,128)} %param.40) | copy-start | bytes 1540
  12.6 10.1 %collective-permute-start.2 = (bf16[192,1024]{1,0:T(8,128)(2,1)}, bf16[192,1024]{1,0:T(8,128)(2,1)S(1)}, u32[]{:S(2)}, u32[]{:S(2)}) collective-permute-start(bf16[192,1024]{1,0:T(8,128)(2,1)} %get-tuple-element.10.refs_1_), channel_id=1, source_target_pairs={{0,16},{16,32},{32,48},{48,0},{64,80},{80,96},{96,112},{112,64},{1... | collective-permute-start | bytes 1179656 | tf_op jit(solution)/shard_map/ppermute | solution.py:270
  14.6 20.0 %collective-permute-start = (bf16[192,1024]{1,0:T(8,128)(2,1)}, bf16[192,1024]{1,0:T(8,128)(2,1)S(1)}, u32[]{:S(2)}, u32[]{:S(2)}) collective-permute-start(bf16[192,1024]{1,0:T(8,128)(2,1)} %get-tuple-element.10.refs_1_), channel_id=1, source_target_pairs={{0,32},{16,48},{32,0},{48,16},{64,96},{80,112},{96,64},{112,80},{1... | collective-permute-start | bytes 1179656 | tf_op jit(solution)/shard_map/ppermute | solution.py:270
  17.0 17.6 %collective-permute-start.1 = (bf16[192,1024]{1,0:T(8,128)(2,1)}, bf16[192,1024]{1,0:T(8,128)(2,1)S(1)}, u32[]{:S(2)}, u32[]{:S(2)}) collective-permute-start(bf16[192,1024]{1,0:T(8,128)(2,1)} %get-tuple-element.10.refs_1_), channel_id=1, source_target_pairs={{0,48},{16,0},{32,16},{48,32},{64,112},{80,64},{96,80},{112,96},{1... | collective-permute-start | bytes 1179656 | tf_op jit(solution)/shard_map/ppermute | solution.py:270
  22.7 0.7 copy-start.8
  34.6 0.7 copy-start.6
  34.6 0.9 copy-start.7
  35.5 24.4 %copy-start.15 = (f32[64,2]{0,1:T(2,128)S(1)}, f32[64,2]{0,1:T(2,128)}, u32[]{:S(2)}) copy-start(f32[64,2]{0,1:T(2,128)} %param.41) | copy-start | bytes 1540
  35.5 39.1 %copy-start.9 = (bf16[64,2048]{1,0:T(8,128)(2,1)S(1)}, bf16[64,2048]{1,0:T(8,128)(2,1)}, u32[]{:S(2)}) copy-start(bf16[64,2048]{1,0:T(8,128)(2,1)} %param.25) | copy-start | bytes 786436
  47.2 26.6 %all-to-all-start = ((bf16[16,64,128]{2,1,0:T(8,128)(2,1)}), bf16[16,64,128]{2,1,0:T(8,128)(2,1)S(1)}, u32[]{:S(2)}, u32[]{:S(2)}) async-start(bf16[16,64,128]{2,1,0:T(8,128)(2,1)} %bitcast.41), calls=%async_computation | async-start | bytes 524288 | tf_op jit(solution)/shard_map/all_to_all | solution.py:330
  59.2 102.9 %all-gather.5.cloned.1.call-start = ((), (), s32[]{:S(2)}) async-start(), calls=%async_computation.5 | async-start | bytes 5898240 | tf_op jit(solution)/shard_map/all_gather | solution.py:360
  60.6 19.3 %copy-start.10 = (f32[2048]{0:T(1024)S(1)}, f32[2048]{0:T(1024)}, u32[]{:S(2)}) copy-start(f32[2048]{0:T(1024)} %param.39) | copy-start | bytes 24580
  60.6 19.3 %copy-start.11 = (f32[2048]{0:T(1024)S(1)}, f32[2048]{0:T(1024)}, u32[]{:S(2)}) copy-start(f32[2048]{0:T(1024)} %param.38) | copy-start | bytes 24580
  81.5 20.1 %copy-start.1 = (bf16[2,2048,192]{1,2,0:T(8,128)(2,1)S(1)}, bf16[2,2048,192]{1,2,0:T(8,128)(2,1)}, u32[]{:S(2)}) copy-start(bf16[2,2048,192]{1,2,0:T(8,128)(2,1)} %param.42) | copy-start | bytes 4718596
  101.6 138.6 %reduce-scatter.2.cloned.1.call-start = ((), (), s32[]{:S(2)}) async-start(), calls=%async_computation.6 | async-start | bytes 5898240 | tf_op jit(solution)/shard_map/reduce_scatter | solution.py:372
  101.6 4.7 %collective-permute-start.3 = (bf16[2,192,2048]{2,1,0:T(8,128)(2,1)S(1)}, bf16[2,192,2048]{2,1,0:T(8,128)(2,1)S(1)}, u32[]{:S(2)}, u32[]{:S(2)}) collective-permute-start(bf16[2,192,2048]{2,1,0:T(8,128)(2,1)S(1)} %bitcast.38), channel_id=1, source_target_pairs={{0,1},{1,0},{2,3},{3,2},{4,5},{5,4},{6,7},{7,6},{8,9},{9,8},{10,11... | collective-permute-start | bytes 4718600 | tf_op jit(solution)/shard_map/ppermute | solution.py:265
  103.3 5.3 %collective-permute-start.4 = (bf16[2,192,2048]{2,1,0:T(8,128)(2,1)}, bf16[2,192,2048]{2,1,0:T(8,128)(2,1)S(1)}, u32[]{:S(2)}, u32[]{:S(2)}) collective-permute-start(bf16[2,192,2048]{2,1,0:T(8,128)(2,1)} %bitcast.39), channel_id=1, source_target_pairs={{0,1},{1,0},{2,3},{3,2},{4,5},{5,4},{6,7},{7,6},{8,9},{9,8},{10,11... | collective-permute-start | bytes 4718600 | tf_op jit(solution)/shard_map/ppermute | solution.py:265
  103.4 7.6 %collective-permute-start.5 = (bf16[2,192,2048]{2,1,0:T(8,128)(2,1)}, bf16[2,192,2048]{2,1,0:T(8,128)(2,1)}, u32[]{:S(2)}, u32[]{:S(2)}) collective-permute-start(bf16[2,192,2048]{2,1,0:T(8,128)(2,1)} %down.1), channel_id=1, source_target_pairs={{0,1},{1,0},{2,3},{3,2},{4,5},{5,4},{6,7},{7,6},{8,9},{9,8},{10,11... | collective-permute-start | bytes 4718600 | tf_op jit(solution)/shard_map/ppermute | solution.py:265
  106.3 1.2 copy-start.2
  108.5 1.2 copy-start.3
  176.1 73.2 %copy-start.4 = (bf16[2048,256]{1,0:T(8,128)(2,1)S(1)}, bf16[2048,256]{1,0:T(8,128)(2,1)}, u32[]{:S(2)}) copy-start(bf16[2048,256]{1,0:T(8,128)(2,1)} %param.45) | copy-start | bytes 3145732
  242.8 18.3 %all-to-all-start.2 = ((bf16[16,2,5,2048]{3,1,2,0:T(2,128)(2,1)}), bf16[16,2,5,2048]{3,1,2,0:T(2,128)(2,1)S(1)}, u32[]{:S(2)}, u32[]{:S(2)}) async-start(bf16[16,2,5,2048]{3,1,2,0:T(2,128)(2,1)} %bitcast.35), calls=%async_computation.3 | async-start | bytes 1310720 | tf_op jit(solution)/shard_map/all_to_all | solution.py:376
  261.7 1.2 copy-start.5
  262.9 2.0 copy-start.12
  262.9 2.0 copy-start.13
Sparse Core Ops, SparseCore 0:
  9.2 65.3 all-gather.2
  101.7 60.3 all-gather.4
  176.2 63.9 reduce-scatter.1

commit v4 on v3

--- a/solution.py
+++ b/solution.py
@@ -188,7 +188,9 @@
             ],
             axis=0,
         )
-        out[b * BLOCK_Q : (b + 1) * BLOCK_Q, :] = rows.T.astype(jnp.bfloat16)
+        rows = rows.astype(jnp.bfloat16)
+        for n in range(BLOCK_Q // 128):
+            out[b * (BLOCK_Q // 128) + n] = rows[:, n * 128 : (n + 1) * 128]
 
 
 def attend(q, packs, earlier=()):
@@ -208,7 +210,9 @@
         scratch.append(pltpu.VMEM((blocks, KEY_ROWS, BLOCK_Q), jnp.float32))
     return pl.pallas_call(
         functools.partial(attend_kernel, pieces=len(packs), resumed=bool(earlier)),
-        out_shape=jax.ShapeDtypeStruct((tokens, 128), jnp.bfloat16) if earlier else (sums, peaks),
+        out_shape=jax.ShapeDtypeStruct((tokens // 128, 128, 128), jnp.bfloat16)
+        if earlier
+        else (sums, peaks),
         in_specs=[vmem] * (1 + len(packs) + len(earlier)),
         out_specs=vmem if earlier else (vmem, vmem),
         scratch_shapes=scratch,
@@ -216,47 +220,64 @@
     )(q, *packs, *earlier)
 
 
-def stack_kernel(first, second, out):
-    out[: first.shape[0]] = first[...]
-    out[first.shape[0] :] = second[...]
+def stack_kernel(first, second, out, arrived):
+    rows = first.shape[0]
+    copies = [
+        pltpu.make_async_copy(first, out.at[pl.ds(0, rows)], arrived.at[0]),
+        pltpu.make_async_copy(second, out.at[pl.ds(rows, second.shape[0])], arrived.at[1]),
+    ]
+    for copy in copies:
+        copy.start()
+    for copy in copies:
+        copy.wait()
 
 
 def stacked(first, second):
-    vmem = pl.BlockSpec(memory_space=pltpu.VMEM)
+    anywhere = pl.BlockSpec(memory_space=pl.ANY)
     return pl.pallas_call(
         stack_kernel,
         out_shape=jax.ShapeDtypeStruct((2 * first.shape[0], first.shape[1]), first.dtype),
-        in_specs=[vmem, vmem],
-        out_specs=vmem,
+        in_specs=[anywhere, anywhere],
+        out_specs=anywhere,
+        scratch_shapes=[pltpu.SemaphoreType.DMA((2,))],
         name="stack_rows",
     )(first, second)
 
 
-def expert_kernel(rows, gate, gate_far, up, up_far, down, down_far, out):
+def expert_kernel(rows, gate, gate_far, up, up_far, down, down_far, out, joined, joined_down):
     sources, _, slots, width = rows.shape
+    part = gate.shape[1]
+    for n, piece in enumerate((gate, gate_far, up, up_far)):
+        joined[n * part : (n + 1) * part, :] = piece[0]
+    for n, piece in enumerate((down, down_far)):
+        joined_down[n * part : (n + 1) * part, :] = piece[0]
     x = rows[...].reshape(sources * slots, width)
-    along = (((1,), (1,)), ((), ()))
-    partial_value = jnp.zeros(x.shape, jnp.float32)
-    for g, u, d in ((gate, up, down), (gate_far, up_far, down_far)):
-        gate_values = lax.dot_general(x, g[0], along, preferred_element_type=jnp.float32)
-        up_values = lax.dot_general(x, u[0], along, preferred_element_type=jnp.float32)
-        active = gate_values / (1.0 + jnp.exp(-gate_values)) * up_values
-        partial_value = partial_value + jnp.dot(
-            active.astype(jnp.bfloat16), d[0], preferred_element_type=jnp.float32
-        )
+    values = lax.dot_general(
+        x, joined[...], (((1,), (1,)), ((), ())), preferred_element_type=jnp.float32
+    )
+    gate_values = values[:, : 2 * part]
+    active = gate_values / (1.0 + jnp.exp(-gate_values)) * values[:, 2 * part :]
+    partial_value = jnp.dot(
+        active.astype(jnp.bfloat16), joined_down[...], preferred_element_type=jnp.float32
+    )
     out[...] = partial_value.astype(jnp.bfloat16).reshape(rows.shape)
 
 
 def run_experts(rows, *weights):
     sources, experts, slots, width = rows.shape
-    block = pl.BlockSpec((sources // 2, 1, slots, width), lambda e, r: (r, e, 0, 0))
-    weight = pl.BlockSpec((1, *weights[0].shape[1:]), lambda e, r: (e, 0, 0))
+    part = weights[0].shape[1]
+    block = pl.BlockSpec((sources, 1, slots, width), lambda e: (0, e, 0, 0))
+    weight = pl.BlockSpec((1, part, width), lambda e: (e, 0, 0))
     return pl.pallas_call(
         expert_kernel,
-        grid=(experts, 2),
+        grid=(experts,),
         out_shape=jax.ShapeDtypeStruct(rows.shape, jnp.bfloat16),
         in_specs=[block] + [weight] * len(weights),
         out_specs=block,
+        scratch_shapes=[
+            pltpu.VMEM((4 * part, width), jnp.bfloat16),
+            pltpu.VMEM((2 * part, width), jnp.bfloat16),
+        ],
         name="run_experts",
     )(rows, *weights)
 
@@ -309,8 +330,9 @@
     second_bias,
 ):
     tp_size = lax.axis_size("tp")
+    core_lines = [list(range(core, tp_size, 2)) for core in range(2)]
     out_weights = lax.all_gather(
-        stacked(wide_out, narrow_out), "tp", axis=0, tiled=True
+        stacked(wide_out, narrow_out), "tp", axis=0, tiled=True, axis_index_groups=core_lines
     )
     rotated_queries, own_pack = prepare(
         wide_query.T,
@@ -327,8 +349,21 @@
     packs = [own_pack] + [turned_ring(own_pack, away) for away in range(1, SEQ_SHARDS)]
     earlier = attend(rotated_queries, packs[:2])
     mixed = attend(rotated_queries, packs[2:], earlier)
-    tokens = lax.all_to_all(mixed, "tp", split_axis=0, concat_axis=1, tiled=True)
-    projected = jnp.dot(tokens, out_weights, preferred_element_type=jnp.float32)
+    tokens = lax.all_to_all(
+        mixed, "tp", split_axis=0, concat_axis=0, tiled=True, axis_index_groups=core_lines
+    ).reshape(out_weights.shape[0], 128)
+    half = residual.shape[0]
+    core = lax.axis_index("tp") % 2
+    own_tokens = lax.dynamic_slice_in_dim(tokens, core * half, half, 1)
+    far_tokens = lax.dynamic_slice_in_dim(tokens, (1 - core) * half, half, 1)
+    heads_first = (((0,), (0,)), ((), ()))
+    far_part = lax.dot_general(
+        far_tokens, out_weights, heads_first, preferred_element_type=jnp.float32
+    )
+    own_part = lax.dot_general(
+        own_tokens, out_weights, heads_first, preferred_element_type=jnp.float32
+    )
+    projected = own_part + other_core(far_part)
     hidden = layer_norm(ALPHA * residual.astype(jnp.float32) + projected, first_gain, first_bias)
     device_rows = hidden.shape[0]
     model_width = hidden.shape[1]
@@ -356,7 +391,6 @@
     slab = jnp.transpose(arrived, (1, 2, 0, 3)).reshape(
         LOCAL_EXPERTS, capacity * sp_size, model_width
     )
-    core_lines = [list(range(core, tp_size, 2)) for core in range(2)]
     piece_rows = lax.all_gather(slab, "tp", axis=0, tiled=False, axis_index_groups=core_lines)
     gate_rows = jnp.transpose(expert_gate, (0, 2, 1))
     up_rows = jnp.transpose(expert_up, (0, 2, 1))
@@ -381,9 +415,8 @@
     shared_up_values = jnp.dot(hidden, shared_up, preferred_element_type=jnp.float32)
     shared_active = (jax.nn.silu(shared_gate_values) * shared_up_values).astype(jnp.bfloat16)
     shared_output = jnp.dot(shared_active, shared_down, preferred_element_type=jnp.float32)
-    return layer_norm(
-        ALPHA * hidden.astype(jnp.float32) + routed + shared_output, second_gain, second_bias
-    )
+    base = lax.optimization_barrier(ALPHA * hidden.astype(jnp.float32) + shared_output)
+    return layer_norm(base + routed, second_gain, second_bias)
 
 
 def solution(mesh):

time: 273 us -> 288 us (1.055)
  Pallas kernels: 42.8 us -> 58 us
    pallas_call x1, Pallas kernels: 1.95 us -> 17 us  [stacked(): pl.pallas_call(stack_kernel, out_shape=jax.ShapeDtypeStruct((2 * first.sh...]
    all_to_all x1, waiting for transfers between devices: 10.8 us -> 7.94 us  [local(): lax.all_to_all(jnp.transpose(summed, (2, 0, 1, 3)), 'sp', split_axis=0, c...]
    ppermute x3 -> x4, waiting for transfers between devices: 4.76 us -> 7.51 us  [other_core(): lax.ppermute(x, 'tp', [(i, i ^ 1) for i in range(lax.axis_size('tp'))])]
    dot_general x1 -> x2, matrix products: 5.06 us -> 6.36 us  [the longest x1 3.24 us: local(): lax.dot_general(own_tokens, out_weights, heads_first, preferred_element_t...]
  transfers between devices with their start and end apart: 11 -> 12, of which waited for: 9 -> 10; matrix products, arithmetic and copies ran while one was open for 1% -> 2% of each run, Pallas kernels for 10% -> 9%
where the time goes in v4:
time: 288 us; the launch traced here: 287 us
  waiting for transfers between devices  150 us (52%)
  Pallas kernels  58 us (20%)
  starting transfers between devices  26.3 us (9%)
  blocking collectives  18.3 us (6%)
  between operations  13.4 us (5%)
  matrix products  11.6 us (4%)
  local copies, waits for them, and re-layouts  7.36 us (3%)
    reduce_scatter x1, waiting for transfers between devices, local(): lax.psum_scatter(partial_value, 'tp', scatter_dimension=0, tiled=False, a...  64.1 us
    all_gather x1, waiting for transfers between devices, local(): lax.all_gather(slab, 'tp', axis=0, tiled=False, axis_index_groups=core_li...  51 us
    pallas_call x2, Pallas kernels, attend(): pl.pallas_call(functools.partial(attend_kernel, pieces=len(packs), resume...  22.5 us
    all_to_all x1, blocking collectives, local(): lax.all_to_all(outgoing, 'sp', split_axis=0, concat_axis=0, tiled=True)  18.3 us
    pallas_call x1, Pallas kernels, stacked(): pl.pallas_call(stack_kernel, out_shape=jax.ShapeDtypeStruct((2 * first.sh...  17 us
    pallas_call x1, Pallas kernels, run_experts(): pl.pallas_call(expert_kernel, grid=(experts,), out_shape=jax.ShapeDtypeSt...  14.4 us
    all_to_all x1, waiting for transfers between devices, local(): lax.all_to_all(mixed, 'tp', split_axis=0, concat_axis=0, tiled=True, axis...  14 us
    all_to_all x1, starting transfers between devices, local(): lax.all_to_all(mixed, 'tp', split_axis=0, concat_axis=0, tiled=True, axis...  10.3 us
  transfers between devices with their start and end apart: 12, of which 10 were waited for; matrix products, arithmetic and copies ran while one was open for 2% of the time, Pallas kernels for 9%

profile of v4, /device:TPU:1, one launch (start us, length us, event | category | flops | bytes accessed | tf_op | source)
XLA Modules:
  0.0 287.5 jit_solution(9325525518403122572)
XLA Ops:
  6.5 17.0 %stack_rows.1 = bf16[128,2048]{1,0:T(8,128)(2,1)} custom-call(bf16[64,2048]{1,0:T(8,128)(2,1)} %first.1, bf16[64,2048]{1,0:T(8,128)(2,1)} %second.1), custom_call_target="tpu_custom_call" | custom-call | tf_op jit(solution)/shard_map/stack_rows/pallas_call | solution.py:237
  23.6 4.1 %prepare_heads.1 = (bf16[128,3072]{1,0:T(8,128)(2,1)}, bf16[192,1024]{1,0:T(8,128)(2,1)}) custom-call(bf16[64,1024]{1,0:T(8,128)(2,1)} %bitcast.35, bf16[64,1024]{1,0:T(8,128)(2,1)} %bitcast.36, bf16[1024,256]{1,0:T(8,128)(2,1)} %wk.1, bf16[1024,256]{1,0:T(8,128)(2,1)} %nk.1, bf16[1024,256]{1,0:T(8,128)(2,1)} %wv.1, bf16[1024,256]{1,0:T(8,128)(2,1)} %nv.1, ...), custom_call_target="tpu_custom_call" | custom-call | tf_op jit(solution)/shard_map/prepare_heads/pallas_call | solution.py:96
  27.7 2.0 collective-permute-start.2
  29.7 2.5 collective-permute-start
  32.1 1.2 collective-permute-start.1
  33.3 4.5 %collective-permute-done.2.refs_2_ = bf16[192,1024]{1,0:T(8,128)(2,1)S(1)} collective-permute-done((bf16[192,1024]{1,0:T(8,128)(2,1)}, bf16[192,1024]{1,0:T(8,128)(2,1)S(1)}, u32[]{:S(2)}, u32[]{:S(2)}) %collective-permute-start.2) | collective-permute-done | bytes 393248 | tf_op jit(solution)/shard_map/ppermute | solution.py:291
  37.8 0.7 copy-done.5
  38.5 10.9 %attend_first.1 = (f32[12,112,256]{2,1,0:T(8,128)}, f32[12,8,256]{2,1,0:T(8,128)}) custom-call(bf16[128,3072]{1,0:T(8,128)(2,1)} %get-tuple-element.9.refs_0_, bf16[192,1024]{1,0:T(8,128)(2,1)} %get-tuple-element.10.refs_1_, bf16[192,1024]{1,0:T(8,128)(2,1)} %copy-done.5), custom_call_target="tpu_custom_call" | custom-call | tf_op jit(solution)/shard_map/attend_first/pallas_call | solution.py:211
  50.4 11.6 %attend_rest.1 = bf16[8,128,128]{2,1,0:T(8,128)(2,1)} custom-call(bf16[128,3072]{1,0:T(8,128)(2,1)} %get-tuple-element.9.refs_0_, bf16[192,1024]{1,0:T(8,128)(2,1)} %copy-done.3, bf16[192,1024]{1,0:T(8,128)(2,1)} %copy-done.4, f32[12,112,256]{2,1,0:T(8,128)} %get-tuple-element.11.refs_3_, f32[12,8,256]{2,1,0:T(8,128)} %get-tuple-element.12.refs_4_), custom_call_target="tpu_custom_call" | custom-call | tf_op jit(solution)/shard_map/attend_rest/pallas_call | solution.py:211
  61.9 10.3 %all-to-all-start = ((bf16[8,128,128]{2,1,0:T(8,128)(2,1)}), bf16[8,128,128]{2,1,0:T(8,128)(2,1)S(1)}, u32[]{:S(2)}, u32[]{:S(2)}) async-start(bf16[8,128,128]{2,1,0:T(8,128)(2,1)} %attend_rest.1), calls=%async_computation | async-start | bytes 524288 | tf_op jit(solution)/shard_map/all_to_all | solution.py:352
  72.6 14.0 %all-to-all-done = bf16[8,128,128]{2,1,0:T(8,128)(2,1)S(1)} async-done(((bf16[8,128,128]{2,1,0:T(8,128)(2,1)}), bf16[8,128,128]{2,1,0:T(8,128)(2,1)S(1)}, u32[]{:S(2)}, u32[]{:S(2)}) %all-to-all-start) | async-done | bytes 262176 | tf_op jit(solution)/shard_map/all_to_all | solution.py:352
  86.6 0.8 all-gather.3.cloned.1.call-done
  87.4 3.1 %fusion.2 = f32[64,2048]{1,0:T(8,128)S(1)} fusion(bf16[1024,2048]{1,0:T(8,128)(2,1)} %all-gather.3.cloned.1.call-done, bf16[1024,128]{1,0:T(8,128)(2,1)S(1)} %bitcast.28, s32[]{:T(128)S(6)} %select_n.15), kind=kOutput, calls=%fused_computation.12 | convolution fusion | flops 268435456 | bytes 4980740 | tf_op jit(solution)/shard_map/dot_general | solution.py:360
  90.5 1.7 collective-permute-start.3
  93.7 3.2 %fusion.16 = (f32[64]{0:T(128)S(1)}, f32[64,2048]{1,0:T(8,128)S(1)}) fusion(f32[64,2048]{1,0:T(8,128)S(1)} %collective-permute-done.3, bf16[1024,2048]{1,0:T(8,128)(2,1)} %all-gather.3.cloned.1.call-done, bf16[1024,128]{1,0:T(8,128)(2,1)S(1)} %bitcast.29, s32[]{:T(128)S(6)} %select_n.14, bf16[64,2048]{1,0:T(8,128)(2,1)S(1)} %copy-done.6), kind=kOutput, calls=%fused_computation.36 | convolution fusion | flops 269090752 | bytes 5767428 | tf_op jit(solution)/shard_map/dot_general | solution.py:363
  98.0 0.7 copy.62
  98.8 18.3 %all_to_all.15 = bf16[16,2,5,2048]{3,1,2,0:T(2,128)(2,1)S(1)} all-to-all(bf16[16,2,5,2048]{3,1,2,0:T(2,128)(2,1)S(1)} %copy.62), channel_id=1, replica_groups=mesh['sp'=16,'tp'=16] {'sp'}, dimensions={0} | all-to-all | bytes 1310720 | tf_op jit(solution)/shard_map/all_to_all | solution.py:390
  117.1 1.1 copy.63
  118.2 1.6 collective-permute-start.4
  120.3 2.7 collective-permute-done.4.gate_far
  123.0 2.4 collective-permute-done.5.up_far
  125.4 2.2 collective-permute-done.6.down_far
  127.7 51.0 %all-gather.5.cloned.1.call-done.rows = bf16[8,2,80,2048]{3,2,1,0:T(8,128)(2,1)} async-done(((bf16[1,2,80,2048]{3,2,1,0:T(8,128)(2,1)}), bf16[8,2,80,2048]{3,2,1,0:T(8,128)(2,1)}) %all-gather.5.cloned.1.call-update) | async-done | bytes 5242896 | tf_op jit(solution)/shard_map/all_gather | solution.py:394
  178.7 14.4 %run_experts.1 = bf16[8,2,80,2048]{3,2,1,0:T(8,128)(2,1)} custom-call(bf16[8,2,80,2048]{3,2,1,0:T(8,128)(2,1)} %all-gather.5.cloned.1.call-done.rows, bf16[2,192,2048]{2,1,0:T(8,128)(2,1)} %bitcast.31, bf16[2,192,2048]{2,1,0:T(8,128)(2,1)} %copy-done.1, bf16[2,192,2048]{2,1,0:T(8,128)(2,1)} %bitcast.33, bf16[2,192,2048]{2,1,0:T(8,128)(2,1)} %collective-permute-done.5.up_far, ...), custom_call_target="tpu_custom_call" | custom-call | tf_op jit(solution)/shard_map/run_experts/pallas_call | solution.py:271
  193.1 64.1 %reduce-scatter.2.cloned.1.call-done = bf16[1,2,80,2048]{3,2,1,0:T(8,128)(2,1)} async-done(((bf16[8,2,80,2048]{3,2,1,0:T(8,128)(2,1)}), bf16[1,2,80,2048]{3,2,1,0:T(8,128)(2,1)}) %reduce-scatter.2.cloned.1.call-update) | async-done | bytes 655376 | tf_op jit(solution)/shard_map/reduce_scatter | solution.py:406
  257.2 2.6 copy.67
  259.8 6.5 %all-to-all-start.2 = ((bf16[16,2,5,2048]{3,1,2,0:T(2,128)(2,1)}), bf16[16,2,5,2048]{3,1,2,0:T(2,128)(2,1)S(1)}, u32[]{:S(2)}, u32[]{:S(2)}) async-start(bf16[16,2,5,2048]{3,1,2,0:T(2,128)(2,1)} %bitcast.26), calls=%async_computation.3 | async-start | bytes 1310720 | tf_op jit(solution)/shard_map/all_to_all | solution.py:410
  266.4 2.1 fusion.18
  268.5 1.7 convolution_add_fusion
  270.2 7.9 %all-to-all-done.2 = bf16[16,2,5,2048]{3,1,2,0:T(2,128)(2,1)S(1)} async-done(((bf16[16,2,5,2048]{3,1,2,0:T(2,128)(2,1)}), bf16[16,2,5,2048]{3,1,2,0:T(2,128)(2,1)S(1)}, u32[]{:S(2)}, u32[]{:S(2)}) %all-to-all-start.2) | async-done | bytes 655392 | tf_op jit(solution)/shard_map/all_to_all | solution.py:410
  278.7 1.1 fusion.17
  280.1 0.9 add_convert_fusion
  (56 shorter events, 5.1 us)
Async XLA Ops:
  6.5 262.0 %copy-start = (bf16[256,2048]{1,0:T(8,128)(2,1)S(1)}, bf16[256,2048]{1,0:T(8,128)(2,1)}, u32[]{:S(2)}) copy-start(bf16[256,2048]{1,0:T(8,128)(2,1)} %param.47) | copy-start | bytes 3145732
  6.5 80.8 %all-gather.3.cloned.1.call-start = ((), (), s32[]{:S(2)}) async-start(), calls=%async_computation.4 | async-start | bytes 4718592 | tf_op jit(solution)/shard_map/all_gather | solution.py:334
  23.5 48.8 %copy-start.11 = (s32[64,2]{0,1:T(2,128)S(1)}, s32[64,2]{0,1:T(2,128)}, u32[]{:S(2)}) copy-start(s32[64,2]{0,1:T(2,128)} %param.40) | copy-start | bytes 1540
  27.7 10.1 %collective-permute-start.2 = (bf16[192,1024]{1,0:T(8,128)(2,1)}, bf16[192,1024]{1,0:T(8,128)(2,1)S(1)}, u32[]{:S(2)}, u32[]{:S(2)}) collective-permute-start(bf16[192,1024]{1,0:T(8,128)(2,1)} %get-tuple-element.10.refs_1_), channel_id=1, source_target_pairs={{0,16},{16,32},{32,48},{48,0},{64,80},{80,96},{96,112},{112,64},{1... | collective-permute-start | bytes 1179656 | tf_op jit(solution)/shard_map/ppermute | solution.py:291
  29.7 19.8 %collective-permute-start = (bf16[192,1024]{1,0:T(8,128)(2,1)}, bf16[192,1024]{1,0:T(8,128)(2,1)S(1)}, u32[]{:S(2)}, u32[]{:S(2)}) collective-permute-start(bf16[192,1024]{1,0:T(8,128)(2,1)} %get-tuple-element.10.refs_1_), channel_id=1, source_target_pairs={{0,32},{16,48},{32,0},{48,16},{64,96},{80,112},{96,64},{112,80},{1... | collective-permute-start | bytes 1179656 | tf_op jit(solution)/shard_map/ppermute | solution.py:291
  32.1 17.3 %collective-permute-start.1 = (bf16[192,1024]{1,0:T(8,128)(2,1)}, bf16[192,1024]{1,0:T(8,128)(2,1)S(1)}, u32[]{:S(2)}, u32[]{:S(2)}) collective-permute-start(bf16[192,1024]{1,0:T(8,128)(2,1)} %get-tuple-element.10.refs_1_), channel_id=1, source_target_pairs={{0,48},{16,0},{32,16},{48,32},{64,112},{80,64},{96,80},{112,96},{1... | collective-permute-start | bytes 1179656 | tf_op jit(solution)/shard_map/ppermute | solution.py:291
  37.8 0.7 copy-start.5
  49.5 0.7 copy-start.3
  49.5 0.9 copy-start.4
  50.4 42.5 %copy-start.12 = (f32[64,2]{0,1:T(2,128)S(1)}, f32[64,2]{0,1:T(2,128)}, u32[]{:S(2)}) copy-start(f32[64,2]{0,1:T(2,128)} %param.41) | copy-start | bytes 1540
  50.4 43.4 %copy-start.6 = (bf16[64,2048]{1,0:T(8,128)(2,1)S(1)}, bf16[64,2048]{1,0:T(8,128)(2,1)}, u32[]{:S(2)}) copy-start(bf16[64,2048]{1,0:T(8,128)(2,1)} %param.25) | copy-start | bytes 786436
  61.9 24.6 %all-to-all-start = ((bf16[8,128,128]{2,1,0:T(8,128)(2,1)}), bf16[8,128,128]{2,1,0:T(8,128)(2,1)S(1)}, u32[]{:S(2)}, u32[]{:S(2)}) async-start(bf16[8,128,128]{2,1,0:T(8,128)(2,1)} %attend_rest.1), calls=%async_computation | async-start | bytes 524288 | tf_op jit(solution)/shard_map/all_to_all | solution.py:352
  72.3 106.4 %all-gather.5.cloned.1.call-start = ((), (), s32[]{:S(2)}) async-start(), calls=%async_computation.5 | async-start | bytes 5898240 | tf_op jit(solution)/shard_map/all_gather | solution.py:394
  90.5 6.7 %copy-start.7 = (f32[2048]{0:T(1024)S(1)}, f32[2048]{0:T(1024)}, u32[]{:S(2)}) copy-start(f32[2048]{0:T(1024)} %param.39) | copy-start | bytes 24580
  90.5 6.7 %copy-start.8 = (f32[2048]{0:T(1024)S(1)}, f32[2048]{0:T(1024)}, u32[]{:S(2)}) copy-start(f32[2048]{0:T(1024)} %param.38) | copy-start | bytes 24580
  90.5 3.2 %collective-permute-start.3 = (f32[64,2048]{1,0:T(8,128)S(1)}, f32[64,2048]{1,0:T(8,128)S(1)}, u32[]{:S(2)}, u32[]{:S(2)}) collective-permute-start(f32[64,2048]{1,0:T(8,128)S(1)} %fusion.2), channel_id=1, source_target_pairs={{0,1},{1,0},{2,3},{3,2},{4,5},{5,4},{6,7},{7,6},{8,9},{9,8},{10,11... | collective-permute-start | bytes 1572872 | tf_op jit(solution)/shard_map/ppermute | solution.py:286
  118.2 139.1 %reduce-scatter.2.cloned.1.call-start = ((), (), s32[]{:S(2)}) async-start(), calls=%async_computation.6 | async-start | bytes 5898240 | tf_op jit(solution)/shard_map/reduce_scatter | solution.py:406
  118.2 4.8 %collective-permute-start.4 = (bf16[2,192,2048]{2,1,0:T(8,128)(2,1)}, bf16[2,192,2048]{2,1,0:T(8,128)(2,1)S(1)}, u32[]{:S(2)}, u32[]{:S(2)}) collective-permute-start(bf16[2,192,2048]{2,1,0:T(8,128)(2,1)} %bitcast.30), channel_id=1, source_target_pairs={{0,1},{1,0},{2,3},{3,2},{4,5},{5,4},{6,7},{7,6},{8,9},{9,8},{10,11... | collective-permute-start | bytes 4718600 | tf_op jit(solution)/shard_map/ppermute | solution.py:286
  119.8 5.6 %collective-permute-start.5 = (bf16[2,192,2048]{2,1,0:T(8,128)(2,1)}, bf16[2,192,2048]{2,1,0:T(8,128)(2,1)}, u32[]{:S(2)}, u32[]{:S(2)}) collective-permute-start(bf16[2,192,2048]{2,1,0:T(8,128)(2,1)} %bitcast.32), channel_id=1, source_target_pairs={{0,1},{1,0},{2,3},{3,2},{4,5},{5,4},{6,7},{7,6},{8,9},{9,8},{10,11... | collective-permute-start | bytes 4718600 | tf_op jit(solution)/shard_map/ppermute | solution.py:286
  119.9 7.8 %collective-permute-start.6 = (bf16[2,192,2048]{2,1,0:T(8,128)(2,1)}, bf16[2,192,2048]{2,1,0:T(8,128)(2,1)}, u32[]{:S(2)}, u32[]{:S(2)}) collective-permute-start(bf16[2,192,2048]{2,1,0:T(8,128)(2,1)} %down.1), channel_id=1, source_target_pairs={{0,1},{1,0},{2,3},{3,2},{4,5},{5,4},{6,7},{7,6},{8,9},{9,8},{10,11... | collective-permute-start | bytes 4718600 | tf_op jit(solution)/shard_map/ppermute | solution.py:286
  123.0 55.7 %copy-start.1 = (bf16[2,192,2048]{2,1,0:T(8,128)(2,1)}, bf16[2,192,2048]{2,1,0:T(8,128)(2,1)S(1)}, u32[]{:S(2)}) copy-start(bf16[2,192,2048]{2,1,0:T(8,128)(2,1)S(1)} %collective-permute-done.4.gate_far) | copy-start | bytes 4718596
  193.1 75.4 %copy-start.2 = (bf16[2048,256]{1,0:T(8,128)(2,1)S(1)}, bf16[2048,256]{1,0:T(8,128)(2,1)}, u32[]{:S(2)}) copy-start(bf16[2048,256]{1,0:T(8,128)(2,1)} %param.46) | copy-start | bytes 3145732
  259.8 18.3 %all-to-all-start.2 = ((bf16[16,2,5,2048]{3,1,2,0:T(2,128)(2,1)}), bf16[16,2,5,2048]{3,1,2,0:T(2,128)(2,1)S(1)}, u32[]{:S(2)}, u32[]{:S(2)}) async-start(bf16[16,2,5,2048]{3,1,2,0:T(2,128)(2,1)} %bitcast.26), calls=%async_computation.3 | async-start | bytes 1310720 | tf_op jit(solution)/shard_map/all_to_all | solution.py:410
  268.5 11.6 %copy-start.9 = (f32[2048]{0:T(1024)S(1)}, f32[2048]{0:T(1024)}, u32[]{:S(2)}) copy-start(f32[2048]{0:T(1024)} %param.49) | copy-start | bytes 24580
  268.5 11.6 %copy-start.10 = (f32[2048]{0:T(1024)S(1)}, f32[2048]{0:T(1024)}, u32[]{:S(2)}) copy-start(f32[2048]{0:T(1024)} %param.48) | copy-start | bytes 24580
Sparse Core Ops, SparseCore 0:
  23.7 63.6 all-gather.2
  118.3 60.3 all-gather.4
  193.3 63.9 reduce-scatter.1

commit v5 on v3

--- a/solution.py
+++ b/solution.py
@@ -232,33 +232,46 @@
     )(first, second)
 
 
-def expert_kernel(rows, gate, gate_far, up, up_far, down, down_far, out):
-    sources, _, slots, width = rows.shape
+def expert_kernel(*refs, expert):
+    rows, gate, gate_far, up, up_far, down, down_far = refs[:7]
+    out = refs[-1]
+    sources, _, slots, width = out.shape
     x = rows[...].reshape(sources * slots, width)
     along = (((1,), (1,)), ((), ()))
-    partial_value = jnp.zeros(x.shape, jnp.float32)
+    partial_value = jnp.zeros((sources * slots, width), jnp.float32)
+    if expert:
+        count = sources * slots
+        place = lax.broadcasted_iota(jnp.int32, (count, 1), 0)
+        source, slot, shard = place // slots, place % slots // 16, place % 16
+        wanted = shard * (count // 16) + source * (slots // 16) + slot
+        order = (wanted == lax.broadcasted_iota(jnp.int32, (count, count), 1)).astype(jnp.bfloat16)
     for g, u, d in ((gate, up, down), (gate_far, up_far, down_far)):
         gate_values = lax.dot_general(x, g[0], along, preferred_element_type=jnp.float32)
         up_values = lax.dot_general(x, u[0], along, preferred_element_type=jnp.float32)
         active = gate_values / (1.0 + jnp.exp(-gate_values)) * up_values
-        partial_value = partial_value + jnp.dot(
-            active.astype(jnp.bfloat16), d[0], preferred_element_type=jnp.float32
-        )
-    out[...] = partial_value.astype(jnp.bfloat16).reshape(rows.shape)
-
-
-def run_experts(rows, *weights):
-    sources, experts, slots, width = rows.shape
-    block = pl.BlockSpec((sources // 2, 1, slots, width), lambda e, r: (r, e, 0, 0))
-    weight = pl.BlockSpec((1, *weights[0].shape[1:]), lambda e, r: (e, 0, 0))
+        active = active.astype(jnp.bfloat16)
+        if expert:
+            active = jnp.dot(order, active, preferred_element_type=jnp.float32)
+            active = active.astype(jnp.bfloat16)
+        partial_value = partial_value + jnp.dot(active, d[0], preferred_element_type=jnp.float32)
+    out[...] = partial_value.astype(jnp.bfloat16).reshape(out.shape)
+
+
+def run_expert(expert, rows, weights, shape, written=None):
+    sources, _, slots, width = shape
+    whole = pl.BlockSpec(rows.shape, lambda i: (0, 0, 0))
+    weight = pl.BlockSpec((1, *weights[0].shape[1:]), lambda i: (expert, 0, 0))
+    block = pl.BlockSpec((sources, 1, slots, width), lambda i: (0, expert, 0, 0))
+    kept = [] if written is None else [written]
     return pl.pallas_call(
-        expert_kernel,
-        grid=(experts, 2),
-        out_shape=jax.ShapeDtypeStruct(rows.shape, jnp.bfloat16),
-        in_specs=[block] + [weight] * len(weights),
+        functools.partial(expert_kernel, expert=expert),
+        grid=(1,),
+        out_shape=jax.ShapeDtypeStruct(shape, jnp.bfloat16),
+        in_specs=[whole] + [weight] * 6 + [pl.BlockSpec(memory_space=pl.ANY)] * len(kept),
         out_specs=block,
-        name="run_experts",
-    )(rows, *weights)
+        input_output_aliases={7: 0} if kept else {},
+        name=f"run_expert_{expert}",
+    )(rows, *weights, *kept)
 
 
 def other_core(x):
@@ -347,21 +360,42 @@
     ).astype(jnp.float32)
     chosen = chosen.reshape(device_rows, top_count, experts * capacity)
     placing = jnp.sum(chosen, axis=1).astype(jnp.bfloat16)
+    placing = placing.reshape(device_rows, sp_size, LOCAL_EXPERTS, capacity)
+    placing = placing[:, :, 0].reshape(device_rows, sp_size * capacity)
+    line_place = lax.axis_index("tp") // 2
+    lines = tp_size // 2
+    slot_of = (flat_ids // 2 * lines + line_place) * capacity + earlier
+    target = jnp.where(flat_ids % 2 == 1, slot_of, -1).reshape(device_rows, top_count)
     mixing = jnp.sum(chosen * route_weights[:, :, None], axis=1)
+    core_lines = [list(range(core, tp_size, 2)) for core in range(2)]
+    line_hidden = lax.all_gather(hidden, "tp", axis=0, tiled=True, axis_index_groups=core_lines)
+    targets = lax.all_gather(
+        target.astype(jnp.float32), "tp", axis=0, tiled=True, axis_index_groups=core_lines
+    )
     outgoing = jnp.einsum("rs,rd->sd", placing, hidden, preferred_element_type=jnp.float32).astype(
         jnp.bfloat16
     )
-    outgoing = outgoing.reshape(sp_size, LOCAL_EXPERTS, capacity, model_width)
+    outgoing = outgoing.reshape(sp_size, capacity, model_width)
     arrived = lax.all_to_all(outgoing, "sp", split_axis=0, concat_axis=0, tiled=True)
-    slab = jnp.transpose(arrived, (1, 2, 0, 3)).reshape(
-        LOCAL_EXPERTS, capacity * sp_size, model_width
-    )
-    core_lines = [list(range(core, tp_size, 2)) for core in range(2)]
-    piece_rows = lax.all_gather(slab, "tp", axis=0, tiled=False, axis_index_groups=core_lines)
+    slab = jnp.transpose(arrived, (1, 0, 2)).reshape(capacity * sp_size, model_width)
+    first_rows = lax.all_gather(slab, "tp", axis=0, tiled=False, axis_index_groups=core_lines)
+    slots = sp_size * lines * capacity
+    picking = jnp.sum(
+        (targets[:, :, None] == jnp.arange(slots, dtype=jnp.float32)).astype(jnp.float32), axis=1
+    ).astype(jnp.bfloat16)
+    leaving = lax.dot_general(
+        picking, line_hidden, (((0,), (0,)), ((), ())), preferred_element_type=jnp.float32
+    ).astype(jnp.bfloat16)
+    second_rows = lax.all_to_all(
+        leaving.reshape(sp_size, lines * capacity, model_width),
+        "sp",
+        split_axis=0,
+        concat_axis=0,
+        tiled=True,
+    )
     gate_rows = jnp.transpose(expert_gate, (0, 2, 1))
     up_rows = jnp.transpose(expert_up, (0, 2, 1))
-    partial_value = run_experts(
-        piece_rows,
+    weights = (
         gate_rows,
         other_core(gate_rows),
         up_rows,
@@ -369,6 +403,9 @@
         expert_down,
         other_core(expert_down),
     )
+    shape = (lines, LOCAL_EXPERTS, capacity * sp_size, model_width)
+    partial_value = run_expert(0, first_rows, weights, shape)
+    partial_value = run_expert(1, second_rows, weights, shape, partial_value)
     summed = lax.psum_scatter(
         partial_value, "tp", scatter_dimension=0, tiled=False, axis_index_groups=core_lines
     )
@@ -381,9 +418,8 @@
     shared_up_values = jnp.dot(hidden, shared_up, preferred_element_type=jnp.float32)
     shared_active = (jax.nn.silu(shared_gate_values) * shared_up_values).astype(jnp.bfloat16)
     shared_output = jnp.dot(shared_active, shared_down, preferred_element_type=jnp.float32)
-    return layer_norm(
-        ALPHA * hidden.astype(jnp.float32) + routed + shared_output, second_gain, second_bias
-    )
+    base = lax.optimization_barrier(ALPHA * hidden.astype(jnp.float32) + shared_output)
+    return layer_norm(base + routed, second_gain, second_bias)
 
 
 def solution(mesh):

time: 273 us -> 277 us (1.015)
  waiting for transfers between devices: 149 us -> 106 us
  blocking collectives: 19 us -> 56 us
  matrix products: 9.2 us -> 15.4 us
  Pallas kernels: 42.8 us -> 48.1 us
    all_gather x1, waiting for transfers between devices: 51.2 us -> 19 us  [local(): lax.all_gather(slab, 'tp', axis=0, tiled=False, axis_index_groups=core_li...]
    all_to_all x0 -> x1, blocking collectives: none -> 26.5 us  [local(): lax.all_to_all(mixed, 'tp', split_axis=0, concat_axis=1, tiled=True)]
    all_to_all x1, waiting for transfers between devices: 13.1 us -> 0.01 us  [local(): lax.all_to_all(leaving.reshape(sp_size, lines * capacity, model_width), '...]
    all_gather x0 -> x1, blocking collectives: none -> 12.3 us  [local(): lax.all_gather(target.astype(jnp.float32), 'tp', axis=0, tiled=True, axis...]
    all_to_all x1, starting transfers between devices: 12 us -> 6.72 us  [local(): lax.all_to_all(leaving.reshape(sp_size, lines * capacity, model_width), '...]
    pallas_call x1 -> x2, Pallas kernels: 13.9 us -> 19.2 us  [run_expert(): pl.pallas_call(functools.partial(expert_kernel, expert=expert), grid=(1,)...]
    dot_general x0 -> x1, matrix products: none -> 4.71 us  [local(): lax.dot_general(picking, line_hidden, (((0,), (0,)), ((), ())), preferred...]
    ppermute x3, starting transfers between devices: 2.14 us -> 5.94 us  [other_core(): lax.ppermute(x, 'tp', [(i, i ^ 1) for i in range(lax.axis_size('tp'))])]
  transfers between devices with their start and end apart: 11 -> 12, of which waited for: 9 -> 9; matrix products, arithmetic and copies ran while one was open for 1% -> 4% of each run, Pallas kernels for 10% -> 13%
where the time goes in v5:
time: 277 us; the launch traced here: 276 us
  waiting for transfers between devices  106 us (38%)
  blocking collectives  56 us (20%)
  Pallas kernels  48.1 us (17%)
  starting transfers between devices  25 us (9%)
  matrix products  15.4 us (6%)
  between operations  13.4 us (5%)
  local copies, waits for them, and re-layouts  8.92 us (3%)
  other arithmetic  3.06 us (1%)
    reduce_scatter x1, waiting for transfers between devices, local(): lax.psum_scatter(partial_value, 'tp', scatter_dimension=0, tiled=False, a...  67 us
    all_to_all x1, blocking collectives, local(): lax.all_to_all(mixed, 'tp', split_axis=0, concat_axis=1, tiled=True)  26.5 us
    pallas_call x2, Pallas kernels, attend(): pl.pallas_call(functools.partial(attend_kernel, pieces=len(packs), resume...  23 us
    pallas_call x2, Pallas kernels, run_expert(): pl.pallas_call(functools.partial(expert_kernel, expert=expert), grid=(1,)...  19.2 us
    all_gather x1, waiting for transfers between devices, local(): lax.all_gather(slab, 'tp', axis=0, tiled=False, axis_index_groups=core_li...  19 us
    all_to_all x1, blocking collectives, local(): lax.all_to_all(outgoing, 'sp', split_axis=0, concat_axis=0, tiled=True)  17.2 us
    all_gather x1, blocking collectives, local(): lax.all_gather(target.astype(jnp.float32), 'tp', axis=0, tiled=True, axis...  12.3 us
    all_to_all x1, waiting for transfers between devices, local(): lax.all_to_all(jnp.transpose(summed, (2, 0, 1, 3)), 'sp', split_axis=0, c...  8.61 us
  transfers between devices with their start and end apart: 12, of which 9 were waited for; matrix products, arithmetic and copies ran while one was open for 4% of the time, Pallas kernels for 13%

profile of v5, /device:TPU:1, one launch (start us, length us, event | category | flops | bytes accessed | tf_op | source)
XLA Modules:
  0.0 276.4 jit_solution(17913375245892256689)
XLA Ops:
  6.5 1.9 stack_rows.1
  8.6 4.1 %prepare_heads.1 = (bf16[128,3072]{1,0:T(8,128)(2,1)}, bf16[192,1024]{1,0:T(8,128)(2,1)}) custom-call(bf16[64,1024]{1,0:T(8,128)(2,1)} %bitcast.57, bf16[64,1024]{1,0:T(8,128)(2,1)} %bitcast.58, bf16[1024,256]{1,0:T(8,128)(2,1)} %wk.1, bf16[1024,256]{1,0:T(8,128)(2,1)} %nk.1, bf16[1024,256]{1,0:T(8,128)(2,1)} %wv.1, bf16[1024,256]{1,0:T(8,128)(2,1)} %nv.1, ...), custom_call_target="tpu_custom_call" | custom-call | tf_op jit(solution)/shard_map/prepare_heads/pallas_call | solution.py:96
  12.6 2.0 collective-permute-start.2
  14.6 2.5 collective-permute-start
  17.1 1.2 collective-permute-start.1
  18.2 4.5 %collective-permute-done.2.refs_2_ = bf16[192,1024]{1,0:T(8,128)(2,1)S(1)} collective-permute-done((bf16[192,1024]{1,0:T(8,128)(2,1)}, bf16[192,1024]{1,0:T(8,128)(2,1)S(1)}, u32[]{:S(2)}, u32[]{:S(2)}) %collective-permute-start.2) | collective-permute-done | bytes 393248 | tf_op jit(solution)/shard_map/ppermute | solution.py:283
  23.5 11.3 %attend_first.1 = (f32[12,112,256]{2,1,0:T(8,128)}, f32[12,8,256]{2,1,0:T(8,128)}) custom-call(bf16[128,3072]{1,0:T(8,128)(2,1)} %get-tuple-element.9.refs_0_, bf16[192,1024]{1,0:T(8,128)(2,1)} %get-tuple-element.10.refs_1_, bf16[192,1024]{1,0:T(8,128)(2,1)} %copy-done.8), custom_call_target="tpu_custom_call" | custom-call | tf_op jit(solution)/shard_map/attend_first/pallas_call | solution.py:209
  35.7 11.7 %attend_rest.1 = bf16[1024,128]{1,0:T(8,128)(2,1)} custom-call(bf16[128,3072]{1,0:T(8,128)(2,1)} %get-tuple-element.9.refs_0_, bf16[192,1024]{1,0:T(8,128)(2,1)} %copy-done.6, bf16[192,1024]{1,0:T(8,128)(2,1)} %copy-done.7, f32[12,112,256]{2,1,0:T(8,128)} %get-tuple-element.11.refs_3_, f32[12,8,256]{2,1,0:T(8,128)} %get-tuple-element.12.refs_4_), custom_call_target="tpu_custom_call" | custom-call | tf_op jit(solution)/shard_map/attend_rest/pallas_call | solution.py:209
  47.4 26.5 %all_to_all.34 = bf16[16,64,128]{2,1,0:T(8,128)(2,1)S(1)} all-to-all(bf16[16,64,128]{2,1,0:T(8,128)(2,1)} %bitcast.55), channel_id=1, replica_groups=mesh['sp'=16,'tp'=16] {'tp'}, dimensions={0} | all-to-all | bytes 524288 | tf_op jit(solution)/shard_map/all_to_all | solution.py:343
  74.6 5.1 %fusion.12 = (f32[64]{0:T(128)S(1)}, f32[64,2048]{1,0:T(8,128)S(1)}) fusion(bf16[2048,2048]{1,0:T(8,128)(2,1)} %all-gather.5.cloned.1.call-done, bf16[64,2048]{1,0:T(8,128)(2,1)S(1)} %copy-done.9, bf16[16,64,128]{2,1,0:T(8,128)(2,1)S(1)} %all_to_all.34), kind=kOutput, calls=%fused_computation.42 | convolution fusion | flops 537395136 | bytes 9437440 | tf_op jit(solution)/shard_map/dot_general | solution.py:344
  82.1 1.2 convolution_convert_fusion.1
  83.4 17.2 %all_to_all.35 = bf16[16,5,2048]{2,1,0:T(8,128)(2,1)S(1)} all-to-all(bf16[16,5,2048]{2,1,0:T(8,128)(2,1)S(1)} %reshape.83), channel_id=1, replica_groups=mesh['sp'=16,'tp'=16] {'sp'}, dimensions={0} | all-to-all | bytes 655360 | tf_op jit(solution)/shard_map/all_to_all | solution.py:379
  101.6 12.3 %all-gather = f32[8,64,2]{1,2,0:T(2,128)S(1)} all-gather(f32[1,64,2]{1,2,0:T(2,128)S(1)} %get-tuple-element.15), channel_id=1, replica_groups={{0,2,4,6,8,10,12,14},{1,3,5,7,9,11,13,15},{16,18,20,22,24,26,28,30},{17..., dimensions={0}, use_global_device_ids=true | all-gather | bytes 4608 | tf_op jit(solution)/shard_map/all_gather | solution.py:372
  114.3 1.7 all-gather.7.cloned.1.call-done
  116.0 4.7 %convolution_convert_fusion = bf16[640,2048]{1,0:T(8,128)(2,1)} fusion(bf16[512,2048]{1,0:T(8,128)(2,1)} %all-gather.7.cloned.1.call-done, bf16[512,640]{1,0:T(8,128)(2,1)S(1)} %convert_reduce_fusion), kind=kOutput, calls=%fused_computation | convolution fusion | flops 1343488000 | bytes 5373952 | tf_op jit(solution)/shard_map/dot_general | solution.py:386
  120.7 6.7 %all-to-all-start.1 = ((bf16[16,40,2048]{2,1,0:T(8,128)(2,1)}), bf16[16,40,2048]{2,1,0:T(8,128)(2,1)}, u32[]{:S(2)}, u32[]{:S(2)}) async-start(bf16[16,40,2048]{2,1,0:T(8,128)(2,1)} %bitcast.52), calls=%async_computation.1 | async-start | bytes 5242880 | tf_op jit(solution)/shard_map/all_to_all | solution.py:389
  127.5 5.4 %collective-permute-start.3 = (bf16[2,192,2048]{2,1,0:T(8,128)(2,1)S(1)}, bf16[2,192,2048]{2,1,0:T(8,128)(2,1)S(1)}, u32[]{:S(2)}, u32[]{:S(2)}) collective-permute-start(bf16[2,192,2048]{2,1,0:T(8,128)(2,1)S(1)} %bitcast.48), channel_id=1, source_target_pairs={{0,1},{1,0},{2,3},{3,2},{4,5},{5,4},{6,7},{7,6},{8,9},{9,8},{10,11... | collective-permute-start | bytes 4718600 | tf_op jit(solution)/shard_map/ppermute | solution.py:278
  133.4 2.5 collective-permute-done.3.refs_2_
  136.0 1.2 copy-done.3
  137.1 1.1 collective-permute-done.4.refs_4_
  138.2 1.2 copy-done.4
  139.4 1.2 collective-permute-done.5.refs_6_
  140.6 19.0 %all-gather.9.cloned.1.call-done.refs_0_ = bf16[8,80,2048]{2,1,0:T(8,128)(2,1)} async-done(((bf16[1,80,2048]{2,1,0:T(8,128)(2,1)}), bf16[8,80,2048]{2,1,0:T(8,128)(2,1)}) %all-gather.9.cloned.1.call-update) | async-done | bytes 2621456 | tf_op jit(solution)/shard_map/all_gather | solution.py:381
  159.6 8.9 %run_expert_0.1.refs_7_ = bf16[8,2,80,2048]{3,2,1,0:T(8,128)(2,1)} custom-call(bf16[8,80,2048]{2,1,0:T(8,128)(2,1)} %all-gather.9.cloned.1.call-done.refs_0_, bf16[2,192,2048]{2,1,0:T(8,128)(2,1)} %bitcast.46, bf16[2,192,2048]{2,1,0:T(8,128)(2,1)} %copy-done.3, bf16[2,192,2048]{2,1,0:T(8,128)(2,1)} %bitcast.50, bf16[2,192,2048]{2,1,0:T(8,128)(2,1)} %copy-done.4, ...), custom_call_target="tpu_custom_call" | custom-call | tf_op jit(solution)/shard_map/run_expert_0/pallas_call | solution.py:266
  168.5 10.3 %run_expert_1.1 = bf16[8,2,80,2048]{3,2,1,0:T(8,128)(2,1)} custom-call(bf16[16,40,2048]{2,1,0:T(8,128)(2,1)} %all-to-all-done.1.refs_0_, bf16[2,192,2048]{2,1,0:T(8,128)(2,1)} %bitcast.47, bf16[2,192,2048]{2,1,0:T(8,128)(2,1)} %copy-done.3, bf16[2,192,2048]{2,1,0:T(8,128)(2,1)} %bitcast.51, ...), custom_call_target="tpu_custom_call", output_to_operand_aliasing={{}: (7, {})} | custom-call | tf_op jit(solution)/shard_map/run_expert_1/pallas_call | solution.py:266
  178.9 67.0 %reduce-scatter.2.cloned.1.call-done = bf16[1,2,80,2048]{3,2,1,0:T(8,128)(2,1)} async-done(((bf16[8,2,80,2048]{3,2,1,0:T(8,128)(2,1)}), bf16[1,2,80,2048]{3,2,1,0:T(8,128)(2,1)}) %reduce-scatter.2.cloned.1.call-update) | async-done | bytes 655376 | tf_op jit(solution)/shard_map/reduce_scatter | solution.py:409
  245.9 2.6 copy.127
  248.5 6.5 %all-to-all-start.3 = ((bf16[16,2,5,2048]{3,1,2,0:T(2,128)(2,1)}), bf16[16,2,5,2048]{3,1,2,0:T(2,128)(2,1)S(1)}, u32[]{:S(2)}, u32[]{:S(2)}) async-start(bf16[16,2,5,2048]{3,1,2,0:T(2,128)(2,1)} %bitcast.45), calls=%async_computation.4 | async-start | bytes 1310720 | tf_op jit(solution)/shard_map/all_to_all | solution.py:413
  255.0 1.5 fusion.14
  256.6 1.6 convolution_add_fusion
  258.2 8.6 %all-to-all-done.3 = bf16[16,2,5,2048]{3,1,2,0:T(2,128)(2,1)S(1)} async-done(((bf16[16,2,5,2048]{3,1,2,0:T(2,128)(2,1)}), bf16[16,2,5,2048]{3,1,2,0:T(2,128)(2,1)S(1)}, u32[]{:S(2)}, u32[]{:S(2)}) %all-to-all-start.3) | async-done | bytes 655392 | tf_op jit(solution)/shard_map/all_to_all | solution.py:413
  267.4 1.4 fusion.13
  (72 shorter events, 8.5 us)
Async XLA Ops:
  6.5 250.0 %copy-start = (bf16[256,2048]{1,0:T(8,128)(2,1)S(1)}, bf16[256,2048]{1,0:T(8,128)(2,1)}, u32[]{:S(2)}) copy-start(bf16[256,2048]{1,0:T(8,128)(2,1)} %param.47) | copy-start | bytes 3145732
  6.5 68.1 %all-gather.5.cloned.1.call-start = ((), (), s32[]{:S(2)}) async-start(), calls=%async_computation.5 | async-start | bytes 8912896 | tf_op jit(solution)/shard_map/all_gather | solution.py:325
  8.5 107.5 %all-gather.7.cloned.1.call-start = ((), (), s32[]{:S(2)}) async-start(), calls=%async_computation.6 | async-start | bytes 2359296 | tf_op jit(solution)/shard_map/all_gather | solution.py:371
  12.6 10.1 %collective-permute-start.2 = (bf16[192,1024]{1,0:T(8,128)(2,1)}, bf16[192,1024]{1,0:T(8,128)(2,1)S(1)}, u32[]{:S(2)}, u32[]{:S(2)}) collective-permute-start(bf16[192,1024]{1,0:T(8,128)(2,1)} %get-tuple-element.10.refs_1_), channel_id=1, source_target_pairs={{0,16},{16,32},{32,48},{48,0},{64,80},{80,96},{96,112},{112,64},{1... | collective-permute-start | bytes 1179656 | tf_op jit(solution)/shard_map/ppermute | solution.py:283
  14.6 20.2 %collective-permute-start = (bf16[192,1024]{1,0:T(8,128)(2,1)}, bf16[192,1024]{1,0:T(8,128)(2,1)S(1)}, u32[]{:S(2)}, u32[]{:S(2)}) collective-permute-start(bf16[192,1024]{1,0:T(8,128)(2,1)} %get-tuple-element.10.refs_1_), channel_id=1, source_target_pairs={{0,32},{16,48},{32,0},{48,16},{64,96},{80,112},{96,64},{112,80},{1... | collective-permute-start | bytes 1179656 | tf_op jit(solution)/shard_map/ppermute | solution.py:283
  17.1 17.7 %collective-permute-start.1 = (bf16[192,1024]{1,0:T(8,128)(2,1)}, bf16[192,1024]{1,0:T(8,128)(2,1)S(1)}, u32[]{:S(2)}, u32[]{:S(2)}) collective-permute-start(bf16[192,1024]{1,0:T(8,128)(2,1)} %get-tuple-element.10.refs_1_), channel_id=1, source_target_pairs={{0,48},{16,0},{32,16},{48,32},{64,112},{80,64},{96,80},{112,96},{1... | collective-permute-start | bytes 1179656 | tf_op jit(solution)/shard_map/ppermute | solution.py:283
  22.8 0.7 copy-start.8
  23.5 51.1 %copy-start.9 = (bf16[64,2048]{1,0:T(8,128)(2,1)S(1)}, bf16[64,2048]{1,0:T(8,128)(2,1)}, u32[]{:S(2)}) copy-start(bf16[64,2048]{1,0:T(8,128)(2,1)} %param.25) | copy-start | bytes 786436
  34.8 0.7 copy-start.6
  34.8 0.9 copy-start.7
  73.9 6.0 %copy-start.10 = (f32[2048]{0:T(1024)S(1)}, f32[2048]{0:T(1024)}, u32[]{:S(2)}) copy-start(f32[2048]{0:T(1024)} %param.39) | copy-start | bytes 24580
  73.9 6.0 %copy-start.11 = (f32[2048]{0:T(1024)S(1)}, f32[2048]{0:T(1024)}, u32[]{:S(2)}) copy-start(f32[2048]{0:T(1024)} %param.38) | copy-start | bytes 24580
  73.9 7.0 %copy-start.14 = (s32[64,2]{0,1:T(2,128)S(1)}, s32[64,2]{0,1:T(2,128)}, u32[]{:S(2)}) copy-start(s32[64,2]{0,1:T(2,128)} %param.40) | copy-start | bytes 1540
  73.9 7.9 %copy-start.15 = (f32[64,2]{0,1:T(2,128)S(1)}, f32[64,2]{0,1:T(2,128)}, u32[]{:S(2)}) copy-start(f32[64,2]{0,1:T(2,128)} %param.41) | copy-start | bytes 1540
  80.8 78.8 %all-gather.9.cloned.1.call-start = ((), (), s32[]{:S(2)}) async-start(), calls=%async_computation.7 | async-start | bytes 2949120 | tf_op jit(solution)/shard_map/all_gather | solution.py:381
  120.7 6.8 %copy-start.2 = (bf16[2,2048,192]{1,2,0:T(8,128)(2,1)S(1)}, bf16[2,2048,192]{1,2,0:T(8,128)(2,1)}, u32[]{:S(2)}) copy-start(bf16[2,2048,192]{1,2,0:T(8,128)(2,1)} %param.42) | copy-start | bytes 4718596
  120.7 47.8 %all-to-all-start.1 = ((bf16[16,40,2048]{2,1,0:T(8,128)(2,1)}), bf16[16,40,2048]{2,1,0:T(8,128)(2,1)}, u32[]{:S(2)}, u32[]{:S(2)}) async-start(bf16[16,40,2048]{2,1,0:T(8,128)(2,1)} %bitcast.52), calls=%async_computation.1 | async-start | bytes 5242880 | tf_op jit(solution)/shard_map/all_to_all | solution.py:389
  127.4 118.4 %reduce-scatter.2.cloned.1.call-start = ((), (), s32[]{:S(2)}) async-start(), calls=%async_computation.8 | async-start | bytes 5898240 | tf_op jit(solution)/shard_map/reduce_scatter | solution.py:409
  127.5 8.5 %collective-permute-start.3 = (bf16[2,192,2048]{2,1,0:T(8,128)(2,1)S(1)}, bf16[2,192,2048]{2,1,0:T(8,128)(2,1)S(1)}, u32[]{:S(2)}, u32[]{:S(2)}) collective-permute-start(bf16[2,192,2048]{2,1,0:T(8,128)(2,1)S(1)} %bitcast.48), channel_id=1, source_target_pairs={{0,1},{1,0},{2,3},{3,2},{4,5},{5,4},{6,7},{7,6},{8,9},{9,8},{10,11... | collective-permute-start | bytes 4718600 | tf_op jit(solution)/shard_map/ppermute | solution.py:278
  132.9 5.3 %collective-permute-start.4 = (bf16[2,192,2048]{2,1,0:T(8,128)(2,1)}, bf16[2,192,2048]{2,1,0:T(8,128)(2,1)S(1)}, u32[]{:S(2)}, u32[]{:S(2)}) collective-permute-start(bf16[2,192,2048]{2,1,0:T(8,128)(2,1)} %bitcast.49), channel_id=1, source_target_pairs={{0,1},{1,0},{2,3},{3,2},{4,5},{5,4},{6,7},{7,6},{8,9},{9,8},{10,11... | collective-permute-start | bytes 4718600 | tf_op jit(solution)/shard_map/ppermute | solution.py:278
  133.0 7.6 %collective-permute-start.5 = (bf16[2,192,2048]{2,1,0:T(8,128)(2,1)}, bf16[2,192,2048]{2,1,0:T(8,128)(2,1)}, u32[]{:S(2)}, u32[]{:S(2)}) collective-permute-start(bf16[2,192,2048]{2,1,0:T(8,128)(2,1)} %refs_5_.3), channel_id=1, source_target_pairs={{0,1},{1,0},{2,3},{3,2},{4,5},{5,4},{6,7},{7,6},{8,9},{9,8},{10,11... | collective-permute-start | bytes 4718600 | tf_op jit(solution)/shard_map/ppermute | solution.py:278
  136.0 1.2 copy-start.3
  138.2 1.2 copy-start.4
  178.8 76.2 %copy-start.1 = (bf16[64,2048]{1,0:T(8,128)(2,1)S(1)}, bf16[64,2048]{1,0:T(8,128)(2,1)}, u32[]{:S(2)}) copy-start(bf16[64,2048]{1,0:T(8,128)(2,1)} %add_convert_fusion.1) | copy-start | bytes 786436
  178.8 77.7 %copy-start.5 = (bf16[2048,256]{1,0:T(8,128)(2,1)S(1)}, bf16[2048,256]{1,0:T(8,128)(2,1)}, u32[]{:S(2)}) copy-start(bf16[2048,256]{1,0:T(8,128)(2,1)} %param.46) | copy-start | bytes 3145732
  248.5 18.3 %all-to-all-start.3 = ((bf16[16,2,5,2048]{3,1,2,0:T(2,128)(2,1)}), bf16[16,2,5,2048]{3,1,2,0:T(2,128)(2,1)S(1)}, u32[]{:S(2)}, u32[]{:S(2)}) async-start(bf16[16,2,5,2048]{3,1,2,0:T(2,128)(2,1)} %bitcast.45), calls=%async_computation.4 | async-start | bytes 1310720 | tf_op jit(solution)/shard_map/all_to_all | solution.py:413
  258.2 10.8 %copy-start.12 = (f32[2048]{0:T(1024)S(1)}, f32[2048]{0:T(1024)}, u32[]{:S(2)}) copy-start(f32[2048]{0:T(1024)} %param.49) | copy-start | bytes 24580
  258.2 10.8 %copy-start.13 = (f32[2048]{0:T(1024)S(1)}, f32[2048]{0:T(1024)}, u32[]{:S(2)}) copy-start(f32[2048]{0:T(1024)} %param.48) | copy-start | bytes 24580
Sparse Core Ops, SparseCore 0:
  9.2 65.3 all-gather.4
  80.9 35.0 all-gather.6
  117.8 41.8 all-gather.8
  179.0 66.8 reduce-scatter.1

commit v6 on v3

--- a/solution.py
+++ b/solution.py
@@ -381,9 +381,8 @@
     shared_up_values = jnp.dot(hidden, shared_up, preferred_element_type=jnp.float32)
     shared_active = (jax.nn.silu(shared_gate_values) * shared_up_values).astype(jnp.bfloat16)
     shared_output = jnp.dot(shared_active, shared_down, preferred_element_type=jnp.float32)
-    return layer_norm(
-        ALPHA * hidden.astype(jnp.float32) + routed + shared_output, second_gain, second_bias
-    )
+    base = lax.optimization_barrier(ALPHA * hidden.astype(jnp.float32) + shared_output)
+    return layer_norm(base + routed, second_gain, second_bias)
 
 
 def solution(mesh):

time: 273 us -> 270 us (0.989)
  waiting for transfers between devices: 149 us -> 146 us
    all_to_all x1, waiting for transfers between devices: 10.8 us -> 7.96 us  [local(): lax.all_to_all(jnp.transpose(summed, (2, 0, 1, 3)), 'sp', split_axis=0, c...]
  transfers between devices with their start and end apart: 11 -> 11, of which waited for: 9 -> 9; matrix products, arithmetic and copies ran while one was open for 1% -> 2% of each run, Pallas kernels for 10% -> 10%
where the time goes in v6:
time: 270 us
  waiting for transfers between devices  146 us (54%)
  Pallas kernels  42.8 us (16%)
  starting transfers between devices  26.5 us (10%)
  blocking collectives  19 us (7%)
  between operations  13.3 us (5%)
  local copies, waits for them, and re-layouts  9.74 us (4%)
  matrix products  9.55 us (4%)
    reduce_scatter x1, waiting for transfers between devices, local(): lax.psum_scatter(partial_value, 'tp', scatter_dimension=0, tiled=False, a...  64.1 us
    all_gather x1, waiting for transfers between devices, local(): lax.all_gather(slab, 'tp', axis=0, tiled=False, axis_index_groups=core_li...  51.2 us
    pallas_call x2, Pallas kernels, attend(): pl.pallas_call(functools.partial(attend_kernel, pieces=len(packs), resume...  22.9 us
    all_to_all x1, blocking collectives, local(): lax.all_to_all(outgoing, 'sp', split_axis=0, concat_axis=0, tiled=True)  19 us
    pallas_call x1, Pallas kernels, run_experts(): pl.pallas_call(expert_kernel, grid=(experts, 2), out_shape=jax.ShapeDtype...  13.9 us
    all_to_all x1, waiting for transfers between devices, local(): lax.all_to_all(mixed, 'tp', split_axis=0, concat_axis=1, tiled=True)  13.1 us
    all_to_all x1, starting transfers between devices, local(): lax.all_to_all(mixed, 'tp', split_axis=0, concat_axis=1, tiled=True)  12 us
    all_to_all x1, waiting for transfers between devices, local(): lax.all_to_all(jnp.transpose(summed, (2, 0, 1, 3)), 'sp', split_axis=0, c...  7.96 us
  transfers between devices with their start and end apart: 11, of which 9 were waited for; matrix products, arithmetic and copies ran while one was open for 2% of the time, Pallas kernels for 10%

profile of v6, /device:TPU:1, one launch (start us, length us, event | category | flops | bytes accessed | tf_op | source)
XLA Modules:
  0.0 269.8 jit_solution(5368447197573805697)
XLA Ops:
  6.5 2.0 stack_rows.1
  8.5 4.0 %prepare_heads.1 = (bf16[128,3072]{1,0:T(8,128)(2,1)}, bf16[192,1024]{1,0:T(8,128)(2,1)}) custom-call(bf16[64,1024]{1,0:T(8,128)(2,1)} %bitcast.43, bf16[64,1024]{1,0:T(8,128)(2,1)} %bitcast.44, bf16[1024,256]{1,0:T(8,128)(2,1)} %wk.1, bf16[1024,256]{1,0:T(8,128)(2,1)} %nk.1, bf16[1024,256]{1,0:T(8,128)(2,1)} %wv.1, bf16[1024,256]{1,0:T(8,128)(2,1)} %nv.1, ...), custom_call_target="tpu_custom_call" | custom-call | tf_op jit(solution)/shard_map/prepare_heads/pallas_call | solution.py:96
  12.6 2.0 collective-permute-start.2
  14.6 2.5 collective-permute-start
  17.0 1.2 collective-permute-start.1
  18.4 4.3 %collective-permute-done.2.refs_2_ = bf16[192,1024]{1,0:T(8,128)(2,1)S(1)} collective-permute-done((bf16[192,1024]{1,0:T(8,128)(2,1)}, bf16[192,1024]{1,0:T(8,128)(2,1)S(1)}, u32[]{:S(2)}, u32[]{:S(2)}) %collective-permute-start.2) | collective-permute-done | bytes 393248 | tf_op jit(solution)/shard_map/ppermute | solution.py:270
  22.7 0.7 copy-done.7
  23.4 11.2 %attend_first.1 = (f32[12,112,256]{2,1,0:T(8,128)}, f32[12,8,256]{2,1,0:T(8,128)}) custom-call(bf16[128,3072]{1,0:T(8,128)(2,1)} %get-tuple-element.9.refs_0_, bf16[192,1024]{1,0:T(8,128)(2,1)} %get-tuple-element.10.refs_1_, bf16[192,1024]{1,0:T(8,128)(2,1)} %copy-done.7), custom_call_target="tpu_custom_call" | custom-call | tf_op jit(solution)/shard_map/attend_first/pallas_call | solution.py:209
  35.5 11.7 %attend_rest.1 = bf16[1024,128]{1,0:T(8,128)(2,1)} custom-call(bf16[128,3072]{1,0:T(8,128)(2,1)} %get-tuple-element.9.refs_0_, bf16[192,1024]{1,0:T(8,128)(2,1)} %copy-done.5, bf16[192,1024]{1,0:T(8,128)(2,1)} %copy-done.6, f32[12,112,256]{2,1,0:T(8,128)} %get-tuple-element.11.refs_3_, f32[12,8,256]{2,1,0:T(8,128)} %get-tuple-element.12.refs_4_), custom_call_target="tpu_custom_call" | custom-call | tf_op jit(solution)/shard_map/attend_rest/pallas_call | solution.py:209
  47.2 12.0 %all-to-all-start = ((bf16[16,64,128]{2,1,0:T(8,128)(2,1)}), bf16[16,64,128]{2,1,0:T(8,128)(2,1)S(1)}, u32[]{:S(2)}, u32[]{:S(2)}) async-start(bf16[16,64,128]{2,1,0:T(8,128)(2,1)} %bitcast.41), calls=%async_computation | async-start | bytes 524288 | tf_op jit(solution)/shard_map/all_to_all | solution.py:330
  59.9 0.7 convert_reduce_fusion
  60.6 13.1 %all-to-all-done = bf16[16,64,128]{2,1,0:T(8,128)(2,1)S(1)} async-done(((bf16[16,64,128]{2,1,0:T(8,128)(2,1)}), bf16[16,64,128]{2,1,0:T(8,128)(2,1)S(1)}, u32[]{:S(2)}, u32[]{:S(2)}) %all-to-all-start) | async-done | bytes 262176 | tf_op jit(solution)/shard_map/all_to_all | solution.py:330
  73.8 0.8 all-gather.3.cloned.1.call-done
  74.6 5.1 %fusion.12 = (f32[64]{0:T(128)S(1)}, f32[64,2048]{1,0:T(8,128)S(1)}) fusion(bf16[2048,2048]{1,0:T(8,128)(2,1)} %all-gather.3.cloned.1.call-done, bf16[64,2048]{1,0:T(8,128)(2,1)S(1)} %copy-done.8, bf16[16,64,128]{2,1,0:T(8,128)(2,1)S(1)} %all-to-all-done), kind=kOutput, calls=%fused_computation.32 | convolution fusion | flops 537395136 | bytes 9437440 | tf_op jit(solution)/shard_map/dot_general | solution.py:331
  80.7 0.7 copy.67
  81.5 19.0 %all_to_all.29 = bf16[16,2,5,2048]{3,1,2,0:T(2,128)(2,1)S(1)} all-to-all(bf16[16,2,5,2048]{3,1,2,0:T(2,128)(2,1)S(1)} %copy.67), channel_id=1, replica_groups=mesh['sp'=16,'tp'=16] {'sp'}, dimensions={0} | all-to-all | bytes 1310720 | tf_op jit(solution)/shard_map/all_to_all | solution.py:355
  100.5 1.1 copy.68
  101.6 1.6 collective-permute-start.3
  103.8 2.5 collective-permute-done.3.gate_far
  106.3 1.2 copy-done.2
  107.4 1.1 collective-permute-done.4.up_far
  108.5 1.2 copy-done.3
  109.8 1.1 collective-permute-done.5.down_far
  110.9 51.2 %all-gather.5.cloned.1.call-done.rows = bf16[8,2,80,2048]{3,2,1,0:T(8,128)(2,1)} async-done(((bf16[1,2,80,2048]{3,2,1,0:T(8,128)(2,1)}), bf16[8,2,80,2048]{3,2,1,0:T(8,128)(2,1)}) %all-gather.5.cloned.1.call-update) | async-done | bytes 5242896 | tf_op jit(solution)/shard_map/all_gather | solution.py:360
  162.1 13.9 %run_experts.1 = bf16[8,2,80,2048]{3,2,1,0:T(8,128)(2,1)} custom-call(bf16[8,2,80,2048]{3,2,1,0:T(8,128)(2,1)} %all-gather.5.cloned.1.call-done.rows, bf16[2,192,2048]{2,1,0:T(8,128)(2,1)} %bitcast.37, bf16[2,192,2048]{2,1,0:T(8,128)(2,1)} %copy-done.2, bf16[2,192,2048]{2,1,0:T(8,128)(2,1)} %bitcast.40, bf16[2,192,2048]{2,1,0:T(8,128)(2,1)} %copy-done.3, ...), custom_call_target="tpu_custom_call" | custom-call | tf_op jit(solution)/shard_map/run_experts/pallas_call | solution.py:254
  176.1 64.1 %reduce-scatter.2.cloned.1.call-done = bf16[1,2,80,2048]{3,2,1,0:T(8,128)(2,1)} async-done(((bf16[8,2,80,2048]{3,2,1,0:T(8,128)(2,1)}), bf16[1,2,80,2048]{3,2,1,0:T(8,128)(2,1)}) %reduce-scatter.2.cloned.1.call-update) | async-done | bytes 655376 | tf_op jit(solution)/shard_map/reduce_scatter | solution.py:372
  240.2 2.6 copy.79
  242.8 6.7 %all-to-all-start.2 = ((bf16[16,2,5,2048]{3,1,2,0:T(2,128)(2,1)}), bf16[16,2,5,2048]{3,1,2,0:T(2,128)(2,1)S(1)}, u32[]{:S(2)}, u32[]{:S(2)}) async-start(bf16[16,2,5,2048]{3,1,2,0:T(2,128)(2,1)} %bitcast.35), calls=%async_computation.3 | async-start | bytes 1310720 | tf_op jit(solution)/shard_map/all_to_all | solution.py:376
  249.4 2.2 fusion.14
  251.6 1.6 convolution_add_fusion
  253.3 8.0 %all-to-all-done.2 = bf16[16,2,5,2048]{3,1,2,0:T(2,128)(2,1)S(1)} async-done(((bf16[16,2,5,2048]{3,1,2,0:T(2,128)(2,1)}), bf16[16,2,5,2048]{3,1,2,0:T(2,128)(2,1)S(1)}, u32[]{:S(2)}, u32[]{:S(2)}) %all-to-all-start.2) | async-done | bytes 655392 | tf_op jit(solution)/shard_map/all_to_all | solution.py:376
  262.4 0.9 add_convert_fusion
  (59 shorter events, 4.6 us)
Async XLA Ops:
  6.5 245.1 %copy-start = (bf16[256,2048]{1,0:T(8,128)(2,1)S(1)}, bf16[256,2048]{1,0:T(8,128)(2,1)}, u32[]{:S(2)}) copy-start(bf16[256,2048]{1,0:T(8,128)(2,1)} %param.47) | copy-start | bytes 3145732
  6.5 68.1 %all-gather.3.cloned.1.call-start = ((), (), s32[]{:S(2)}) async-start(), calls=%async_computation.4 | async-start | bytes 8912896 | tf_op jit(solution)/shard_map/all_gather | solution.py:312
  8.5 9.7 %copy-start.14 = (s32[64,2]{0,1:T(2,128)S(1)}, s32[64,2]{0,1:T(2,128)}, u32[]{:S(2)}) copy-start(s32[64,2]{0,1:T(2,128)} %param.40) | copy-start | bytes 1540
  12.6 10.1 %collective-permute-start.2 = (bf16[192,1024]{1,0:T(8,128)(2,1)}, bf16[192,1024]{1,0:T(8,128)(2,1)S(1)}, u32[]{:S(2)}, u32[]{:S(2)}) collective-permute-start(bf16[192,1024]{1,0:T(8,128)(2,1)} %get-tuple-element.10.refs_1_), channel_id=1, source_target_pairs={{0,16},{16,32},{32,48},{48,0},{64,80},{80,96},{96,112},{112,64},{1... | collective-permute-start | bytes 1179656 | tf_op jit(solution)/shard_map/ppermute | solution.py:270
  14.6 20.0 %collective-permute-start = (bf16[192,1024]{1,0:T(8,128)(2,1)}, bf16[192,1024]{1,0:T(8,128)(2,1)S(1)}, u32[]{:S(2)}, u32[]{:S(2)}) collective-permute-start(bf16[192,1024]{1,0:T(8,128)(2,1)} %get-tuple-element.10.refs_1_), channel_id=1, source_target_pairs={{0,32},{16,48},{32,0},{48,16},{64,96},{80,112},{96,64},{112,80},{1... | collective-permute-start | bytes 1179656 | tf_op jit(solution)/shard_map/ppermute | solution.py:270
  17.0 17.6 %collective-permute-start.1 = (bf16[192,1024]{1,0:T(8,128)(2,1)}, bf16[192,1024]{1,0:T(8,128)(2,1)S(1)}, u32[]{:S(2)}, u32[]{:S(2)}) collective-permute-start(bf16[192,1024]{1,0:T(8,128)(2,1)} %get-tuple-element.10.refs_1_), channel_id=1, source_target_pairs={{0,48},{16,0},{32,16},{48,32},{64,112},{80,64},{96,80},{112,96},{1... | collective-permute-start | bytes 1179656 | tf_op jit(solution)/shard_map/ppermute | solution.py:270
  22.7 0.7 copy-start.7
  34.6 0.7 copy-start.5
  34.6 0.9 copy-start.6
  35.5 24.4 %copy-start.15 = (f32[64,2]{0,1:T(2,128)S(1)}, f32[64,2]{0,1:T(2,128)}, u32[]{:S(2)}) copy-start(f32[64,2]{0,1:T(2,128)} %param.41) | copy-start | bytes 1540
  35.5 39.1 %copy-start.8 = (bf16[64,2048]{1,0:T(8,128)(2,1)S(1)}, bf16[64,2048]{1,0:T(8,128)(2,1)}, u32[]{:S(2)}) copy-start(bf16[64,2048]{1,0:T(8,128)(2,1)} %param.25) | copy-start | bytes 786436
  47.2 26.6 %all-to-all-start = ((bf16[16,64,128]{2,1,0:T(8,128)(2,1)}), bf16[16,64,128]{2,1,0:T(8,128)(2,1)S(1)}, u32[]{:S(2)}, u32[]{:S(2)}) async-start(bf16[16,64,128]{2,1,0:T(8,128)(2,1)} %bitcast.41), calls=%async_computation | async-start | bytes 524288 | tf_op jit(solution)/shard_map/all_to_all | solution.py:330
  59.2 102.9 %all-gather.5.cloned.1.call-start = ((), (), s32[]{:S(2)}) async-start(), calls=%async_computation.5 | async-start | bytes 5898240 | tf_op jit(solution)/shard_map/all_gather | solution.py:360
  60.6 19.3 %copy-start.10 = (f32[2048]{0:T(1024)S(1)}, f32[2048]{0:T(1024)}, u32[]{:S(2)}) copy-start(f32[2048]{0:T(1024)} %param.39) | copy-start | bytes 24580
  60.6 19.3 %copy-start.11 = (f32[2048]{0:T(1024)S(1)}, f32[2048]{0:T(1024)}, u32[]{:S(2)}) copy-start(f32[2048]{0:T(1024)} %param.38) | copy-start | bytes 24580
  81.5 20.1 %copy-start.1 = (bf16[2,2048,192]{1,2,0:T(8,128)(2,1)S(1)}, bf16[2,2048,192]{1,2,0:T(8,128)(2,1)}, u32[]{:S(2)}) copy-start(bf16[2,2048,192]{1,2,0:T(8,128)(2,1)} %param.42) | copy-start | bytes 4718596
  101.6 138.6 %reduce-scatter.2.cloned.1.call-start = ((), (), s32[]{:S(2)}) async-start(), calls=%async_computation.6 | async-start | bytes 5898240 | tf_op jit(solution)/shard_map/reduce_scatter | solution.py:372
  101.6 4.7 %collective-permute-start.3 = (bf16[2,192,2048]{2,1,0:T(8,128)(2,1)S(1)}, bf16[2,192,2048]{2,1,0:T(8,128)(2,1)S(1)}, u32[]{:S(2)}, u32[]{:S(2)}) collective-permute-start(bf16[2,192,2048]{2,1,0:T(8,128)(2,1)S(1)} %bitcast.38), channel_id=1, source_target_pairs={{0,1},{1,0},{2,3},{3,2},{4,5},{5,4},{6,7},{7,6},{8,9},{9,8},{10,11... | collective-permute-start | bytes 4718600 | tf_op jit(solution)/shard_map/ppermute | solution.py:265
  103.3 5.3 %collective-permute-start.4 = (bf16[2,192,2048]{2,1,0:T(8,128)(2,1)}, bf16[2,192,2048]{2,1,0:T(8,128)(2,1)S(1)}, u32[]{:S(2)}, u32[]{:S(2)}) collective-permute-start(bf16[2,192,2048]{2,1,0:T(8,128)(2,1)} %bitcast.39), channel_id=1, source_target_pairs={{0,1},{1,0},{2,3},{3,2},{4,5},{5,4},{6,7},{7,6},{8,9},{9,8},{10,11... | collective-permute-start | bytes 4718600 | tf_op jit(solution)/shard_map/ppermute | solution.py:265
  103.4 7.6 %collective-permute-start.5 = (bf16[2,192,2048]{2,1,0:T(8,128)(2,1)}, bf16[2,192,2048]{2,1,0:T(8,128)(2,1)}, u32[]{:S(2)}, u32[]{:S(2)}) collective-permute-start(bf16[2,192,2048]{2,1,0:T(8,128)(2,1)} %down.1), channel_id=1, source_target_pairs={{0,1},{1,0},{2,3},{3,2},{4,5},{5,4},{6,7},{7,6},{8,9},{9,8},{10,11... | collective-permute-start | bytes 4718600 | tf_op jit(solution)/shard_map/ppermute | solution.py:265
  106.3 1.2 copy-start.2
  108.5 1.2 copy-start.3
  242.8 8.8 %copy-start.4 = (bf16[2048,256]{1,0:T(8,128)(2,1)S(1)}, bf16[2048,256]{1,0:T(8,128)(2,1)}, u32[]{:S(2)}) copy-start(bf16[2048,256]{1,0:T(8,128)(2,1)} %param.46) | copy-start | bytes 3145732
  242.8 18.5 %all-to-all-start.2 = ((bf16[16,2,5,2048]{3,1,2,0:T(2,128)(2,1)}), bf16[16,2,5,2048]{3,1,2,0:T(2,128)(2,1)S(1)}, u32[]{:S(2)}, u32[]{:S(2)}) async-start(bf16[16,2,5,2048]{3,1,2,0:T(2,128)(2,1)} %bitcast.35), calls=%async_computation.3 | async-start | bytes 1310720 | tf_op jit(solution)/shard_map/all_to_all | solution.py:376
  253.3 8.6 %copy-start.9 = (bf16[64,160]{1,0:T(8,128)(2,1)S(1)}, bf16[64,160]{1,0:T(8,128)(2,1)}, u32[]{:S(2)}) copy-start(bf16[64,160]{1,0:T(8,128)(2,1)} %get-tuple-element.14) | copy-start | bytes 61444
  261.5 0.9 copy-start.12
  261.5 0.9 copy-start.13
Sparse Core Ops, SparseCore 0:
  9.2 65.3 all-gather.2
  101.7 60.3 all-gather.4
  176.2 63.9 reduce-scatter.1

commit v7 on v6

--- a/solution.py
+++ b/solution.py
@@ -249,11 +249,11 @@
 
 def run_experts(rows, *weights):
     sources, experts, slots, width = rows.shape
-    block = pl.BlockSpec((sources // 2, 1, slots, width), lambda e, r: (r, e, 0, 0))
-    weight = pl.BlockSpec((1, *weights[0].shape[1:]), lambda e, r: (e, 0, 0))
+    block = pl.BlockSpec((sources, 1, slots, width), lambda e: (0, e, 0, 0))
+    weight = pl.BlockSpec((1, *weights[0].shape[1:]), lambda e: (e, 0, 0))
     return pl.pallas_call(
         expert_kernel,
-        grid=(experts, 2),
+        grid=(experts,),
         out_shape=jax.ShapeDtypeStruct(rows.shape, jnp.bfloat16),
         in_specs=[block] + [weight] * len(weights),
         out_specs=block,

time: 270 us -> 270 us (level)
  no operation moved by 1% of the time
where the time goes in v7:
time: 270 us; the launch traced here: 269 us
  waiting for transfers between devices  146 us (54%)
  Pallas kernels  42 us (16%)
  starting transfers between devices  26.5 us (10%)
  blocking collectives  19 us (7%)
  between operations  13.3 us (5%)
  local copies, waits for them, and re-layouts  9.74 us (4%)
  matrix products  9.55 us (4%)
    reduce_scatter x1, waiting for transfers between devices, local(): lax.psum_scatter(partial_value, 'tp', scatter_dimension=0, tiled=False, a...  64.1 us
    all_gather x1, waiting for transfers between devices, local(): lax.all_gather(slab, 'tp', axis=0, tiled=False, axis_index_groups=core_li...  51.2 us
    pallas_call x2, Pallas kernels, attend(): pl.pallas_call(functools.partial(attend_kernel, pieces=len(packs), resume...  22.9 us
    all_to_all x1, blocking collectives, local(): lax.all_to_all(outgoing, 'sp', split_axis=0, concat_axis=0, tiled=True)  19 us
    all_to_all x1, waiting for transfers between devices, local(): lax.all_to_all(mixed, 'tp', split_axis=0, concat_axis=1, tiled=True)  13.1 us
    pallas_call x1, Pallas kernels, run_experts(): pl.pallas_call(expert_kernel, grid=(experts,), out_shape=jax.ShapeDtypeSt...  13.1 us
    all_to_all x1, starting transfers between devices, local(): lax.all_to_all(mixed, 'tp', split_axis=0, concat_axis=1, tiled=True)  12 us
    all_to_all x1, waiting for transfers between devices, local(): lax.all_to_all(jnp.transpose(summed, (2, 0, 1, 3)), 'sp', split_axis=0, c...  7.96 us
  transfers between devices with their start and end apart: 11, of which 9 were waited for; matrix products, arithmetic and copies ran while one was open for 2% of the time, Pallas kernels for 10%

profile of v7, /device:TPU:1, one launch (start us, length us, event | category | flops | bytes accessed | tf_op | source)
XLA Modules:
  0.0 269.0 jit_solution(8605101318426211649)
XLA Ops:
  6.5 2.0 stack_rows.1
  8.5 4.0 %prepare_heads.1 = (bf16[128,3072]{1,0:T(8,128)(2,1)}, bf16[192,1024]{1,0:T(8,128)(2,1)}) custom-call(bf16[64,1024]{1,0:T(8,128)(2,1)} %bitcast.43, bf16[64,1024]{1,0:T(8,128)(2,1)} %bitcast.44, bf16[1024,256]{1,0:T(8,128)(2,1)} %wk.1, bf16[1024,256]{1,0:T(8,128)(2,1)} %nk.1, bf16[1024,256]{1,0:T(8,128)(2,1)} %wv.1, bf16[1024,256]{1,0:T(8,128)(2,1)} %nv.1, ...), custom_call_target="tpu_custom_call" | custom-call | tf_op jit(solution)/shard_map/prepare_heads/pallas_call | solution.py:96
  12.6 2.0 collective-permute-start.2
  14.6 2.5 collective-permute-start
  17.0 1.2 collective-permute-start.1
  18.4 4.3 %collective-permute-done.2.refs_2_ = bf16[192,1024]{1,0:T(8,128)(2,1)S(1)} collective-permute-done((bf16[192,1024]{1,0:T(8,128)(2,1)}, bf16[192,1024]{1,0:T(8,128)(2,1)S(1)}, u32[]{:S(2)}, u32[]{:S(2)}) %collective-permute-start.2) | collective-permute-done | bytes 393248 | tf_op jit(solution)/shard_map/ppermute | solution.py:270
  22.7 0.7 copy-done.7
  23.4 11.2 %attend_first.1 = (f32[12,112,256]{2,1,0:T(8,128)}, f32[12,8,256]{2,1,0:T(8,128)}) custom-call(bf16[128,3072]{1,0:T(8,128)(2,1)} %get-tuple-element.9.refs_0_, bf16[192,1024]{1,0:T(8,128)(2,1)} %get-tuple-element.10.refs_1_, bf16[192,1024]{1,0:T(8,128)(2,1)} %copy-done.7), custom_call_target="tpu_custom_call" | custom-call | tf_op jit(solution)/shard_map/attend_first/pallas_call | solution.py:209
  35.5 11.7 %attend_rest.1 = bf16[1024,128]{1,0:T(8,128)(2,1)} custom-call(bf16[128,3072]{1,0:T(8,128)(2,1)} %get-tuple-element.9.refs_0_, bf16[192,1024]{1,0:T(8,128)(2,1)} %copy-done.5, bf16[192,1024]{1,0:T(8,128)(2,1)} %copy-done.6, f32[12,112,256]{2,1,0:T(8,128)} %get-tuple-element.11.refs_3_, f32[12,8,256]{2,1,0:T(8,128)} %get-tuple-element.12.refs_4_), custom_call_target="tpu_custom_call" | custom-call | tf_op jit(solution)/shard_map/attend_rest/pallas_call | solution.py:209
  47.2 12.0 %all-to-all-start = ((bf16[16,64,128]{2,1,0:T(8,128)(2,1)}), bf16[16,64,128]{2,1,0:T(8,128)(2,1)S(1)}, u32[]{:S(2)}, u32[]{:S(2)}) async-start(bf16[16,64,128]{2,1,0:T(8,128)(2,1)} %bitcast.41), calls=%async_computation | async-start | bytes 524288 | tf_op jit(solution)/shard_map/all_to_all | solution.py:330
  59.9 0.7 convert_reduce_fusion
  60.6 13.1 %all-to-all-done = bf16[16,64,128]{2,1,0:T(8,128)(2,1)S(1)} async-done(((bf16[16,64,128]{2,1,0:T(8,128)(2,1)}), bf16[16,64,128]{2,1,0:T(8,128)(2,1)S(1)}, u32[]{:S(2)}, u32[]{:S(2)}) %all-to-all-start) | async-done | bytes 262176 | tf_op jit(solution)/shard_map/all_to_all | solution.py:330
  73.8 0.8 all-gather.3.cloned.1.call-done
  74.6 5.1 %fusion.12 = (f32[64]{0:T(128)S(1)}, f32[64,2048]{1,0:T(8,128)S(1)}) fusion(bf16[2048,2048]{1,0:T(8,128)(2,1)} %all-gather.3.cloned.1.call-done, bf16[64,2048]{1,0:T(8,128)(2,1)S(1)} %copy-done.8, bf16[16,64,128]{2,1,0:T(8,128)(2,1)S(1)} %all-to-all-done), kind=kOutput, calls=%fused_computation.32 | convolution fusion | flops 537395136 | bytes 9437440 | tf_op jit(solution)/shard_map/dot_general | solution.py:331
  80.7 0.7 copy.67
  81.5 19.0 %all_to_all.29 = bf16[16,2,5,2048]{3,1,2,0:T(2,128)(2,1)S(1)} all-to-all(bf16[16,2,5,2048]{3,1,2,0:T(2,128)(2,1)S(1)} %copy.67), channel_id=1, replica_groups=mesh['sp'=16,'tp'=16] {'sp'}, dimensions={0} | all-to-all | bytes 1310720 | tf_op jit(solution)/shard_map/all_to_all | solution.py:355
  100.5 1.1 copy.68
  101.6 1.6 collective-permute-start.3
  103.8 2.5 collective-permute-done.3.gate_far
  106.3 1.2 copy-done.2
  107.4 1.1 collective-permute-done.4.up_far
  108.5 1.2 copy-done.3
  109.8 1.1 collective-permute-done.5.down_far
  110.9 51.2 %all-gather.5.cloned.1.call-done.rows = bf16[8,2,80,2048]{3,2,1,0:T(8,128)(2,1)} async-done(((bf16[1,2,80,2048]{3,2,1,0:T(8,128)(2,1)}), bf16[8,2,80,2048]{3,2,1,0:T(8,128)(2,1)}) %all-gather.5.cloned.1.call-update) | async-done | bytes 5242896 | tf_op jit(solution)/shard_map/all_gather | solution.py:360
  162.1 13.1 %run_experts.1 = bf16[8,2,80,2048]{3,2,1,0:T(8,128)(2,1)} custom-call(bf16[8,2,80,2048]{3,2,1,0:T(8,128)(2,1)} %all-gather.5.cloned.1.call-done.rows, bf16[2,192,2048]{2,1,0:T(8,128)(2,1)} %bitcast.37, bf16[2,192,2048]{2,1,0:T(8,128)(2,1)} %copy-done.2, bf16[2,192,2048]{2,1,0:T(8,128)(2,1)} %bitcast.40, bf16[2,192,2048]{2,1,0:T(8,128)(2,1)} %copy-done.3, ...), custom_call_target="tpu_custom_call" | custom-call | tf_op jit(solution)/shard_map/run_experts/pallas_call | solution.py:254
  175.2 64.1 %reduce-scatter.2.cloned.1.call-done = bf16[1,2,80,2048]{3,2,1,0:T(8,128)(2,1)} async-done(((bf16[8,2,80,2048]{3,2,1,0:T(8,128)(2,1)}), bf16[1,2,80,2048]{3,2,1,0:T(8,128)(2,1)}) %reduce-scatter.2.cloned.1.call-update) | async-done | bytes 655376 | tf_op jit(solution)/shard_map/reduce_scatter | solution.py:372
  239.3 2.6 copy.79
  241.9 6.7 %all-to-all-start.2 = ((bf16[16,2,5,2048]{3,1,2,0:T(2,128)(2,1)}), bf16[16,2,5,2048]{3,1,2,0:T(2,128)(2,1)S(1)}, u32[]{:S(2)}, u32[]{:S(2)}) async-start(bf16[16,2,5,2048]{3,1,2,0:T(2,128)(2,1)} %bitcast.35), calls=%async_computation.3 | async-start | bytes 1310720 | tf_op jit(solution)/shard_map/all_to_all | solution.py:376
  248.6 2.2 fusion.14
  250.8 1.6 convolution_add_fusion
  252.4 8.0 %all-to-all-done.2 = bf16[16,2,5,2048]{3,1,2,0:T(2,128)(2,1)S(1)} async-done(((bf16[16,2,5,2048]{3,1,2,0:T(2,128)(2,1)}), bf16[16,2,5,2048]{3,1,2,0:T(2,128)(2,1)S(1)}, u32[]{:S(2)}, u32[]{:S(2)}) %all-to-all-start.2) | async-done | bytes 655392 | tf_op jit(solution)/shard_map/all_to_all | solution.py:376
  261.6 0.9 add_convert_fusion
  (59 shorter events, 4.6 us)
Async XLA Ops:
  6.5 244.2 %copy-start = (bf16[256,2048]{1,0:T(8,128)(2,1)S(1)}, bf16[256,2048]{1,0:T(8,128)(2,1)}, u32[]{:S(2)}) copy-start(bf16[256,2048]{1,0:T(8,128)(2,1)} %param.47) | copy-start | bytes 3145732
  6.5 68.1 %all-gather.3.cloned.1.call-start = ((), (), s32[]{:S(2)}) async-start(), calls=%async_computation.4 | async-start | bytes 8912896 | tf_op jit(solution)/shard_map/all_gather | solution.py:312
  8.5 9.7 %copy-start.14 = (s32[64,2]{0,1:T(2,128)S(1)}, s32[64,2]{0,1:T(2,128)}, u32[]{:S(2)}) copy-start(s32[64,2]{0,1:T(2,128)} %param.40) | copy-start | bytes 1540
  12.6 10.1 %collective-permute-start.2 = (bf16[192,1024]{1,0:T(8,128)(2,1)}, bf16[192,1024]{1,0:T(8,128)(2,1)S(1)}, u32[]{:S(2)}, u32[]{:S(2)}) collective-permute-start(bf16[192,1024]{1,0:T(8,128)(2,1)} %get-tuple-element.10.refs_1_), channel_id=1, source_target_pairs={{0,16},{16,32},{32,48},{48,0},{64,80},{80,96},{96,112},{112,64},{1... | collective-permute-start | bytes 1179656 | tf_op jit(solution)/shard_map/ppermute | solution.py:270
  14.6 20.0 %collective-permute-start = (bf16[192,1024]{1,0:T(8,128)(2,1)}, bf16[192,1024]{1,0:T(8,128)(2,1)S(1)}, u32[]{:S(2)}, u32[]{:S(2)}) collective-permute-start(bf16[192,1024]{1,0:T(8,128)(2,1)} %get-tuple-element.10.refs_1_), channel_id=1, source_target_pairs={{0,32},{16,48},{32,0},{48,16},{64,96},{80,112},{96,64},{112,80},{1... | collective-permute-start | bytes 1179656 | tf_op jit(solution)/shard_map/ppermute | solution.py:270
  17.0 17.6 %collective-permute-start.1 = (bf16[192,1024]{1,0:T(8,128)(2,1)}, bf16[192,1024]{1,0:T(8,128)(2,1)S(1)}, u32[]{:S(2)}, u32[]{:S(2)}) collective-permute-start(bf16[192,1024]{1,0:T(8,128)(2,1)} %get-tuple-element.10.refs_1_), channel_id=1, source_target_pairs={{0,48},{16,0},{32,16},{48,32},{64,112},{80,64},{96,80},{112,96},{1... | collective-permute-start | bytes 1179656 | tf_op jit(solution)/shard_map/ppermute | solution.py:270
  22.7 0.7 copy-start.7
  34.6 0.7 copy-start.5
  34.6 0.9 copy-start.6
  35.5 24.4 %copy-start.15 = (f32[64,2]{0,1:T(2,128)S(1)}, f32[64,2]{0,1:T(2,128)}, u32[]{:S(2)}) copy-start(f32[64,2]{0,1:T(2,128)} %param.41) | copy-start | bytes 1540
  35.5 39.1 %copy-start.8 = (bf16[64,2048]{1,0:T(8,128)(2,1)S(1)}, bf16[64,2048]{1,0:T(8,128)(2,1)}, u32[]{:S(2)}) copy-start(bf16[64,2048]{1,0:T(8,128)(2,1)} %param.25) | copy-start | bytes 786436
  47.2 26.6 %all-to-all-start = ((bf16[16,64,128]{2,1,0:T(8,128)(2,1)}), bf16[16,64,128]{2,1,0:T(8,128)(2,1)S(1)}, u32[]{:S(2)}, u32[]{:S(2)}) async-start(bf16[16,64,128]{2,1,0:T(8,128)(2,1)} %bitcast.41), calls=%async_computation | async-start | bytes 524288 | tf_op jit(solution)/shard_map/all_to_all | solution.py:330
  59.2 102.9 %all-gather.5.cloned.1.call-start = ((), (), s32[]{:S(2)}) async-start(), calls=%async_computation.5 | async-start | bytes 5898240 | tf_op jit(solution)/shard_map/all_gather | solution.py:360
  60.6 19.3 %copy-start.10 = (f32[2048]{0:T(1024)S(1)}, f32[2048]{0:T(1024)}, u32[]{:S(2)}) copy-start(f32[2048]{0:T(1024)} %param.39) | copy-start | bytes 24580
  60.6 19.3 %copy-start.11 = (f32[2048]{0:T(1024)S(1)}, f32[2048]{0:T(1024)}, u32[]{:S(2)}) copy-start(f32[2048]{0:T(1024)} %param.38) | copy-start | bytes 24580
  81.5 20.1 %copy-start.1 = (bf16[2,2048,192]{1,2,0:T(8,128)(2,1)S(1)}, bf16[2,2048,192]{1,2,0:T(8,128)(2,1)}, u32[]{:S(2)}) copy-start(bf16[2,2048,192]{1,2,0:T(8,128)(2,1)} %param.42) | copy-start | bytes 4718596
  101.6 137.8 %reduce-scatter.2.cloned.1.call-start = ((), (), s32[]{:S(2)}) async-start(), calls=%async_computation.6 | async-start | bytes 5898240 | tf_op jit(solution)/shard_map/reduce_scatter | solution.py:372
  101.6 4.7 %collective-permute-start.3 = (bf16[2,192,2048]{2,1,0:T(8,128)(2,1)S(1)}, bf16[2,192,2048]{2,1,0:T(8,128)(2,1)S(1)}, u32[]{:S(2)}, u32[]{:S(2)}) collective-permute-start(bf16[2,192,2048]{2,1,0:T(8,128)(2,1)S(1)} %bitcast.38), channel_id=1, source_target_pairs={{0,1},{1,0},{2,3},{3,2},{4,5},{5,4},{6,7},{7,6},{8,9},{9,8},{10,11... | collective-permute-start | bytes 4718600 | tf_op jit(solution)/shard_map/ppermute | solution.py:265
  103.3 5.3 %collective-permute-start.4 = (bf16[2,192,2048]{2,1,0:T(8,128)(2,1)}, bf16[2,192,2048]{2,1,0:T(8,128)(2,1)S(1)}, u32[]{:S(2)}, u32[]{:S(2)}) collective-permute-start(bf16[2,192,2048]{2,1,0:T(8,128)(2,1)} %bitcast.39), channel_id=1, source_target_pairs={{0,1},{1,0},{2,3},{3,2},{4,5},{5,4},{6,7},{7,6},{8,9},{9,8},{10,11... | collective-permute-start | bytes 4718600 | tf_op jit(solution)/shard_map/ppermute | solution.py:265
  103.4 7.6 %collective-permute-start.5 = (bf16[2,192,2048]{2,1,0:T(8,128)(2,1)}, bf16[2,192,2048]{2,1,0:T(8,128)(2,1)}, u32[]{:S(2)}, u32[]{:S(2)}) collective-permute-start(bf16[2,192,2048]{2,1,0:T(8,128)(2,1)} %down.1), channel_id=1, source_target_pairs={{0,1},{1,0},{2,3},{3,2},{4,5},{5,4},{6,7},{7,6},{8,9},{9,8},{10,11... | collective-permute-start | bytes 4718600 | tf_op jit(solution)/shard_map/ppermute | solution.py:265
  106.3 1.2 copy-start.2
  108.5 1.2 copy-start.3
  241.9 8.8 %copy-start.4 = (bf16[2048,256]{1,0:T(8,128)(2,1)S(1)}, bf16[2048,256]{1,0:T(8,128)(2,1)}, u32[]{:S(2)}) copy-start(bf16[2048,256]{1,0:T(8,128)(2,1)} %param.46) | copy-start | bytes 3145732
  241.9 18.4 %all-to-all-start.2 = ((bf16[16,2,5,2048]{3,1,2,0:T(2,128)(2,1)}), bf16[16,2,5,2048]{3,1,2,0:T(2,128)(2,1)S(1)}, u32[]{:S(2)}, u32[]{:S(2)}) async-start(bf16[16,2,5,2048]{3,1,2,0:T(2,128)(2,1)} %bitcast.35), calls=%async_computation.3 | async-start | bytes 1310720 | tf_op jit(solution)/shard_map/all_to_all | solution.py:376
  252.4 8.6 %copy-start.9 = (bf16[64,160]{1,0:T(8,128)(2,1)S(1)}, bf16[64,160]{1,0:T(8,128)(2,1)}, u32[]{:S(2)}) copy-start(bf16[64,160]{1,0:T(8,128)(2,1)} %get-tuple-element.14) | copy-start | bytes 61444
  260.7 0.9 copy-start.12
  260.7 0.9 copy-start.13
Sparse Core Ops, SparseCore 0:
  9.2 65.3 all-gather.2
  101.7 60.3 all-gather.4
  175.4 63.9 reduce-scatter.1
